TPU v7x, 256 devices: a whole 4x4x8 slice. The times are simulated.
256 devices in a mesh: sp: 32 (over z, x), tp: 8 (over y, core).
Axes of the slice: x: 4, y: 4, z: 8, core: 2. Of those that a mesh axis runs over, the one named last changes fastest.
Arguments:
- inputs: bfloat16 [32768, 2048], P('sp'), may hold values from -6 to 6
- w_query: bfloat16 [2048, 2048], P(None, 'tp'), may hold values from -0.125 to 0.125
- w_key: bfloat16 [2048, 2048], P(None, 'tp'), may hold values from -0.125 to 0.125
- w_value: bfloat16 [2048, 2048], P(None, 'tp'), may hold values from -0.125 to 0.125
- rel_table: float32 [16, 257], P('tp'), may hold values from -4 to 254
- out_grad: bfloat16 [32768, 2048], P('sp', 'tp'), may hold values from -6 to 6
Outputs:
- query_grad: bfloat16 [32768, 2048], P('sp', 'tp')
- key_grad: bfloat16 [32768, 2048], P('sp', 'tp')
- value_grad: bfloat16 [32768, 2048], P('sp', 'tp')
- query_weight_grad: float32 [2048, 2048], P('sp', 'tp')
- key_weight_grad: float32 [2048, 2048], P('sp', 'tp')
- value_weight_grad: float32 [2048, 2048], P('sp', 'tp')
- table_grad: float32 [16, 257], P('tp')
All inputs are finite; a program needn't handle non-finite values.
Results may differ from a plain program's by a relative error of at most 0.017.
The roundings to bfloat16 on the way count: a program that leaves them out, or rounds other values in their place, can miss the bound.
Values may be sent and summed in bfloat16 or wider, within the bound.
No kernel may reach another device: no remote copies, remote signals or barrier semaphores. Data moves between devices by JAX's collectives and lax.ppermute only.
A program may use at most 128 MiB of HBM per device.

v0:
```python
import jax
import jax.numpy as jnp
from jax import lax
from jax.experimental import pallas as pl
from jax.experimental.pallas import tpu as pltpu
from jax.sharding import Mesh
from jax.sharding import PartitionSpec as P


HDIM = 128
SEG = 64
PREV = 4
REACH = PREV * SEG
TILE = 128
BAND = REACH + TILE
SP = ("sp_0", "sp_1")
NZ, NX = 8, 4
ROWS = 64
EXTRA = 16
VMEM_LIMIT = 24 << 20
CHUNKS = 4
WIDTH = 2048 // CHUNKS
SCALE = HDIM ** (-0.5)
F32 = jnp.float32
BF16 = jnp.bfloat16


def odd_pair(i):
    return i ^ 1


def even_pair(n):
    return lambda i: (i + 1) % n if i % 2 else (i - 1) % n


XO, XE = ("sp_1", odd_pair), ("sp_1", even_pair(NX))
ZO, ZE = ("sp_0", odd_pair), ("sp_0", even_pair(NZ))
ZF = ("sp_0", lambda i: (i + NZ // 2) % NZ)
OWN = ((XO, XE, ZO, ZE, ZF), (ZO, ZE, XO, XE, ZF))
OTHER = ((XE, XO, ZO, ZE, ZF), (ZE, ZO, XO, XE, ZF))


def held_order(steps, device):
    if not steps:
        return [device]
    return held_order(steps[1:], steps[0](device)) + held_order(steps[1:], device)


def axis_codes(levels, axis):
    n = NZ if axis == "sp_0" else NX
    mine = [f for a, f in levels if a == axis]
    spots = [len(levels) - 1 - i for i, (a, _) in enumerate(levels) if a == axis]
    wanted = [0] * n
    for device in range(n):
        order = held_order(mine, device)
        assert sorted(order) == list(range(n))
        for at, unit in enumerate(order):
            wanted[unit] |= at << (4 * device)
    me = lax.axis_index(axis)
    codes = []
    for packed in wanted:
        at = jnp.int32(0)
        for device in range(n):
            at = jnp.where(me == device, jnp.int32((packed >> (4 * device)) & 15), at)
        code = jnp.int32(0)
        for i, spot in enumerate(spots):
            code = code | (((at >> (len(spots) - 1 - i)) & 1) << spot)
        codes.append(code)
    return codes


def unit_places(sequences):
    core = lax.axis_index("core")
    places = []
    for levels in sequences:
        along_z, along_x = axis_codes(levels, "sp_0"), axis_codes(levels, "sp_1")
        places.append([along_z[unit // NX] + along_x[unit % NX] for unit in range(NZ * NX)])
    return [jnp.where(core == 0, a, b) for a, b in zip(*places)]


def level_route(sequences, level):
    route = []
    for core, levels in enumerate(sequences):
        axis, f = levels[level]
        for z in range(NZ):
            for x in range(NX):
                to = f(z) * NX + x if axis == "sp_0" else z * NX + f(x)
                route.append(((z * NX + x) * 2 + core, to * 2 + core))
    return route


def exchange(block, sequences, level):
    return lax.ppermute(block, SP + ("core",), level_route(sequences, level))


def core_swap(block):
    return lax.ppermute(block, "core", [(0, 1), (1, 0)])


def dot(a, b, contract=((1,), (0,))):
    return lax.dot_general(a, b, (contract, ((), ())), preferred_element_type=F32)


def tile_grads(query, grad, key, value, key_t, value_t, bias):
    scores = dot(key, query, ((1,), (1,))) * SCALE + bias
    top = jnp.max(scores, axis=0, keepdims=True)
    raised = jnp.exp(scores - top)
    probs = raised * (1.0 / jnp.sum(raised, axis=0, keepdims=True))
    probs_low = probs.astype(BF16)
    attn_out = dot(value_t, probs_low).astype(BF16).astype(F32)
    out_dot = jnp.sum(attn_out * grad.T.astype(F32), axis=0, keepdims=True)
    value_part = dot(probs_low, grad)
    score_grad = probs * (dot(value, grad, ((1,), (1,))) - out_dot)
    score_low = score_grad.astype(BF16)
    query_part = (dot(key_t, score_low) * SCALE).T
    key_part = dot(score_low, query) * SCALE
    return score_grad, query_part, key_part, value_part


def tail_kernel(x_ref, wk_ref, wv_ref, out_ref):
    x = x_ref[...]
    out_ref[:, :256] = dot(x, wk_ref[...]).astype(BF16)
    out_ref[:, 256:] = dot(x, wv_ref[...]).astype(BF16)


def proj_kernel(x_ref, wq_ref, wk_ref, wv_ref, q_ref, k_ref, v_ref):
    x = x_ref[...]
    q_ref[...] = dot(x, wq_ref[...]).astype(BF16)
    k_ref[...] = dot(x, wk_ref[...]).astype(BF16)
    v_ref[...] = dot(x, wv_ref[...]).astype(BF16)


def first_kernel(
    q_ref, k_ref, v_ref, halo_ref, og_ref, far_ref,
    dq_ref, edge_ref, back_ref, bias_ref, pat_ref,
    k_s, v_s, kt_s, vt_s, ka_s, va_s,
):
    k_s[:REACH] = halo_ref[:, :256]
    v_s[:REACH] = halo_ref[:, 256:]
    k_s[REACH:] = k_ref[...]
    v_s[REACH:] = v_ref[...]
    kt_s[...] = k_s[...].T
    vt_s[...] = v_s[...].T
    ka_s[...] = jnp.zeros_like(ka_s)
    va_s[...] = jnp.zeros_like(va_s)
    outside = (lax.axis_index("sp_0") == 0) & (lax.axis_index("sp_1") == 0)
    u = lax.broadcasted_iota(jnp.int32, (BAND, TILE), 0)
    col = lax.broadcasted_iota(jnp.int32, (BAND, TILE), 1)
    low = jnp.where(col < SEG, 0, SEG)
    inside = (u >= low) & (u < low + REACH + SEG)
    for h in range(2):
        far = jnp.broadcast_to(far_ref[h : h + 1, :], (BAND, 512))
        skew = pltpu.roll(far, 0, 1, stride=1, stride_axis=0)[:, BAND:]
        bias_ref[h] = jnp.where(inside, skew, -jnp.inf)
    for t in range(2):
        rows = slice(t * TILE, (t + 1) * TILE)
        band = slice(t * TILE, t * TILE + BAND)
        for h in range(2):
            cols = slice(h * HDIM, (h + 1) * HDIM)
            bias = jnp.where(outside & (u < REACH - t * TILE), -jnp.inf, bias_ref[h])
            score_grad, query_part, key_part, value_part = tile_grads(
                q_ref[rows, cols], og_ref[rows, cols], k_s[band, cols], v_s[band, cols],
                kt_s[cols, band], vt_s[cols, band], bias,
            )
            if t == 0:
                pat_ref[h] = score_grad
            else:
                pat_ref[h] += score_grad
            dq_ref[rows, cols] = query_part.astype(BF16)
            ka_s[band, cols] += key_part
            va_s[band, cols] += value_part
    edge_ref[:, :256] = ka_s[REACH:]
    edge_ref[:, 256:] = va_s[REACH:]
    back_ref[:, :256] = ka_s[:REACH].astype(BF16)
    back_ref[:, 256:] = va_s[:REACH].astype(BF16)


def attn_kernel(
    q_ref, k_ref, v_ref, og_ref, bias_ref, pat_in, edge_in, dq_in,
    dq_ref, kg_ref, vg_ref, edge_ref, pat_ref,
    kt_s, vt_s, ka_s, va_s,
):
    i = pl.program_id(0)

    @pl.when(i == 0)
    def _():
        kt_s[...] = k_ref[...].T
        vt_s[...] = v_ref[...].T
        ka_s[:REACH] = edge_in[:, :256]
        va_s[:REACH] = edge_in[:, 256:]
        ka_s[REACH:] = jnp.zeros((768, 256), F32)
        va_s[REACH:] = jnp.zeros((768, 256), F32)
        pat_ref[...] = pat_in[...]
        dq_ref[:REACH] = dq_in[...]

    for t in range(2):
        rows = pl.ds(pl.multiple_of((i + 1) * REACH + t * TILE, TILE), TILE)
        band = pl.ds(pl.multiple_of(i * REACH + t * TILE, TILE), BAND)
        for h in range(2):
            cols = slice(h * HDIM, (h + 1) * HDIM)
            score_grad, query_part, key_part, value_part = tile_grads(
                q_ref[rows, cols], og_ref[rows, cols], k_ref[band, cols], v_ref[band, cols],
                kt_s[cols, band], vt_s[cols, band], bias_ref[h],
            )
            pat_ref[h] += score_grad
            dq_ref[rows, cols] = query_part.astype(BF16)
            ka_s[band, cols] += key_part
            va_s[band, cols] += value_part

    @pl.when(i == 2)
    def _():
        kg_ref[...] = ka_s[:768].astype(BF16)
        vg_ref[...] = va_s[:768].astype(BF16)
        edge_ref[:, :256] = ka_s[768:]
        edge_ref[:, 256:] = va_s[768:]


def finish_kernel(kg_in, vg_in, edge_ref, back_ref, dq_ref, kg_ref, vg_ref, own_ref, swap_ref):
    kg_ref[:768] = kg_in[...]
    vg_ref[:768] = vg_in[...]
    kg_ref[768:] = (edge_ref[:, :256] + back_ref[:, :256].astype(F32)).astype(BF16)
    vg_ref[768:] = (edge_ref[:, 256:] + back_ref[:, 256:].astype(F32)).astype(BF16)
    core = lax.axis_index("core")

    @pl.when(core == 0)
    def _():
        own_ref[:, :256] = kg_ref[...]
        own_ref[:, 256:] = dq_ref[:, :128]
        swap_ref[:, :256] = vg_ref[...]
        swap_ref[:, 256:] = dq_ref[:, 128:]

    @pl.when(core == 1)
    def _():
        own_ref[:, :256] = vg_ref[...]
        own_ref[:, 256:] = dq_ref[:, 128:]
        swap_ref[:, :256] = kg_ref[...]
        swap_ref[:, 256:] = dq_ref[:, :128]


def store_units(value, chunk, places, out_s):
    units = WIDTH // ROWS
    for i in range(units):
        at = pl.multiple_of(places[chunk * units + i] * ROWS, ROWS)
        out_s[pl.ds(at, ROWS), :] = value[i * ROWS : (i + 1) * ROWS].astype(BF16)


def placed_product(x_ref, grad_ref, sequences, out_s):
    places = unit_places(sequences)
    for c in range(CHUNKS):
        cols = slice(c * WIDTH, (c + 1) * WIDTH)
        store_units(dot(x_ref[:, cols], grad_ref[...], ((0,), (0,))), c, places, out_s)


def three_parts(table):
    high = table.astype(BF16).astype(F32)
    mid = (table - high).astype(BF16).astype(F32)
    low = table - high - mid
    rest = jnp.zeros((EXTRA - 6, table.shape[1]), F32)
    return jnp.concatenate([high, mid, low, rest], axis=0).astype(BF16)


def table_of(parts):
    parts = parts.astype(F32)
    return parts[0:2] + parts[2:4] + parts[4:6]


def copy_out(pairs, sem):
    copies = [pltpu.make_async_copy(src, dst, sem.at[i]) for i, (src, dst) in enumerate(pairs)]
    for copy in copies:
        copy.start()
    for copy in copies:
        copy.wait()


def own_kernel(x_ref, grad_ref, pat_ref, send_hbm, keep_hbm, table_ref, out_s, parts_s, diag_s, sem):
    placed_product(x_ref, grad_ref, OWN, out_s)
    for h in range(2):
        diag_s[...] = jnp.zeros_like(diag_s)
        for a in range(BAND // 8):
            off = BAND - 8 * a
            diag_s[:, off : off + TILE] += pat_ref[h, 8 * a : 8 * a + 8, :]
        total = jnp.zeros((1, 512), F32)
        for s in range(8):
            total += diag_s[s : s + 1, s : s + 512]
        far = jnp.sum(total[:, 256:], axis=1, keepdims=True)
        table_ref[h : h + 1, :256] = total[:, :256]
        table_ref[h : h + 1, 256:] = jnp.broadcast_to(far, (1, 128))
    parts_s[...] = three_parts(table_ref[...])
    copy_out(
        [(out_s.at[:1024], send_hbm.at[:1024]), (parts_s, send_hbm.at[1024:]), (out_s.at[1024:], keep_hbm)],
        sem,
    )


def other_kernel(x_ref, grad_ref, send_hbm, keep_hbm, out_s, sem):
    placed_product(x_ref, grad_ref, OTHER, out_s)
    copy_out([(out_s.at[:1024], send_hbm), (out_s.at[1024:], keep_hbm)], sem)


def added(keep, got):
    return keep.astype(F32) + got.astype(F32)


def level_kernel(keep_ref, got_ref, table_in, send_ref, next_ref, table_ref):
    half = next_ref.shape[0]
    n = 2 * half
    total = table_in[...] + table_of(got_ref[n:, :384])
    table_ref[...] = total
    send_ref[:half] = added(keep_ref[:half], got_ref[:half]).astype(BF16)
    next_ref[...] = added(keep_ref[half:], got_ref[half:n]).astype(BF16)
    send_ref[half:, :384] = three_parts(total)
    if send_ref.shape[1] > 384:
        send_ref[half:, 384:] = jnp.zeros((EXTRA, send_ref.shape[1] - 384), BF16)


def merge_kernel(keep_ref, got_ref, keep2_ref, got2_ref, table_in, send_ref, next_ref, table_ref):
    half = next_ref.shape[0]
    n = 2 * half
    total = table_in[...] + table_of(got_ref[n:])
    table_ref[...] = total
    send_ref[:half, :384] = added(keep_ref[:half], got_ref[:half]).astype(BF16)
    send_ref[:half, 384:] = added(keep2_ref[:half], got2_ref[:half]).astype(BF16)
    next_ref[:, :384] = added(keep_ref[half:], got_ref[half:n]).astype(BF16)
    next_ref[:, 384:] = added(keep2_ref[half:], got2_ref[half:]).astype(BF16)
    send_ref[half:, :384] = three_parts(total)
    send_ref[half:, 384:] = jnp.zeros((EXTRA, 384), BF16)


def last_kernel(keep_ref, got_ref, table_in, own_ref, swap_ref, table_ref):
    n = keep_ref.shape[0]
    table_ref[...] = table_in[...] + table_of(got_ref[n:, :384])
    own_ref[...] = added(keep_ref[:, :384], got_ref[:n, :384])
    swap_ref[...] = added(keep_ref[:, 384:], got_ref[:n, 384:])


def output_kernel(own_ref, got_ref, q_ref, k_ref, v_ref):
    core = lax.axis_index("core")

    @pl.when(core == 0)
    def _():
        k_ref[...] = own_ref[:, :256]
        v_ref[...] = got_ref[:, :256]
        q_ref[:, :128] = own_ref[:, 256:]
        q_ref[:, 128:] = got_ref[:, 256:]

    @pl.when(core == 1)
    def _():
        v_ref[...] = own_ref[:, :256]
        k_ref[...] = got_ref[:, :256]
        q_ref[:, 128:] = own_ref[:, 256:]
        q_ref[:, :128] = got_ref[:, 256:]


def sds(shape, dtype):
    return jax.ShapeDtypeStruct(shape, dtype)


def whole(shape):
    return pl.BlockSpec(shape, lambda *_: (0,) * len(shape))


def cost(flops, byte_count):
    return pl.CostEstimate(flops=flops, bytes_accessed=byte_count, transcendentals=0)


def params():
    return pltpu.CompilerParams(dimension_semantics=("arbitrary",), vmem_limit_bytes=VMEM_LIMIT)


def call(kernel, operands, outs, scratch=(), grid=(1,), flops=1 << 20, blocks=None, any_outs=()):
    specs = [whole(x.shape) for x in operands]
    for at, shape in (blocks or {}).items():
        specs[at] = whole(shape)
    out_specs = [pl.BlockSpec(memory_space=pl.ANY) if i in any_outs else whole(x.shape) for i, x in enumerate(outs)]
    moved = sum(x.size * x.dtype.itemsize for x in (*operands, *outs))
    return pl.pallas_call(
        kernel,
        grid=grid,
        in_specs=specs,
        out_specs=out_specs,
        out_shape=list(outs),
        scratch_shapes=list(scratch),
        compiler_params=params(),
        cost_estimate=cost(flops, moved),
    )(*operands)


def neighbour(block, distance):
    count = NZ * NX
    route = [(i, i + distance) for i in range(count) if 0 <= i + distance < count]
    return lax.ppermute(block, SP, route)


def staged(inputs, w_query, w_key, w_value, rel_table, out_grad):
    f32, b16 = (lambda *s: sds(s, F32)), (lambda *s: sds(s, BF16))
    v32, v16 = (lambda *s: pltpu.VMEM(s, F32)), (lambda *s: pltpu.VMEM(s, BF16))
    tile_flops = 6 * 2 * TILE * BAND * HDIM
    (tail,) = call(
        tail_kernel, (inputs[1024 - REACH :], w_key, w_value), (b16(REACH, 512),), flops=2 * 256 * 2048 * 512
    )
    halo = neighbour(tail, 1)
    far = jnp.pad(rel_table, ((0, 0), (0, 512 - rel_table.shape[1])), mode="edge")
    query, key, value = call(
        proj_kernel, (inputs, w_query, w_key, w_value), (b16(1024, 256),) * 3,
        flops=2 * 1024 * 2048 * 768,
    )
    block = (REACH, 256)
    dq0, edge, back, bias, pat = call(
        first_kernel, (query, key, value, halo, out_grad, far),
        (b16(REACH, 256), f32(REACH, 512), b16(REACH, 512), f32(2, BAND, TILE), f32(2, BAND, TILE)),
        (v16(512, 256), v16(512, 256), v16(256, 512), v16(256, 512), v32(512, 256), v32(512, 256)),
        flops=4 * tile_flops, blocks={0: block, 1: block, 2: block, 4: block},
    )
    back = neighbour(back, -1)
    dq, kg, vg, edge, pat = call(
        attn_kernel, (query, key, value, out_grad, bias, pat, edge, dq0),
        (b16(1024, 256), b16(768, 256), b16(768, 256), f32(REACH, 512), f32(2, BAND, TILE)),
        (v16(256, 1024), v16(256, 1024), v32(1024, 256), v32(1024, 256)),
        grid=(3,), flops=12 * tile_flops,
    )
    kg, vg, own, swap = call(finish_kernel, (kg, vg, edge, back, dq), (b16(1024, 256),) * 2 + (b16(1024, 384),) * 2)
    got = core_swap(swap)
    sem = pltpu.SemaphoreType.DMA((3,))
    product = 2 * 1024 * 2048 * 384
    send, keep, table = call(
        own_kernel, (inputs, own, pat), (b16(1024 + EXTRA, 384), b16(1024, 384), f32(2, 384)),
        (v16(2048, 384), v16(EXTRA, 384), v32(8, 640), sem), flops=product, any_outs=(0, 1),
    )
    send2, keep2 = call(
        other_kernel, (inputs, got), (b16(1024, 384),) * 2, (v16(2048, 384), sem),
        flops=product, any_outs=(0, 1),
    )
    got = exchange(send, OWN, 0)
    got2 = exchange(send2, OTHER, 0)
    send, keep, table = call(level_kernel, (keep, got, table), (b16(512 + EXTRA, 384), b16(512, 384), f32(2, 384)))
    got = exchange(send, OWN, 1)
    send2, keep2 = added(keep2[:512], got2[:512]).astype(BF16), added(keep2[512:], got2[512:]).astype(BF16)
    got2 = exchange(send2, OTHER, 1)
    send, keep, table = call(
        merge_kernel, (keep, got, keep2, got2, table), (b16(256 + EXTRA, 768), b16(256, 768), f32(2, 384))
    )
    for level, rows in ((2, 128), (3, 64)):
        got = exchange(send, OWN, level)
        send, keep, table = call(
            level_kernel, (keep, got, table),
            (b16(rows + EXTRA, 768), b16(rows, 768), f32(2, 384)),
        )
    got = exchange(send, OWN, 4)
    own, swap, table = call(last_kernel, (keep, got, table), (f32(64, 384), f32(64, 384), f32(2, 384)))
    got = core_swap(swap)
    dwq, dwk, dwv = call(output_kernel, (own, got), (f32(64, 256),) * 3)
    return dq, kg, vg, dwq, dwk, dwv, table[:, : rel_table.shape[1]]


def solution(mesh):
    torus = Mesh(mesh.devices.reshape(NZ, NX, -1, 2), SP + ("row", "core"))
    tp = ("row", "core")
    in_specs = (P(SP, None), P(None, tp), P(None, tp), P(None, tp), P(tp, None), P(SP, tp))
    out_specs = (P(SP, tp),) * 6 + (P(tp, None),)
    return jax.shard_map(staged, mesh=torus, in_specs=in_specs, out_specs=out_specs, check_vma=False)
```

profile of v0, /device:TPU:27, one launch (start us, length us, event | category | flops | bytes accessed | tf_op | source)
XLA Modules:
  0.0 93.7 jit_solution(10025758405085584988)
XLA Ops:
  0.6 0.0 copy-start.2
  0.6 0.0 copy-start.4
  0.7 1.5 %slice.24.x_ref = bf16[256,2048]{1,0:T(8,128)(2,1)S(1)} slice(bf16[1024,2048]{1,0:T(8,128)(2,1)} %x_ref.5), slice={[768:1024], [0:2048]} | slice | bytes 2097152 | tf_op jit(solution)/shard_map/slice | solution.py:399
  2.1 0.0 copy-start.1
  2.1 1.2 %copy-done.1 = bf16[2048,256]{1,0:T(8,128)(2,1)S(1)} copy-done((bf16[2048,256]{1,0:T(8,128)(2,1)S(1)}, bf16[2048,256]{1,0:T(8,128)(2,1)}, u32[]{:S(2)}) %copy-start.1) | copy-done | bytes 1048600
  3.4 0.0 copy-start.3
  3.4 1.2 %copy-done.3 = bf16[2048,256]{1,0:T(8,128)(2,1)S(1)} copy-done((bf16[2048,256]{1,0:T(8,128)(2,1)S(1)}, bf16[2048,256]{1,0:T(8,128)(2,1)}, u32[]{:S(2)}) %copy-start.3) | copy-done | bytes 1048600
  4.6 0.7 shard_map.118
  5.3 3.1 %collective-permute-start = (bf16[256,512]{1,0:T(8,128)(2,1)S(1)}, bf16[256,512]{1,0:T(8,128)(2,1)S(1)}, u32[]{:S(2)}, u32[]{:S(2)}) collective-permute-start(bf16[256,512]{1,0:T(8,128)(2,1)S(1)} %shard_map.118), channel_id=1, source_target_pairs={{0,8},{8,16},{16,24},{24,32},{32,40},{40,48},{48,56},{56,64},{64,7... | collective-permute-start | bytes 786440 | tf_op jit(solution)/shard_map/ppermute | solution.py:391
  8.4 0.8 slice_reduce_fusion
  9.2 0.1 reshape.19
  9.3 0.8 pad_maximum_fusion.far_ref
  10.1 0.0 copy-done.2
  10.1 0.0 copy-done.4
  10.1 0.0 copy-start.6
  10.1 2.2 %copy-done.6 = bf16[1024,2048]{1,0:T(8,128)(2,1)S(1)} copy-done((bf16[1024,2048]{1,0:T(8,128)(2,1)S(1)}, bf16[1024,2048]{1,0:T(8,128)(2,1)}, u32[]{:S(2)}) %copy-start.6) | copy-done | bytes 4194328
  12.3 0.0 copy-start.8
  12.3 1.2 %copy-done.8 = bf16[2048,256]{1,0:T(8,128)(2,1)S(1)} copy-done((bf16[2048,256]{1,0:T(8,128)(2,1)S(1)}, bf16[2048,256]{1,0:T(8,128)(2,1)}, u32[]{:S(2)}) %copy-start.8) | copy-done | bytes 1048600
  13.5 0.0 copy-start
  13.5 3.4 %shard_map.117 = (bf16[1024,256]{1,0:T(8,128)(2,1)S(1)}, bf16[1024,256]{1,0:T(8,128)(2,1)S(1)}, bf16[1024,256]{1,0:T(8,128)(2,1)S(1)}) custom-call(bf16[1024,2048]{1,0:T(8,128)(2,1)S(1)} %copy-done.6, bf16[2048,256]{1,0:T(8,128)(2,1)S(1)} %copy-done.8, bf16[2048,256]{1,0:T(8,128)(2,1)S(1)} %copy-done.2, bf16[2048,256]{1,0:T(8,128)(2,1)S(1)} %copy-done.4), custom_call_target="tpu_custom_call" | custom-call | flops 3221225472 | bytes 8912896 | tf_op jit(solution)/shard_map/pallas_call | solution.py:376
  16.9 0.0 copy-start.7
  16.9 0.0 collective-permute-done.halo_ref
  16.9 0.0 copy-done
  16.9 2.3 %shard_map.119 = (bf16[256,256]{1,0:T(8,128)(2,1)S(1)}, f32[256,512]{1,0:T(8,128)S(1)}, bf16[256,512]{1,0:T(8,128)(2,1)S(1)}, f32[2,384,128]{2,1,0:T(8,128)S(1)}, f32[2,384,128]{2,1,0:T(8,128)S(1)}) custom-call(bf16[1024,256]{1,0:T(8,128)(2,1)S(1)} %get-tuple-element.47.q_ref, bf16[1024,256]{1,0:T(8,128)(2,1)S(1)} %get-tuple-element.48.k_ref, ...), custom_call_target="tpu_custom_call" | custom-call | flops 301989888 | bytes 4067328 | tf_op jit(solution)/shard_map/pallas_call | solution.py:376
  19.3 2.2 %collective-permute-start.1 = (bf16[256,512]{1,0:T(8,128)(2,1)S(1)}, bf16[256,512]{1,0:T(8,128)(2,1)S(1)}, u32[]{:S(2)}, u32[]{:S(2)}) collective-permute-start(bf16[256,512]{1,0:T(8,128)(2,1)S(1)} %get-tuple-element.58), channel_id=1, source_target_pairs={{8,0},{16,8},{24,16},{32,24},{40,32},{48,40},{56,48},{64,56},{72,6... | collective-permute-start | bytes 786440 | tf_op jit(solution)/shard_map/ppermute | solution.py:391
  21.5 8.4 %shard_map.120 = (bf16[1024,256]{1,0:T(8,128)(2,1)}, bf16[768,256]{1,0:T(8,128)(2,1)S(1)}, bf16[768,256]{1,0:T(8,128)(2,1)S(1)}, f32[256,512]{1,0:T(8,128)S(1)}, f32[2,384,128]{2,1,0:T(8,128)S(1)}) custom-call(bf16[1024,256]{1,0:T(8,128)(2,1)S(1)} %get-tuple-element.47.q_ref, bf16[1024,256]{1,0:T(8,128)(2,1)S(1)} %get-tuple-element.48.k_ref, ...), custom_call_target="tpu_custom_call" | custom-call | flops 905969664 | bytes 5767168 | tf_op jit(solution)/shard_map/pallas_call | solution.py:376
  29.9 0.0 collective-permute-done.1.back_ref
  29.9 0.0 copy-start.5
  29.9 1.0 %copy-done.5 = bf16[1024,256]{1,0:T(8,128)(2,1)S(1)} copy-done((bf16[1024,256]{1,0:T(8,128)(2,1)S(1)}, bf16[1024,256]{1,0:T(8,128)(2,1)}, u32[]{:S(2)}) %copy-start.5) | copy-done | bytes 524312
  30.9 1.2 %shard_map.121 = (bf16[1024,256]{1,0:T(8,128)(2,1)}, bf16[1024,256]{1,0:T(8,128)(2,1)}, bf16[1024,384]{1,0:T(8,128)(2,1)S(1)}, bf16[1024,384]{1,0:T(8,128)(2,1)S(1)}) custom-call(bf16[768,256]{1,0:T(8,128)(2,1)S(1)} %get-tuple-element.55.kg_in, bf16[768,256]{1,0:T(8,128)(2,1)S(1)} %get-tuple-element.56.vg_in, f32[256,512]{1,0:T(8,128)S(1)} %get-tuple-element.57.edge_ref, ...), custom_call_target="tpu_custom_call" | custom-call | flops 1048576 | bytes 4718592 | tf_op jit(solution)/shard_map/pallas_call | solution.py:376
  32.2 1.2 %collective-permute-start.4 = (bf16[1024,384]{1,0:T(8,128)(2,1)S(1)}, bf16[1024,384]{1,0:T(8,128)(2,1)S(1)}, u32[]{:S(2)}, u32[]{:S(2)}) collective-permute-start(bf16[1024,384]{1,0:T(8,128)(2,1)S(1)} %get-tuple-element.68), channel_id=1, source_target_pairs={{0,1},{1,0},{2,3},{3,2},{4,5},{5,4},{6,7},{7,6},{8,9},{9,8},{10,11... | collective-permute-start | bytes 2359304 | tf_op jit(solution)/shard_map/ppermute | solution.py:97
  33.4 0.0 copy-done.7
  33.4 2.7 %shard_map.122 = (bf16[1040,384]{1,0:T(8,128)(2,1)S(1)}, bf16[1024,384]{1,0:T(8,128)(2,1)S(1)}, f32[2,384]{1,0:T(2,128)S(1)}) custom-call(bf16[1024,2048]{1,0:T(8,128)(2,1)S(1)} %copy-done.7, bf16[1024,384]{1,0:T(8,128)(2,1)S(1)} %get-tuple-element.61.grad_ref, f32[2,384,128]{2,1,0:T(8,128)S(1)} %get-tuple-element.62.pat_ref), custom_call_target="tpu_custom_call" | custom-call | flops 1610612736 | bytes 6962176 | tf_op jit(solution)/shard_map/pallas_call | solution.py:376
  36.1 2.0 %collective-permute-start.2 = (bf16[1040,384]{1,0:T(8,128)(2,1)S(1)}, bf16[1040,384]{1,0:T(8,128)(2,1)S(1)}, u32[]{:S(2)}, u32[]{:S(2)}) collective-permute-start(bf16[1040,384]{1,0:T(8,128)(2,1)S(1)} %get-tuple-element.64), channel_id=1, source_target_pairs={{0,8},{8,0},{16,24},{24,16},{32,40},{40,32},{48,56},{56,48},{64,72... | collective-permute-start | bytes 2396168 | tf_op jit(solution)/shard_map/ppermute | solution.py:93
  38.1 0.0 collective-permute-done.4.grad_ref
  38.1 2.6 %shard_map.124 = (bf16[1024,384]{1,0:T(8,128)(2,1)S(1)}, bf16[1024,384]{1,0:T(8,128)(2,1)S(1)}) custom-call(bf16[1024,2048]{1,0:T(8,128)(2,1)S(1)} %copy-done.7, bf16[1024,384]{1,0:T(8,128)(2,1)S(1)} %collective-permute-done.4.grad_ref), custom_call_target="tpu_custom_call" | custom-call | flops 1610612736 | bytes 6553600 | tf_op jit(solution)/shard_map/pallas_call | solution.py:376
  40.7 4.8 %collective-permute-start.5 = (bf16[1024,384]{1,0:T(8,128)(2,1)S(1)}, bf16[1024,384]{1,0:T(8,128)(2,1)S(1)}, u32[]{:S(2)}, u32[]{:S(2)}) collective-permute-start(bf16[1024,384]{1,0:T(8,128)(2,1)S(1)} %get-tuple-element.70), channel_id=1, source_target_pairs={{0,24},{8,16},{16,8},{24,0},{32,56},{40,48},{48,40},{56,32},{64,88... | collective-permute-start | bytes 2359304 | tf_op jit(solution)/shard_map/ppermute | solution.py:93
  45.4 2.5 %collective-permute-done.2.got_ref = bf16[1040,384]{1,0:T(8,128)(2,1)S(1)} collective-permute-done((bf16[1040,384]{1,0:T(8,128)(2,1)S(1)}, bf16[1040,384]{1,0:T(8,128)(2,1)S(1)}, u32[]{:S(2)}, u32[]{:S(2)}) %collective-permute-start.2) | collective-permute-done | bytes 798752 | tf_op jit(solution)/shard_map/ppermute | solution.py:93
  47.9 0.2 shard_map.123
  48.1 5.5 %collective-permute-start.3 = (bf16[528,384]{1,0:T(8,128)(2,1)S(1)}, bf16[528,384]{1,0:T(8,128)(2,1)S(1)}, u32[]{:S(2)}, u32[]{:S(2)}) collective-permute-start(bf16[528,384]{1,0:T(8,128)(2,1)S(1)} %get-tuple-element.67), channel_id=1, source_target_pairs={{0,24},{8,16},{16,8},{24,0},{32,56},{40,48},{48,40},{56,32},{64,88... | collective-permute-start | bytes 1216520 | tf_op jit(solution)/shard_map/ppermute | solution.py:93
  53.6 1.2 %collective-permute-done.5 = bf16[1024,384]{1,0:T(8,128)(2,1)S(1)} collective-permute-done((bf16[1024,384]{1,0:T(8,128)(2,1)S(1)}, bf16[1024,384]{1,0:T(8,128)(2,1)S(1)}, u32[]{:S(2)}, u32[]{:S(2)}) %collective-permute-start.5) | collective-permute-done | bytes 786464 | tf_op jit(solution)/shard_map/ppermute | solution.py:93
  54.8 0.2 add_convert_fusion
  55.0 0.1 collective-permute-start.6
  55.1 4.0 %collective-permute-done.3.got_ref = bf16[528,384]{1,0:T(8,128)(2,1)S(1)} collective-permute-done((bf16[528,384]{1,0:T(8,128)(2,1)S(1)}, bf16[528,384]{1,0:T(8,128)(2,1)S(1)}, u32[]{:S(2)}, u32[]{:S(2)}) %collective-permute-start.3) | collective-permute-done | bytes 405536 | tf_op jit(solution)/shard_map/ppermute | solution.py:93
  59.2 2.6 %collective-permute-done.6.got2_ref = bf16[512,384]{1,0:T(8,128)(2,1)S(1)} collective-permute-done((bf16[512,384]{1,0:T(8,128)(2,1)S(1)}, bf16[512,384]{1,0:T(8,128)(2,1)S(1)}, u32[]{:S(2)}, u32[]{:S(2)}) %collective-permute-start.6) | collective-permute-done | bytes 393248 | tf_op jit(solution)/shard_map/ppermute | solution.py:93
  61.8 0.2 shard_map.125
  62.0 2.6 %collective-permute-start.7 = (bf16[272,768]{1,0:T(8,128)(2,1)S(1)}, bf16[272,768]{1,0:T(8,128)(2,1)S(1)}, u32[]{:S(2)}, u32[]{:S(2)}) collective-permute-start(bf16[272,768]{1,0:T(8,128)(2,1)S(1)} %get-tuple-element.73), channel_id=1, source_target_pairs={{0,32},{8,40},{16,48},{24,56},{32,0},{40,8},{48,16},{56,24},{64,96... | collective-permute-start | bytes 1253384 | tf_op jit(solution)/shard_map/ppermute | solution.py:93
  64.6 5.4 %collective-permute-done.7.got_ref = bf16[272,768]{1,0:T(8,128)(2,1)S(1)} collective-permute-done((bf16[272,768]{1,0:T(8,128)(2,1)S(1)}, bf16[272,768]{1,0:T(8,128)(2,1)S(1)}, u32[]{:S(2)}, u32[]{:S(2)}) %collective-permute-start.7) | collective-permute-done | bytes 417824 | tf_op jit(solution)/shard_map/ppermute | solution.py:93
  70.0 0.1 shard_map.126
  70.2 0.7 collective-permute-start.8
  70.9 4.1 %collective-permute-done.8.got_ref = bf16[144,768]{1,0:T(8,128)(2,1)S(1)} collective-permute-done((bf16[144,768]{1,0:T(8,128)(2,1)S(1)}, bf16[144,768]{1,0:T(8,128)(2,1)S(1)}, u32[]{:S(2)}, u32[]{:S(2)}) %collective-permute-start.8) | collective-permute-done | bytes 221216 | tf_op jit(solution)/shard_map/ppermute | solution.py:93
  75.0 0.1 shard_map.127
  75.1 5.2 %collective-permute-start.9 = (bf16[80,768]{1,0:T(8,128)(2,1)S(1)}, bf16[80,768]{1,0:T(8,128)(2,1)S(1)}, u32[]{:S(2)}, u32[]{:S(2)}) collective-permute-start(bf16[80,768]{1,0:T(8,128)(2,1)S(1)} %get-tuple-element.79), channel_id=1, source_target_pairs={{0,128},{8,136},{16,144},{24,152},{32,160},{40,168},{48,176},{56,1... | collective-permute-start | bytes 368648 | tf_op jit(solution)/shard_map/ppermute | solution.py:93
  80.3 2.6 %collective-permute-done.9.got_ref = bf16[80,768]{1,0:T(8,128)(2,1)S(1)} collective-permute-done((bf16[80,768]{1,0:T(8,128)(2,1)S(1)}, bf16[80,768]{1,0:T(8,128)(2,1)S(1)}, u32[]{:S(2)}, u32[]{:S(2)}) %collective-permute-start.9) | collective-permute-done | bytes 122912 | tf_op jit(solution)/shard_map/ppermute | solution.py:93
  82.9 0.6 shard_map.128
  83.5 8.6 %collective-permute-start.10 = (f32[64,384]{1,0:T(8,128)S(1)}, f32[64,384]{1,0:T(8,128)S(1)}, u32[]{:S(2)}, u32[]{:S(2)}) collective-permute-start(f32[64,384]{1,0:T(8,128)S(1)} %get-tuple-element.82), channel_id=1, source_target_pairs={{0,1},{1,0},{2,3},{3,2},{4,5},{5,4},{6,7},{7,6},{8,9},{9,8},{10,11... | collective-permute-start | bytes 294920 | tf_op jit(solution)/shard_map/ppermute | solution.py:97
  92.1 0.9 %collective-permute-done.10.got_ref = f32[64,384]{1,0:T(8,128)S(1)} collective-permute-done((f32[64,384]{1,0:T(8,128)S(1)}, f32[64,384]{1,0:T(8,128)S(1)}, u32[]{:S(2)}, u32[]{:S(2)}) %collective-permute-start.10) | collective-permute-done | bytes 98336 | tf_op jit(solution)/shard_map/ppermute | solution.py:97
  93.0 0.7 shard_map.129
Async XLA Ops:
  0.6 9.4 %copy-start.2 = (bf16[2048,256]{1,0:T(8,128)(2,1)S(1)}, bf16[2048,256]{1,0:T(8,128)(2,1)}, u32[]{:S(2)}) copy-start(bf16[2048,256]{1,0:T(8,128)(2,1)} %wk_ref.3) | copy-start | bytes 3145732
  0.6 9.4 %copy-start.4 = (bf16[2048,256]{1,0:T(8,128)(2,1)S(1)}, bf16[2048,256]{1,0:T(8,128)(2,1)}, u32[]{:S(2)}) copy-start(bf16[2048,256]{1,0:T(8,128)(2,1)} %wv_ref.3) | copy-start | bytes 3145732
  2.1 1.2 %copy-start.1 = (bf16[2048,256]{1,0:T(8,128)(2,1)S(1)}, bf16[2048,256]{1,0:T(8,128)(2,1)}, u32[]{:S(2)}) copy-start(bf16[2048,256]{1,0:T(8,128)(2,1)} %wk_ref.3) | copy-start | bytes 3145732
  3.4 1.2 %copy-start.3 = (bf16[2048,256]{1,0:T(8,128)(2,1)S(1)}, bf16[2048,256]{1,0:T(8,128)(2,1)}, u32[]{:S(2)}) copy-start(bf16[2048,256]{1,0:T(8,128)(2,1)} %wv_ref.3) | copy-start | bytes 3145732
  5.3 11.6 %collective-permute-start = (bf16[256,512]{1,0:T(8,128)(2,1)S(1)}, bf16[256,512]{1,0:T(8,128)(2,1)S(1)}, u32[]{:S(2)}, u32[]{:S(2)}) collective-permute-start(bf16[256,512]{1,0:T(8,128)(2,1)S(1)} %shard_map.118), channel_id=1, source_target_pairs={{0,8},{8,16},{16,24},{24,32},{32,40},{40,48},{48,56},{56,64},{64,7... | collective-permute-start | bytes 786440 | tf_op jit(solution)/shard_map/ppermute | solution.py:391
  10.1 2.2 %copy-start.6 = (bf16[1024,2048]{1,0:T(8,128)(2,1)S(1)}, bf16[1024,2048]{1,0:T(8,128)(2,1)}, u32[]{:S(2)}) copy-start(bf16[1024,2048]{1,0:T(8,128)(2,1)} %x_ref.5) | copy-start | bytes 12582916
  12.3 1.2 %copy-start.8 = (bf16[2048,256]{1,0:T(8,128)(2,1)S(1)}, bf16[2048,256]{1,0:T(8,128)(2,1)}, u32[]{:S(2)}) copy-start(bf16[2048,256]{1,0:T(8,128)(2,1)} %wq_ref.1) | copy-start | bytes 3145732
  13.5 3.4 %copy-start = (bf16[1024,256]{1,0:T(8,128)(2,1)S(1)}, bf16[1024,256]{1,0:T(8,128)(2,1)}, u32[]{:S(2)}) copy-start(bf16[1024,256]{1,0:T(8,128)(2,1)} %og_ref.3) | copy-start | bytes 1572868
  16.9 16.5 %copy-start.7 = (bf16[1024,2048]{1,0:T(8,128)(2,1)S(1)}, bf16[1024,2048]{1,0:T(8,128)(2,1)}, u32[]{:S(2)}) copy-start(bf16[1024,2048]{1,0:T(8,128)(2,1)} %x_ref.5) | copy-start | bytes 12582916
  19.3 10.6 %collective-permute-start.1 = (bf16[256,512]{1,0:T(8,128)(2,1)S(1)}, bf16[256,512]{1,0:T(8,128)(2,1)S(1)}, u32[]{:S(2)}, u32[]{:S(2)}) collective-permute-start(bf16[256,512]{1,0:T(8,128)(2,1)S(1)} %get-tuple-element.58), channel_id=1, source_target_pairs={{8,0},{16,8},{24,16},{32,24},{40,32},{48,40},{56,48},{64,56},{72,6... | collective-permute-start | bytes 786440 | tf_op jit(solution)/shard_map/ppermute | solution.py:391
  29.9 1.0 %copy-start.5 = (bf16[1024,256]{1,0:T(8,128)(2,1)S(1)}, bf16[1024,256]{1,0:T(8,128)(2,1)}, u32[]{:S(2)}) copy-start(bf16[1024,256]{1,0:T(8,128)(2,1)} %get-tuple-element.40.dq_ref) | copy-start | bytes 1572868
  32.2 5.9 %collective-permute-start.4 = (bf16[1024,384]{1,0:T(8,128)(2,1)S(1)}, bf16[1024,384]{1,0:T(8,128)(2,1)S(1)}, u32[]{:S(2)}, u32[]{:S(2)}) collective-permute-start(bf16[1024,384]{1,0:T(8,128)(2,1)S(1)} %get-tuple-element.68), channel_id=1, source_target_pairs={{0,1},{1,0},{2,3},{3,2},{4,5},{5,4},{6,7},{7,6},{8,9},{9,8},{10,11... | collective-permute-start | bytes 2359304 | tf_op jit(solution)/shard_map/ppermute | solution.py:97
  36.1 11.8 %collective-permute-start.2 = (bf16[1040,384]{1,0:T(8,128)(2,1)S(1)}, bf16[1040,384]{1,0:T(8,128)(2,1)S(1)}, u32[]{:S(2)}, u32[]{:S(2)}) collective-permute-start(bf16[1040,384]{1,0:T(8,128)(2,1)S(1)} %get-tuple-element.64), channel_id=1, source_target_pairs={{0,8},{8,0},{16,24},{24,16},{32,40},{40,32},{48,56},{56,48},{64,72... | collective-permute-start | bytes 2396168 | tf_op jit(solution)/shard_map/ppermute | solution.py:93
  40.7 14.1 %collective-permute-start.5 = (bf16[1024,384]{1,0:T(8,128)(2,1)S(1)}, bf16[1024,384]{1,0:T(8,128)(2,1)S(1)}, u32[]{:S(2)}, u32[]{:S(2)}) collective-permute-start(bf16[1024,384]{1,0:T(8,128)(2,1)S(1)} %get-tuple-element.70), channel_id=1, source_target_pairs={{0,24},{8,16},{16,8},{24,0},{32,56},{40,48},{48,40},{56,32},{64,88... | collective-permute-start | bytes 2359304 | tf_op jit(solution)/shard_map/ppermute | solution.py:93
  48.1 11.0 %collective-permute-start.3 = (bf16[528,384]{1,0:T(8,128)(2,1)S(1)}, bf16[528,384]{1,0:T(8,128)(2,1)S(1)}, u32[]{:S(2)}, u32[]{:S(2)}) collective-permute-start(bf16[528,384]{1,0:T(8,128)(2,1)S(1)} %get-tuple-element.67), channel_id=1, source_target_pairs={{0,24},{8,16},{16,8},{24,0},{32,56},{40,48},{48,40},{56,32},{64,88... | collective-permute-start | bytes 1216520 | tf_op jit(solution)/shard_map/ppermute | solution.py:93
  55.0 6.7 %collective-permute-start.6 = (bf16[512,384]{1,0:T(8,128)(2,1)S(1)}, bf16[512,384]{1,0:T(8,128)(2,1)S(1)}, u32[]{:S(2)}, u32[]{:S(2)}) collective-permute-start(bf16[512,384]{1,0:T(8,128)(2,1)S(1)} %get-tuple-element.87), channel_id=1, source_target_pairs={{0,8},{8,0},{16,24},{24,16},{32,40},{40,32},{48,56},{56,48},{64,72... | collective-permute-start | bytes 1179656 | tf_op jit(solution)/shard_map/ppermute | solution.py:93
  62.0 8.0 %collective-permute-start.7 = (bf16[272,768]{1,0:T(8,128)(2,1)S(1)}, bf16[272,768]{1,0:T(8,128)(2,1)S(1)}, u32[]{:S(2)}, u32[]{:S(2)}) collective-permute-start(bf16[272,768]{1,0:T(8,128)(2,1)S(1)} %get-tuple-element.73), channel_id=1, source_target_pairs={{0,32},{8,40},{16,48},{24,56},{32,0},{40,8},{48,16},{56,24},{64,96... | collective-permute-start | bytes 1253384 | tf_op jit(solution)/shard_map/ppermute | solution.py:93
  70.2 4.9 %collective-permute-start.8 = (bf16[144,768]{1,0:T(8,128)(2,1)S(1)}, bf16[144,768]{1,0:T(8,128)(2,1)S(1)}, u32[]{:S(2)}, u32[]{:S(2)}) collective-permute-start(bf16[144,768]{1,0:T(8,128)(2,1)S(1)} %get-tuple-element.76), channel_id=1, source_target_pairs={{0,224},{8,232},{16,240},{24,248},{32,64},{40,72},{48,80},{56,88},... | collective-permute-start | bytes 663560 | tf_op jit(solution)/shard_map/ppermute | solution.py:93
  75.1 7.8 %collective-permute-start.9 = (bf16[80,768]{1,0:T(8,128)(2,1)S(1)}, bf16[80,768]{1,0:T(8,128)(2,1)S(1)}, u32[]{:S(2)}, u32[]{:S(2)}) collective-permute-start(bf16[80,768]{1,0:T(8,128)(2,1)S(1)} %get-tuple-element.79), channel_id=1, source_target_pairs={{0,128},{8,136},{16,144},{24,152},{32,160},{40,168},{48,176},{56,1... | collective-permute-start | bytes 368648 | tf_op jit(solution)/shard_map/ppermute | solution.py:93
  83.5 9.5 %collective-permute-start.10 = (f32[64,384]{1,0:T(8,128)S(1)}, f32[64,384]{1,0:T(8,128)S(1)}, u32[]{:S(2)}, u32[]{:S(2)}) collective-permute-start(f32[64,384]{1,0:T(8,128)S(1)} %get-tuple-element.82), channel_id=1, source_target_pairs={{0,1},{1,0},{2,3},{3,2},{4,5},{5,4},{6,7},{7,6},{8,9},{9,8},{10,11... | collective-permute-start | bytes 294920 | tf_op jit(solution)/shard_map/ppermute | solution.py:97
where the time goes:
time: 94.1 us; the launch traced here: 93.7 us
  starting transfers between devices  36 us (38%)
  waiting for transfers between devices  23.4 us (25%)
  Pallas kernels  23.3 us (25%)
  local copies, waits for them, and re-layouts  9.26 us (10%)
  other arithmetic  0.97 us (1%)
    pallas_call x13, Pallas kernels, call(): pl.pallas_call(kernel, grid=grid, in_specs=specs, out_specs=out_specs, ou...  23.3 us
    ppermute x7, waiting for transfers between devices, exchange(): return lax.ppermute(block, SP + ('core',), level_route(sequences, level))  22.5 us
    ppermute x7, starting transfers between devices, exchange(): return lax.ppermute(block, SP + ('core',), level_route(sequences, level))  20.9 us
    ppermute x2, starting transfers between devices, core_swap(): return lax.ppermute(block, 'core', [(0, 1), (1, 0)])  9.79 us
    unnamed x18, local copies, waits for them, and re-layouts  6.92 us
    ppermute x2, starting transfers between devices, neighbour(): return lax.ppermute(block, SP, route)  5.3 us
  transfers between devices with their start and end apart: 11, of which 8 were waited for; matrix products, arithmetic and copies ran while one was open for 2% of the time, Pallas kernels for 19%

commit v1 on v0

--- a/solution.py
+++ b/solution.py
@@ -18,6 +18,7 @@
 ROWS = 64
 EXTRA = 16
 VMEM_LIMIT = 24 << 20
+LOAD_LIMIT = 24 << 20
 CHUNKS = 4
 WIDTH = 2048 // CHUNKS
 SCALE = HDIM ** (-0.5)
@@ -36,8 +37,9 @@
 XO, XE = ("sp_1", odd_pair), ("sp_1", even_pair(NX))
 ZO, ZE = ("sp_0", odd_pair), ("sp_0", even_pair(NZ))
 ZF = ("sp_0", lambda i: (i + NZ // 2) % NZ)
-OWN = ((XO, XE, ZO, ZE, ZF), (ZO, ZE, XO, XE, ZF))
-OTHER = ((XE, XO, ZO, ZE, ZF), (ZE, ZO, XO, XE, ZF))
+Z3 = ("sp_0", lambda i: (3, 6, 5, 0, 7, 2, 1, 4)[i])
+OWN = ((XO, XE, ZO, ZE, Z3), (ZO, ZE, XO, XE, ZF))
+OTHER = ((XE, XO, ZO, ZE, Z3), (ZE, ZO, XO, XE, ZF))
 
 
 def held_order(steps, device):
@@ -78,19 +80,19 @@
     return [jnp.where(core == 0, a, b) for a, b in zip(*places)]
 
 
-def level_route(sequences, level):
+def level_route(sequences, level, across=0):
     route = []
     for core, levels in enumerate(sequences):
         axis, f = levels[level]
         for z in range(NZ):
             for x in range(NX):
                 to = f(z) * NX + x if axis == "sp_0" else z * NX + f(x)
-                route.append(((z * NX + x) * 2 + core, to * 2 + core))
+                route.append(((z * NX + x) * 2 + core, to * 2 + (core ^ across)))
     return route
 
 
-def exchange(block, sequences, level):
-    return lax.ppermute(block, SP + ("core",), level_route(sequences, level))
+def exchange(block, sequences, level, across=0):
+    return lax.ppermute(block, SP + ("core",), level_route(sequences, level, across))
 
 
 def core_swap(block):
@@ -117,10 +119,22 @@
     return score_grad, query_part, key_part, value_part
 
 
-def tail_kernel(x_ref, wk_ref, wv_ref, out_ref):
-    x = x_ref[...]
-    out_ref[:, :256] = dot(x, wk_ref[...]).astype(BF16)
-    out_ref[:, 256:] = dot(x, wv_ref[...]).astype(BF16)
+def load_kernel(x_hbm, wq_hbm, wk_hbm, wv_hbm, tail_ref, x_ref, wq_ref, wk_ref, wv_ref, sem):
+    top = 1024 - REACH
+    pairs = (
+        (wk_hbm, wk_ref), (wv_hbm, wv_ref), (x_hbm.at[top:], x_ref.at[top:]),
+        (wq_hbm, wq_ref), (x_hbm.at[:top], x_ref.at[:top]),
+    )
+    copies = [pltpu.make_async_copy(src, dst, sem.at[i]) for i, (src, dst) in enumerate(pairs)]
+    for copy in copies:
+        copy.start()
+    for copy in copies[:3]:
+        copy.wait()
+    x = x_ref[top:]
+    tail_ref[:, :256] = dot(x, wk_ref[...]).astype(BF16)
+    tail_ref[:, 256:] = dot(x, wv_ref[...]).astype(BF16)
+    for copy in copies[3:]:
+        copy.wait()
 
 
 def proj_kernel(x_ref, wq_ref, wk_ref, wv_ref, q_ref, k_ref, v_ref):
@@ -131,7 +145,7 @@
 
 
 def first_kernel(
-    q_ref, k_ref, v_ref, halo_ref, og_ref, far_ref,
+    q_ref, k_ref, v_ref, halo_ref, og_ref, rel_ref,
     dq_ref, edge_ref, back_ref, bias_ref, pat_ref,
     k_s, v_s, kt_s, vt_s, ka_s, va_s,
 ):
@@ -149,7 +163,9 @@
     low = jnp.where(col < SEG, 0, SEG)
     inside = (u >= low) & (u < low + REACH + SEG)
     for h in range(2):
-        far = jnp.broadcast_to(far_ref[h : h + 1, :], (BAND, 512))
+        table = rel_ref[h : h + 1, :]
+        far = jnp.concatenate([table[:, :256], jnp.broadcast_to(table[:, 256:257], (1, 256))], axis=1)
+        far = jnp.broadcast_to(far, (BAND, 512))
         skew = pltpu.roll(far, 0, 1, stride=1, stride_axis=0)[:, BAND:]
         bias_ref[h] = jnp.where(inside, skew, -jnp.inf)
     for t in range(2):
@@ -177,25 +193,20 @@
 
 def attn_kernel(
     q_ref, k_ref, v_ref, og_ref, bias_ref, pat_in, edge_in, dq_in,
-    dq_ref, kg_ref, vg_ref, edge_ref, pat_ref,
+    dq_ref, near_ref, kg_ref, vg_ref, edge_ref, pat_ref,
     kt_s, vt_s, ka_s, va_s,
 ):
-    i = pl.program_id(0)
-
-    @pl.when(i == 0)
-    def _():
-        kt_s[...] = k_ref[...].T
-        vt_s[...] = v_ref[...].T
-        ka_s[:REACH] = edge_in[:, :256]
-        va_s[:REACH] = edge_in[:, 256:]
-        ka_s[REACH:] = jnp.zeros((768, 256), F32)
-        va_s[REACH:] = jnp.zeros((768, 256), F32)
-        pat_ref[...] = pat_in[...]
-        dq_ref[:REACH] = dq_in[...]
-
-    for t in range(2):
-        rows = pl.ds(pl.multiple_of((i + 1) * REACH + t * TILE, TILE), TILE)
-        band = pl.ds(pl.multiple_of(i * REACH + t * TILE, TILE), BAND)
+    kt_s[...] = k_ref[...].T
+    vt_s[...] = v_ref[...].T
+    ka_s[:REACH] = edge_in[:, :256]
+    va_s[:REACH] = edge_in[:, 256:]
+    ka_s[REACH:] = jnp.zeros((768, 256), F32)
+    va_s[REACH:] = jnp.zeros((768, 256), F32)
+    pat_ref[...] = pat_in[...]
+    near_ref[:REACH] = dq_in[...]
+    for tile in range(6):
+        rows = slice(REACH + tile * TILE, REACH + (tile + 1) * TILE)
+        band = slice(tile * TILE, tile * TILE + BAND)
         for h in range(2):
             cols = slice(h * HDIM, (h + 1) * HDIM)
             score_grad, query_part, key_part, value_part = tile_grads(
@@ -203,16 +214,14 @@
                 kt_s[cols, band], vt_s[cols, band], bias_ref[h],
             )
             pat_ref[h] += score_grad
-            dq_ref[rows, cols] = query_part.astype(BF16)
+            near_ref[rows, cols] = query_part.astype(BF16)
             ka_s[band, cols] += key_part
             va_s[band, cols] += value_part
-
-    @pl.when(i == 2)
-    def _():
-        kg_ref[...] = ka_s[:768].astype(BF16)
-        vg_ref[...] = va_s[:768].astype(BF16)
-        edge_ref[:, :256] = ka_s[768:]
-        edge_ref[:, 256:] = va_s[768:]
+    dq_ref[...] = near_ref[...]
+    kg_ref[...] = ka_s[:768].astype(BF16)
+    vg_ref[...] = va_s[:768].astype(BF16)
+    edge_ref[:, :256] = ka_s[768:]
+    edge_ref[:, 256:] = va_s[768:]
 
 
 def finish_kernel(kg_in, vg_in, edge_ref, back_ref, dq_ref, kg_ref, vg_ref, own_ref, swap_ref):
@@ -326,29 +335,40 @@
     send_ref[half:, 384:] = jnp.zeros((EXTRA, 384), BF16)
 
 
-def last_kernel(keep_ref, got_ref, table_in, own_ref, swap_ref, table_ref):
-    n = keep_ref.shape[0]
-    table_ref[...] = table_in[...] + table_of(got_ref[n:, :384])
-    own_ref[...] = added(keep_ref[:, :384], got_ref[:n, :384])
-    swap_ref[...] = added(keep_ref[:, 384:], got_ref[:n, 384:])
-
-
-def output_kernel(own_ref, got_ref, q_ref, k_ref, v_ref):
+def split_kernel(keep_ref, got_ref, table_in, one_ref, two_ref, three_ref, own_ref, table_ref):
+    n = own_ref.shape[0]
+    total = table_in[...] + table_of(got_ref[2 * n :, :384])
+    table_ref[...] = total
+    far = added(keep_ref[:n], got_ref[:n])
+    one_ref[:n] = far[:, :384].astype(BF16)
+    one_ref[n:] = three_parts(total)
+    two_ref[...] = far[:, 384:].astype(BF16)
+    near = added(keep_ref[n:], got_ref[n : 2 * n])
+    own_ref[...] = near[:, :384]
+    three_ref[...] = near[:, 384:]
+
+
+def output_kernel(own_ref, one_ref, two_ref, three_ref, table_in, q_ref, k_ref, v_ref, table_ref):
     core = lax.axis_index("core")
+    n = own_ref.shape[0]
+    table = table_in[...] + table_of(one_ref[n:])
+    table_ref[...] = table[:, : table_ref.shape[1]]
+    own = own_ref[...] + one_ref[:n].astype(F32)
+    got = three_ref[...] + two_ref[...].astype(F32)
 
     @pl.when(core == 0)
     def _():
-        k_ref[...] = own_ref[:, :256]
-        v_ref[...] = got_ref[:, :256]
-        q_ref[:, :128] = own_ref[:, 256:]
-        q_ref[:, 128:] = got_ref[:, 256:]
+        k_ref[...] = own[:, :256]
+        v_ref[...] = got[:, :256]
+        q_ref[:, :128] = own[:, 256:]
+        q_ref[:, 128:] = got[:, 256:]
 
     @pl.when(core == 1)
     def _():
-        v_ref[...] = own_ref[:, :256]
-        k_ref[...] = got_ref[:, :256]
-        q_ref[:, 128:] = own_ref[:, 256:]
-        q_ref[:, :128] = got_ref[:, 256:]
+        v_ref[...] = own[:, :256]
+        k_ref[...] = got[:, :256]
+        q_ref[:, 128:] = own[:, 256:]
+        q_ref[:, :128] = got[:, 256:]
 
 
 def sds(shape, dtype):
@@ -363,12 +383,12 @@
     return pl.CostEstimate(flops=flops, bytes_accessed=byte_count, transcendentals=0)
 
 
-def params():
-    return pltpu.CompilerParams(dimension_semantics=("arbitrary",), vmem_limit_bytes=VMEM_LIMIT)
-
-
-def call(kernel, operands, outs, scratch=(), grid=(1,), flops=1 << 20, blocks=None, any_outs=()):
-    specs = [whole(x.shape) for x in operands]
+def params(limit=None):
+    return pltpu.CompilerParams(dimension_semantics=("arbitrary",), vmem_limit_bytes=limit or VMEM_LIMIT)
+
+
+def call(kernel, operands, outs, scratch=(), grid=(1,), flops=1 << 20, blocks=None, any_outs=(), any_ins=(), limit=None):
+    specs = [pl.BlockSpec(memory_space=pltpu.HBM) if i in any_ins else whole(x.shape) for i, x in enumerate(operands)]
     for at, shape in (blocks or {}).items():
         specs[at] = whole(shape)
     out_specs = [pl.BlockSpec(memory_space=pl.ANY) if i in any_outs else whole(x.shape) for i, x in enumerate(outs)]
@@ -380,7 +400,7 @@
         out_specs=out_specs,
         out_shape=list(outs),
         scratch_shapes=list(scratch),
-        compiler_params=params(),
+        compiler_params=params(limit),
         cost_estimate=cost(flops, moved),
     )(*operands)
 
@@ -395,39 +415,40 @@
     f32, b16 = (lambda *s: sds(s, F32)), (lambda *s: sds(s, BF16))
     v32, v16 = (lambda *s: pltpu.VMEM(s, F32)), (lambda *s: pltpu.VMEM(s, BF16))
     tile_flops = 6 * 2 * TILE * BAND * HDIM
-    (tail,) = call(
-        tail_kernel, (inputs[1024 - REACH :], w_key, w_value), (b16(REACH, 512),), flops=2 * 256 * 2048 * 512
+    tail, x, wq, wk, wv = call(
+        load_kernel, (inputs, w_query, w_key, w_value),
+        (b16(REACH, 512), b16(1024, 2048), b16(2048, 256), b16(2048, 256), b16(2048, 256)),
+        (pltpu.SemaphoreType.DMA((5,)),), flops=2 * 256 * 2048 * 512, any_ins=(0, 1, 2, 3), limit=LOAD_LIMIT,
     )
     halo = neighbour(tail, 1)
-    far = jnp.pad(rel_table, ((0, 0), (0, 512 - rel_table.shape[1])), mode="edge")
     query, key, value = call(
-        proj_kernel, (inputs, w_query, w_key, w_value), (b16(1024, 256),) * 3,
+        proj_kernel, (x, wq, wk, wv), (b16(1024, 256),) * 3,
         flops=2 * 1024 * 2048 * 768,
     )
     block = (REACH, 256)
     dq0, edge, back, bias, pat = call(
-        first_kernel, (query, key, value, halo, out_grad, far),
+        first_kernel, (query, key, value, halo, out_grad, rel_table),
         (b16(REACH, 256), f32(REACH, 512), b16(REACH, 512), f32(2, BAND, TILE), f32(2, BAND, TILE)),
         (v16(512, 256), v16(512, 256), v16(256, 512), v16(256, 512), v32(512, 256), v32(512, 256)),
         flops=4 * tile_flops, blocks={0: block, 1: block, 2: block, 4: block},
     )
     back = neighbour(back, -1)
-    dq, kg, vg, edge, pat = call(
+    dq, near, kg, vg, edge, pat = call(
         attn_kernel, (query, key, value, out_grad, bias, pat, edge, dq0),
-        (b16(1024, 256), b16(768, 256), b16(768, 256), f32(REACH, 512), f32(2, BAND, TILE)),
+        (b16(1024, 256), b16(1024, 256), b16(768, 256), b16(768, 256), f32(REACH, 512), f32(2, BAND, TILE)),
         (v16(256, 1024), v16(256, 1024), v32(1024, 256), v32(1024, 256)),
-        grid=(3,), flops=12 * tile_flops,
-    )
-    kg, vg, own, swap = call(finish_kernel, (kg, vg, edge, back, dq), (b16(1024, 256),) * 2 + (b16(1024, 384),) * 2)
+        flops=12 * tile_flops,
+    )
+    kg, vg, own, swap = call(finish_kernel, (kg, vg, edge, back, near), (b16(1024, 256),) * 2 + (b16(1024, 384),) * 2)
     got = core_swap(swap)
     sem = pltpu.SemaphoreType.DMA((3,))
     product = 2 * 1024 * 2048 * 384
     send, keep, table = call(
-        own_kernel, (inputs, own, pat), (b16(1024 + EXTRA, 384), b16(1024, 384), f32(2, 384)),
+        own_kernel, (x, own, pat), (b16(1024 + EXTRA, 384), b16(1024, 384), f32(2, 384)),
         (v16(2048, 384), v16(EXTRA, 384), v32(8, 640), sem), flops=product, any_outs=(0, 1),
     )
     send2, keep2 = call(
-        other_kernel, (inputs, got), (b16(1024, 384),) * 2, (v16(2048, 384), sem),
+        other_kernel, (x, got), (b16(1024, 384),) * 2, (v16(2048, 384), sem),
         flops=product, any_outs=(0, 1),
     )
     got = exchange(send, OWN, 0)
@@ -439,17 +460,20 @@
     send, keep, table = call(
         merge_kernel, (keep, got, keep2, got2, table), (b16(256 + EXTRA, 768), b16(256, 768), f32(2, 384))
     )
-    for level, rows in ((2, 128), (3, 64)):
-        got = exchange(send, OWN, level)
-        send, keep, table = call(
-            level_kernel, (keep, got, table),
-            (b16(rows + EXTRA, 768), b16(rows, 768), f32(2, 384)),
-        )
-    got = exchange(send, OWN, 4)
-    own, swap, table = call(last_kernel, (keep, got, table), (f32(64, 384), f32(64, 384), f32(2, 384)))
-    got = core_swap(swap)
-    dwq, dwk, dwv = call(output_kernel, (own, got), (f32(64, 256),) * 3)
-    return dq, kg, vg, dwq, dwk, dwv, table[:, : rel_table.shape[1]]
+    got = exchange(send, OWN, 2)
+    send, keep, table = call(level_kernel, (keep, got, table), (b16(128 + EXTRA, 768), b16(128, 768), f32(2, 384)))
+    got = exchange(send, OWN, 3)
+    one, two, three, own, table = call(
+        split_kernel, (keep, got, table),
+        (b16(64 + EXTRA, 384), b16(64, 384), f32(64, 384), f32(64, 384), f32(2, 384)),
+    )
+    one = exchange(one, OWN, 4)
+    two = exchange(two, OWN, 4, across=1)
+    three = core_swap(three)
+    dwq, dwk, dwv, table = call(
+        output_kernel, (own, one, two, three, table), (f32(64, 256),) * 3 + (f32(*rel_table.shape),)
+    )
+    return dq, kg, vg, dwq, dwk, dwv, table
 
 
 def solution(mesh):

time: 94.1 us -> 94.3 us (level)
  the two profiles are of different devices: /device:TPU:27 before, /device:TPU:8 now
where the time goes in v1:
time: 94.3 us; the launch traced here: 92.9 us
  starting transfers between devices  33.9 us (36%)
  waiting for transfers between devices  29.9 us (32%)
  Pallas kernels  22.2 us (24%)
  local copies, waits for them, and re-layouts  5.87 us (6%)
    ppermute x8, starting transfers between devices, exchange(): lax.ppermute(block, SP + ('core',), level_route(sequences, level, across))  29.1 us
    ppermute x8, waiting for transfers between devices, exchange(): lax.ppermute(block, SP + ('core',), level_route(sequences, level, across))  26.6 us
    pallas_call x12, Pallas kernels, call(): pl.pallas_call(kernel, grid=grid, in_specs=specs, out_specs=out_specs, ou...  22.2 us
    unnamed x12, local copies, waits for them, and re-layouts  5.87 us
    ppermute x2, starting transfers between devices, neighbour(): return lax.ppermute(block, SP, route)  4.7 us
    ppermute x2, waiting for transfers between devices, neighbour(): return lax.ppermute(block, SP, route)  3.26 us
  transfers between devices with their start and end apart: 12, of which 9 were waited for; matrix products, arithmetic and copies ran while one was open for 0% of the time, Pallas kernels for 18%

profile of v1, /device:TPU:8, one launch (start us, length us, event | category | flops | bytes accessed | tf_op | source)
XLA Modules:
  0.0 92.9 jit_solution(6834879335049807363)
XLA Ops:
  0.6 0.0 copy-start
  0.6 2.2 %copy-done = bf16[1024,2048]{1,0:T(8,128)(2,1)S(1)} copy-done((bf16[1024,2048]{1,0:T(8,128)(2,1)S(1)}, bf16[1024,2048]{1,0:T(8,128)(2,1)}, u32[]{:S(2)}) %copy-start) | copy-done | bytes 4194328
  2.8 0.0 copy-start.2
  2.8 1.2 %copy-done.2 = bf16[2048,256]{1,0:T(8,128)(2,1)S(1)} copy-done((bf16[2048,256]{1,0:T(8,128)(2,1)S(1)}, bf16[2048,256]{1,0:T(8,128)(2,1)}, u32[]{:S(2)}) %copy-start.2) | copy-done | bytes 1048600
  4.0 0.0 copy-start.3
  4.0 1.2 %copy-done.3 = bf16[2048,256]{1,0:T(8,128)(2,1)S(1)} copy-done((bf16[2048,256]{1,0:T(8,128)(2,1)S(1)}, bf16[2048,256]{1,0:T(8,128)(2,1)}, u32[]{:S(2)}) %copy-start.3) | copy-done | bytes 1048600
  5.3 0.0 copy-start.4
  5.3 1.2 %copy-done.4 = bf16[2048,256]{1,0:T(8,128)(2,1)S(1)} copy-done((bf16[2048,256]{1,0:T(8,128)(2,1)S(1)}, bf16[2048,256]{1,0:T(8,128)(2,1)}, u32[]{:S(2)}) %copy-start.4) | copy-done | bytes 1048600
  6.5 1.3 %shard_map.117 = (bf16[256,512]{1,0:T(8,128)(2,1)S(1)}, bf16[1024,2048]{1,0:T(8,128)(2,1)S(1)}, bf16[2048,256]{1,0:T(8,128)(2,1)S(1)}, bf16[2048,256]{1,0:T(8,128)(2,1)S(1)}, bf16[2048,256]{1,0:T(8,128)(2,1)S(1)}) custom-call(bf16[1024,2048]{1,0:T(8,128)(2,1)S(1)} %copy-done, bf16[2048,256]{1,0:T(8,128)(2,1)S(1)} %copy-done.2, ...), custom_call_target="tpu_custom_call" | custom-call | flops 536870912 | bytes 14942208 | tf_op jit(solution)/shard_map/pallas_call | solution.py:396
  7.8 3.4 %collective-permute-start = (bf16[256,512]{1,0:T(8,128)(2,1)S(1)}, bf16[256,512]{1,0:T(8,128)(2,1)S(1)}, u32[]{:S(2)}, u32[]{:S(2)}) collective-permute-start(bf16[256,512]{1,0:T(8,128)(2,1)S(1)} %get-tuple-element.60), channel_id=1, source_target_pairs={{0,8},{8,16},{16,24},{24,32},{32,40},{40,48},{48,56},{56,64},{64,7... | collective-permute-start | bytes 786440 | tf_op jit(solution)/shard_map/ppermute | solution.py:411
  11.2 0.0 copy-start.1
  11.2 0.0 copy-start.5
  11.2 3.4 %shard_map.118 = (bf16[1024,256]{1,0:T(8,128)(2,1)S(1)}, bf16[1024,256]{1,0:T(8,128)(2,1)S(1)}, bf16[1024,256]{1,0:T(8,128)(2,1)S(1)}) custom-call(bf16[1024,2048]{1,0:T(8,128)(2,1)S(1)} %get-tuple-element.53.x_ref, bf16[2048,256]{1,0:T(8,128)(2,1)S(1)} %get-tuple-element.54.wq_ref, bf16[2048,256]{1,0:T(8,128)(2,1)S(1)} %get-tuple-element.55.wk_ref, ...), custom_call_target="tpu_custom_call" | custom-call | flops 3221225472 | bytes 8912896 | tf_op jit(solution)/shard_map/pallas_call | solution.py:396
  14.7 2.1 %collective-permute-done.halo_ref = bf16[256,512]{1,0:T(8,128)(2,1)S(1)} collective-permute-done((bf16[256,512]{1,0:T(8,128)(2,1)S(1)}, bf16[256,512]{1,0:T(8,128)(2,1)S(1)}, u32[]{:S(2)}, u32[]{:S(2)}) %collective-permute-start) | collective-permute-done | bytes 262176 | tf_op jit(solution)/shard_map/ppermute | solution.py:411
  16.7 0.0 copy-done.1
  16.7 0.0 copy-done.5
  16.7 2.3 %shard_map.119 = (bf16[256,256]{1,0:T(8,128)(2,1)S(1)}, f32[256,512]{1,0:T(8,128)S(1)}, bf16[256,512]{1,0:T(8,128)(2,1)S(1)}, f32[2,384,128]{2,1,0:T(8,128)S(1)}, f32[2,384,128]{2,1,0:T(8,128)S(1)}) custom-call(bf16[1024,256]{1,0:T(8,128)(2,1)S(1)} %get-tuple-element.57.q_ref, bf16[1024,256]{1,0:T(8,128)(2,1)S(1)} %get-tuple-element.58.k_ref, ...), custom_call_target="tpu_custom_call" | custom-call | flops 301989888 | bytes 4065288 | tf_op jit(solution)/shard_map/pallas_call | solution.py:396
  19.1 1.3 %collective-permute-start.1 = (bf16[256,512]{1,0:T(8,128)(2,1)S(1)}, bf16[256,512]{1,0:T(8,128)(2,1)S(1)}, u32[]{:S(2)}, u32[]{:S(2)}) collective-permute-start(bf16[256,512]{1,0:T(8,128)(2,1)S(1)} %get-tuple-element.69), channel_id=1, source_target_pairs={{8,0},{16,8},{24,16},{32,24},{40,32},{48,40},{56,48},{64,56},{72,6... | collective-permute-start | bytes 786440 | tf_op jit(solution)/shard_map/ppermute | solution.py:411
  20.4 7.3 %shard_map.120 = (bf16[1024,256]{1,0:T(8,128)(2,1)}, bf16[1024,256]{1,0:T(8,128)(2,1)S(1)}, bf16[768,256]{1,0:T(8,128)(2,1)S(1)}, bf16[768,256]{1,0:T(8,128)(2,1...) custom-call(bf16[1024,256]{1,0:T(8,128)(2,1)S(1)} %get-tuple-element.57.q_ref, ...), custom_call_target="tpu_custom_call" | custom-call | flops 905969664 | bytes 6291456 | tf_op jit(solution)/shard_map/pallas_call | solution.py:396
  27.7 1.2 %collective-permute-done.1.back_ref = bf16[256,512]{1,0:T(8,128)(2,1)S(1)} collective-permute-done((bf16[256,512]{1,0:T(8,128)(2,1)S(1)}, bf16[256,512]{1,0:T(8,128)(2,1)S(1)}, u32[]{:S(2)}, u32[]{:S(2)}) %collective-permute-start.1) | collective-permute-done | bytes 262176 | tf_op jit(solution)/shard_map/ppermute | solution.py:411
  28.9 1.2 %shard_map.121 = (bf16[1024,256]{1,0:T(8,128)(2,1)}, bf16[1024,256]{1,0:T(8,128)(2,1)}, bf16[1024,384]{1,0:T(8,128)(2,1)S(1)}, bf16[1024,384]{1,0:T(8,128)(2,1)S(1)}) custom-call(bf16[768,256]{1,0:T(8,128)(2,1)S(1)} %get-tuple-element.66.kg_in, bf16[768,256]{1,0:T(8,128)(2,1)S(1)} %get-tuple-element.67.vg_in, f32[256,512]{1,0:T(8,128)S(1)} %get-tuple-element.68.edge_ref, ...), custom_call_target="tpu_custom_call" | custom-call | flops 1048576 | bytes 4718592 | tf_op jit(solution)/shard_map/pallas_call | solution.py:396
  30.1 0.0 collective-permute-start.4
  30.1 2.7 %shard_map.122 = (bf16[1040,384]{1,0:T(8,128)(2,1)S(1)}, bf16[1024,384]{1,0:T(8,128)(2,1)S(1)}, f32[2,384]{1,0:T(2,128)S(1)}) custom-call(bf16[1024,2048]{1,0:T(8,128)(2,1)S(1)} %get-tuple-element.53.x_ref, bf16[1024,384]{1,0:T(8,128)(2,1)S(1)} %get-tuple-element.73.grad_ref, f32[2,384,128]{2,1,0:T(8,128)S(1)} %get-tuple-element.74.pat_ref), custom_call_target="tpu_custom_call" | custom-call | flops 1610612736 | bytes 6962176 | tf_op jit(solution)/shard_map/pallas_call | solution.py:396
  32.8 2.0 %collective-permute-start.2 = (bf16[1040,384]{1,0:T(8,128)(2,1)S(1)}, bf16[1040,384]{1,0:T(8,128)(2,1)S(1)}, u32[]{:S(2)}, u32[]{:S(2)}) collective-permute-start(bf16[1040,384]{1,0:T(8,128)(2,1)S(1)} %get-tuple-element.76), channel_id=1, source_target_pairs={{0,8},{8,0},{16,24},{24,16},{32,40},{40,32},{48,56},{56,48},{64,72... | collective-permute-start | bytes 2396168 | tf_op jit(solution)/shard_map/ppermute | solution.py:95
  34.8 0.0 collective-permute-done.4.grad_ref
  34.8 2.6 %shard_map.124 = (bf16[1024,384]{1,0:T(8,128)(2,1)S(1)}, bf16[1024,384]{1,0:T(8,128)(2,1)S(1)}) custom-call(bf16[1024,2048]{1,0:T(8,128)(2,1)S(1)} %get-tuple-element.53.x_ref, bf16[1024,384]{1,0:T(8,128)(2,1)S(1)} %collective-permute-done.4.grad_ref), custom_call_target="tpu_custom_call" | custom-call | flops 1610612736 | bytes 6553600 | tf_op jit(solution)/shard_map/pallas_call | solution.py:396
  37.4 3.4 %collective-permute-start.5 = (bf16[1024,384]{1,0:T(8,128)(2,1)S(1)}, bf16[1024,384]{1,0:T(8,128)(2,1)S(1)}, u32[]{:S(2)}, u32[]{:S(2)}) collective-permute-start(bf16[1024,384]{1,0:T(8,128)(2,1)S(1)} %get-tuple-element.82), channel_id=1, source_target_pairs={{0,24},{8,16},{16,8},{24,0},{32,56},{40,48},{48,40},{56,32},{64,88... | collective-permute-start | bytes 2359304 | tf_op jit(solution)/shard_map/ppermute | solution.py:95
  40.8 4.2 %collective-permute-done.2.got_ref = bf16[1040,384]{1,0:T(8,128)(2,1)S(1)} collective-permute-done((bf16[1040,384]{1,0:T(8,128)(2,1)S(1)}, bf16[1040,384]{1,0:T(8,128)(2,1)S(1)}, u32[]{:S(2)}, u32[]{:S(2)}) %collective-permute-start.2) | collective-permute-done | bytes 798752 | tf_op jit(solution)/shard_map/ppermute | solution.py:95
  45.0 0.2 shard_map.123
  45.3 5.3 %collective-permute-start.3 = (bf16[528,384]{1,0:T(8,128)(2,1)S(1)}, bf16[528,384]{1,0:T(8,128)(2,1)S(1)}, u32[]{:S(2)}, u32[]{:S(2)}) collective-permute-start(bf16[528,384]{1,0:T(8,128)(2,1)S(1)} %get-tuple-element.79), channel_id=1, source_target_pairs={{0,24},{8,16},{16,8},{24,0},{32,56},{40,48},{48,40},{56,32},{64,88... | collective-permute-start | bytes 1216520 | tf_op jit(solution)/shard_map/ppermute | solution.py:95
  50.6 0.2 collective-permute-done.5
  50.8 0.2 add_convert_fusion
  51.0 1.5 %collective-permute-start.6 = (bf16[512,384]{1,0:T(8,128)(2,1)S(1)}, bf16[512,384]{1,0:T(8,128)(2,1)S(1)}, u32[]{:S(2)}, u32[]{:S(2)}) collective-permute-start(bf16[512,384]{1,0:T(8,128)(2,1)S(1)} %get-tuple-element.99), channel_id=1, source_target_pairs={{0,8},{8,0},{16,24},{24,16},{32,40},{40,32},{48,56},{56,48},{64,72... | collective-permute-start | bytes 1179656 | tf_op jit(solution)/shard_map/ppermute | solution.py:95
  52.5 4.0 %collective-permute-done.3.got_ref = bf16[528,384]{1,0:T(8,128)(2,1)S(1)} collective-permute-done((bf16[528,384]{1,0:T(8,128)(2,1)S(1)}, bf16[528,384]{1,0:T(8,128)(2,1)S(1)}, u32[]{:S(2)}, u32[]{:S(2)}) %collective-permute-start.3) | collective-permute-done | bytes 405536 | tf_op jit(solution)/shard_map/ppermute | solution.py:95
  56.5 2.4 %collective-permute-done.6.got2_ref = bf16[512,384]{1,0:T(8,128)(2,1)S(1)} collective-permute-done((bf16[512,384]{1,0:T(8,128)(2,1)S(1)}, bf16[512,384]{1,0:T(8,128)(2,1)S(1)}, u32[]{:S(2)}, u32[]{:S(2)}) %collective-permute-start.6) | collective-permute-done | bytes 393248 | tf_op jit(solution)/shard_map/ppermute | solution.py:95
  58.9 0.2 shard_map.125
  59.1 4.5 %collective-permute-start.7 = (bf16[272,768]{1,0:T(8,128)(2,1)S(1)}, bf16[272,768]{1,0:T(8,128)(2,1)S(1)}, u32[]{:S(2)}, u32[]{:S(2)}) collective-permute-start(bf16[272,768]{1,0:T(8,128)(2,1)S(1)} %get-tuple-element.85), channel_id=1, source_target_pairs={{0,32},{8,40},{16,48},{24,56},{32,0},{40,8},{48,16},{56,24},{64,96... | collective-permute-start | bytes 1253384 | tf_op jit(solution)/shard_map/ppermute | solution.py:95
  63.7 6.0 %collective-permute-done.7.got_ref = bf16[272,768]{1,0:T(8,128)(2,1)S(1)} collective-permute-done((bf16[272,768]{1,0:T(8,128)(2,1)S(1)}, bf16[272,768]{1,0:T(8,128)(2,1)S(1)}, u32[]{:S(2)}, u32[]{:S(2)}) %collective-permute-start.7) | collective-permute-done | bytes 417824 | tf_op jit(solution)/shard_map/ppermute | solution.py:95
  69.7 0.1 shard_map.126
  69.8 6.0 %collective-permute-start.8 = (bf16[144,768]{1,0:T(8,128)(2,1)S(1)}, bf16[144,768]{1,0:T(8,128)(2,1)S(1)}, u32[]{:S(2)}, u32[]{:S(2)}) collective-permute-start(bf16[144,768]{1,0:T(8,128)(2,1)S(1)} %get-tuple-element.88), channel_id=1, source_target_pairs={{0,224},{8,232},{16,240},{24,248},{32,64},{40,72},{48,80},{56,88},... | collective-permute-start | bytes 663560 | tf_op jit(solution)/shard_map/ppermute | solution.py:95
  75.9 3.9 %collective-permute-done.8.got_ref = bf16[144,768]{1,0:T(8,128)(2,1)S(1)} collective-permute-done((bf16[144,768]{1,0:T(8,128)(2,1)S(1)}, bf16[144,768]{1,0:T(8,128)(2,1)S(1)}, u32[]{:S(2)}, u32[]{:S(2)}) %collective-permute-start.8) | collective-permute-done | bytes 221216 | tf_op jit(solution)/shard_map/ppermute | solution.py:95
  79.8 0.1 shard_map.127
  79.8 0.1 collective-permute-start.11
  79.9 3.2 %collective-permute-start.9 = (bf16[80,384]{1,0:T(8,128)(2,1)S(1)}, bf16[80,384]{1,0:T(8,128)(2,1)S(1)}, u32[]{:S(2)}, u32[]{:S(2)}) collective-permute-start(bf16[80,384]{1,0:T(8,128)(2,1)S(1)} %get-tuple-element.91), channel_id=1, source_target_pairs={{0,96},{8,104},{16,112},{24,120},{32,192},{40,200},{48,208},{56,21... | collective-permute-start | bytes 184328 | tf_op jit(solution)/shard_map/ppermute | solution.py:95
  83.1 3.1 %collective-permute-start.10 = (bf16[64,384]{1,0:T(8,128)(2,1)S(1)}, bf16[64,384]{1,0:T(8,128)(2,1)S(1)}, u32[]{:S(2)}, u32[]{:S(2)}) collective-permute-start(bf16[64,384]{1,0:T(8,128)(2,1)S(1)} %get-tuple-element.92), channel_id=1, source_target_pairs={{0,97},{8,105},{16,113},{24,121},{32,193},{40,201},{48,209},{56,21... | collective-permute-start | bytes 147464 | tf_op jit(solution)/shard_map/ppermute | solution.py:95
  86.2 5.9 %collective-permute-done.10.two_ref = bf16[64,384]{1,0:T(8,128)(2,1)S(1)} collective-permute-done((bf16[64,384]{1,0:T(8,128)(2,1)S(1)}, bf16[64,384]{1,0:T(8,128)(2,1)S(1)}, u32[]{:S(2)}, u32[]{:S(2)}) %collective-permute-start.10) | collective-permute-done | bytes 49184 | tf_op jit(solution)/shard_map/ppermute | solution.py:95
  92.1 0.0 collective-permute-done.9.one_ref
  92.1 0.0 collective-permute-done.11.three_ref
  92.1 0.7 shard_map.128
Async XLA Ops:
  0.6 2.2 %copy-start = (bf16[1024,2048]{1,0:T(8,128)(2,1)S(1)}, bf16[1024,2048]{1,0:T(8,128)(2,1)}, u32[]{:S(2)}) copy-start(bf16[1024,2048]{1,0:T(8,128)(2,1)} %x_hbm.1) | copy-start | bytes 12582916
  2.8 1.2 %copy-start.2 = (bf16[2048,256]{1,0:T(8,128)(2,1)S(1)}, bf16[2048,256]{1,0:T(8,128)(2,1)}, u32[]{:S(2)}) copy-start(bf16[2048,256]{1,0:T(8,128)(2,1)} %wq_hbm.1) | copy-start | bytes 3145732
  4.0 1.2 %copy-start.3 = (bf16[2048,256]{1,0:T(8,128)(2,1)S(1)}, bf16[2048,256]{1,0:T(8,128)(2,1)}, u32[]{:S(2)}) copy-start(bf16[2048,256]{1,0:T(8,128)(2,1)} %wk_hbm.1) | copy-start | bytes 3145732
  5.3 1.2 %copy-start.4 = (bf16[2048,256]{1,0:T(8,128)(2,1)S(1)}, bf16[2048,256]{1,0:T(8,128)(2,1)}, u32[]{:S(2)}) copy-start(bf16[2048,256]{1,0:T(8,128)(2,1)} %wv_hbm.1) | copy-start | bytes 3145732
  7.8 8.9 %collective-permute-start = (bf16[256,512]{1,0:T(8,128)(2,1)S(1)}, bf16[256,512]{1,0:T(8,128)(2,1)S(1)}, u32[]{:S(2)}, u32[]{:S(2)}) collective-permute-start(bf16[256,512]{1,0:T(8,128)(2,1)S(1)} %get-tuple-element.60), channel_id=1, source_target_pairs={{0,8},{8,16},{16,24},{24,32},{32,40},{40,48},{48,56},{56,64},{64,7... | collective-permute-start | bytes 786440 | tf_op jit(solution)/shard_map/ppermute | solution.py:411
  11.2 5.5 %copy-start.1 = (bf16[1024,256]{1,0:T(8,128)(2,1)S(1)}, bf16[1024,256]{1,0:T(8,128)(2,1)}, u32[]{:S(2)}) copy-start(bf16[1024,256]{1,0:T(8,128)(2,1)} %og_ref.3) | copy-start | bytes 1572868
  11.2 5.5 %copy-start.5 = (f32[2,257]{1,0:T(2,128)S(1)}, f32[2,257]{1,0:T(2,128)}, u32[]{:S(2)}) copy-start(f32[2,257]{1,0:T(2,128)} %rel_ref.1) | copy-start | bytes 6172
  19.1 9.8 %collective-permute-start.1 = (bf16[256,512]{1,0:T(8,128)(2,1)S(1)}, bf16[256,512]{1,0:T(8,128)(2,1)S(1)}, u32[]{:S(2)}, u32[]{:S(2)}) collective-permute-start(bf16[256,512]{1,0:T(8,128)(2,1)S(1)} %get-tuple-element.69), channel_id=1, source_target_pairs={{8,0},{16,8},{24,16},{32,24},{40,32},{48,40},{56,48},{64,56},{72,6... | collective-permute-start | bytes 786440 | tf_op jit(solution)/shard_map/ppermute | solution.py:411
  30.1 4.7 %collective-permute-start.4 = (bf16[1024,384]{1,0:T(8,128)(2,1)S(1)}, bf16[1024,384]{1,0:T(8,128)(2,1)S(1)}, u32[]{:S(2)}, u32[]{:S(2)}) collective-permute-start(bf16[1024,384]{1,0:T(8,128)(2,1)S(1)} %get-tuple-element.80), channel_id=1, source_target_pairs={{0,1},{1,0},{2,3},{3,2},{4,5},{5,4},{6,7},{7,6},{8,9},{9,8},{10,11... | collective-permute-start | bytes 2359304 | tf_op jit(solution)/shard_map/ppermute | solution.py:99
  32.8 12.2 %collective-permute-start.2 = (bf16[1040,384]{1,0:T(8,128)(2,1)S(1)}, bf16[1040,384]{1,0:T(8,128)(2,1)S(1)}, u32[]{:S(2)}, u32[]{:S(2)}) collective-permute-start(bf16[1040,384]{1,0:T(8,128)(2,1)S(1)} %get-tuple-element.76), channel_id=1, source_target_pairs={{0,8},{8,0},{16,24},{24,16},{32,40},{40,32},{48,56},{56,48},{64,72... | collective-permute-start | bytes 2396168 | tf_op jit(solution)/shard_map/ppermute | solution.py:95
  37.4 13.4 %collective-permute-start.5 = (bf16[1024,384]{1,0:T(8,128)(2,1)S(1)}, bf16[1024,384]{1,0:T(8,128)(2,1)S(1)}, u32[]{:S(2)}, u32[]{:S(2)}) collective-permute-start(bf16[1024,384]{1,0:T(8,128)(2,1)S(1)} %get-tuple-element.82), channel_id=1, source_target_pairs={{0,24},{8,16},{16,8},{24,0},{32,56},{40,48},{48,40},{56,32},{64,88... | collective-permute-start | bytes 2359304 | tf_op jit(solution)/shard_map/ppermute | solution.py:95
  45.3 11.2 %collective-permute-start.3 = (bf16[528,384]{1,0:T(8,128)(2,1)S(1)}, bf16[528,384]{1,0:T(8,128)(2,1)S(1)}, u32[]{:S(2)}, u32[]{:S(2)}) collective-permute-start(bf16[528,384]{1,0:T(8,128)(2,1)S(1)} %get-tuple-element.79), channel_id=1, source_target_pairs={{0,24},{8,16},{16,8},{24,0},{32,56},{40,48},{48,40},{56,32},{64,88... | collective-permute-start | bytes 1216520 | tf_op jit(solution)/shard_map/ppermute | solution.py:95
  51.0 7.9 %collective-permute-start.6 = (bf16[512,384]{1,0:T(8,128)(2,1)S(1)}, bf16[512,384]{1,0:T(8,128)(2,1)S(1)}, u32[]{:S(2)}, u32[]{:S(2)}) collective-permute-start(bf16[512,384]{1,0:T(8,128)(2,1)S(1)} %get-tuple-element.99), channel_id=1, source_target_pairs={{0,8},{8,0},{16,24},{24,16},{32,40},{40,32},{48,56},{56,48},{64,72... | collective-permute-start | bytes 1179656 | tf_op jit(solution)/shard_map/ppermute | solution.py:95
  59.1 10.6 %collective-permute-start.7 = (bf16[272,768]{1,0:T(8,128)(2,1)S(1)}, bf16[272,768]{1,0:T(8,128)(2,1)S(1)}, u32[]{:S(2)}, u32[]{:S(2)}) collective-permute-start(bf16[272,768]{1,0:T(8,128)(2,1)S(1)} %get-tuple-element.85), channel_id=1, source_target_pairs={{0,32},{8,40},{16,48},{24,56},{32,0},{40,8},{48,16},{56,24},{64,96... | collective-permute-start | bytes 1253384 | tf_op jit(solution)/shard_map/ppermute | solution.py:95
  69.8 10.0 %collective-permute-start.8 = (bf16[144,768]{1,0:T(8,128)(2,1)S(1)}, bf16[144,768]{1,0:T(8,128)(2,1)S(1)}, u32[]{:S(2)}, u32[]{:S(2)}) collective-permute-start(bf16[144,768]{1,0:T(8,128)(2,1)S(1)} %get-tuple-element.88), channel_id=1, source_target_pairs={{0,224},{8,232},{16,240},{24,248},{32,64},{40,72},{48,80},{56,88},... | collective-permute-start | bytes 663560 | tf_op jit(solution)/shard_map/ppermute | solution.py:95
  79.8 12.3 %collective-permute-start.11 = (f32[64,384]{1,0:T(8,128)S(1)}, f32[64,384]{1,0:T(8,128)S(1)}, u32[]{:S(2)}, u32[]{:S(2)}) collective-permute-start(f32[64,384]{1,0:T(8,128)S(1)} %get-tuple-element.93), channel_id=1, source_target_pairs={{0,1},{1,0},{2,3},{3,2},{4,5},{5,4},{6,7},{7,6},{8,9},{9,8},{10,11... | collective-permute-start | bytes 294920 | tf_op jit(solution)/shard_map/ppermute | solution.py:99
  79.9 12.2 %collective-permute-start.9 = (bf16[80,384]{1,0:T(8,128)(2,1)S(1)}, bf16[80,384]{1,0:T(8,128)(2,1)S(1)}, u32[]{:S(2)}, u32[]{:S(2)}) collective-permute-start(bf16[80,384]{1,0:T(8,128)(2,1)S(1)} %get-tuple-element.91), channel_id=1, source_target_pairs={{0,96},{8,104},{16,112},{24,120},{32,192},{40,200},{48,208},{56,21... | collective-permute-start | bytes 184328 | tf_op jit(solution)/shard_map/ppermute | solution.py:95
  83.1 9.0 %collective-permute-start.10 = (bf16[64,384]{1,0:T(8,128)(2,1)S(1)}, bf16[64,384]{1,0:T(8,128)(2,1)S(1)}, u32[]{:S(2)}, u32[]{:S(2)}) collective-permute-start(bf16[64,384]{1,0:T(8,128)(2,1)S(1)} %get-tuple-element.92), channel_id=1, source_target_pairs={{0,97},{8,105},{16,113},{24,121},{32,193},{40,201},{48,209},{56,21... | collective-permute-start | bytes 147464 | tf_op jit(solution)/shard_map/ppermute | solution.py:95

commit v2 on v1

--- a/solution.py
+++ b/solution.py
@@ -80,19 +80,27 @@
     return [jnp.where(core == 0, a, b) for a, b in zip(*places)]
 
 
-def level_route(sequences, level, across=0):
+def level_route(sequences, steps, across=0):
     route = []
     for core, levels in enumerate(sequences):
-        axis, f = levels[level]
         for z in range(NZ):
             for x in range(NX):
-                to = f(z) * NX + x if axis == "sp_0" else z * NX + f(x)
+                at = {"sp_0": z, "sp_1": x}
+                for step in steps:
+                    axis, f = levels[step]
+                    at[axis] = f(at[axis])
+                to = at["sp_0"] * NX + at["sp_1"]
                 route.append(((z * NX + x) * 2 + core, to * 2 + (core ^ across)))
     return route
 
 
-def exchange(block, sequences, level, across=0):
-    return lax.ppermute(block, SP + ("core",), level_route(sequences, level, across))
+def exchange(block, sequences, steps, across=0):
+    return lax.ppermute(block, SP + ("core",), level_route(sequences, steps, across))
+
+
+def exchange_quarters(blocks, sequences, level):
+    paths = ((level, level + 1), (level,), (level + 1,))
+    return [exchange(x, sequences, path) for x, path in zip(blocks, paths)]
 
 
 def core_swap(block):
@@ -281,8 +289,15 @@
         copy.wait()
 
 
-def own_kernel(x_ref, grad_ref, pat_ref, send_hbm, keep_hbm, table_ref, out_s, parts_s, diag_s, sem):
+def own_kernel(x_ref, grad_ref, m0_hbm, m1_hbm, m2_hbm, keep_hbm, out_s, sem):
     placed_product(x_ref, grad_ref, OWN, out_s)
+    copy_out([(out_s.at[512 * i : 512 * (i + 1)], m) for i, m in enumerate((m0_hbm, m1_hbm, m2_hbm, keep_hbm))], sem)
+
+
+def other_kernel(
+    x_ref, grad_ref, pat_ref, m0_hbm, m1_hbm, m2_hbm, keep_hbm, table_ref, out_s, parts_s, diag_s, sem
+):
+    placed_product(x_ref, grad_ref, OTHER, out_s)
     for h in range(2):
         diag_s[...] = jnp.zeros_like(diag_s)
         for a in range(BAND // 8):
@@ -295,55 +310,50 @@
         table_ref[h : h + 1, :256] = total[:, :256]
         table_ref[h : h + 1, 256:] = jnp.broadcast_to(far, (1, 128))
     parts_s[...] = three_parts(table_ref[...])
-    copy_out(
-        [(out_s.at[:1024], send_hbm.at[:1024]), (parts_s, send_hbm.at[1024:]), (out_s.at[1024:], keep_hbm)],
-        sem,
-    )
-
-
-def other_kernel(x_ref, grad_ref, send_hbm, keep_hbm, out_s, sem):
-    placed_product(x_ref, grad_ref, OTHER, out_s)
-    copy_out([(out_s.at[:1024], send_hbm), (out_s.at[1024:], keep_hbm)], sem)
-
-
-def added(keep, got):
-    return keep.astype(F32) + got.astype(F32)
-
-
-def level_kernel(keep_ref, got_ref, table_in, send_ref, next_ref, table_ref):
-    half = next_ref.shape[0]
-    n = 2 * half
-    total = table_in[...] + table_of(got_ref[n:, :384])
+    pairs = [(out_s.at[1536:], keep_hbm)]
+    for i, m in enumerate((m0_hbm, m1_hbm, m2_hbm)):
+        pairs += [(out_s.at[512 * i : 512 * (i + 1)], m.at[:512]), (parts_s, m.at[512:])]
+    copy_out(pairs, sem)
+
+
+def summed(keep_ref, got_refs, rows):
+    total = keep_ref[rows].astype(F32)
+    for got in got_refs:
+        total += got[rows].astype(F32)
+    return total
+
+
+def summed_table(table_in, got_refs, n):
+    total = table_in[...]
+    for got in got_refs:
+        total += table_of(got[n:, :384])
+    return total
+
+
+def merge_kernel(
+    keep_ref, a0, a1, a2, keep2_ref, b0, b1, b2, table_in, m0_ref, m1_ref, m2_ref, next_ref, table_ref
+):
+    total = summed_table(table_in, (b0, b1, b2), 512)
     table_ref[...] = total
-    send_ref[:half] = added(keep_ref[:half], got_ref[:half]).astype(BF16)
-    next_ref[...] = added(keep_ref[half:], got_ref[half:n]).astype(BF16)
-    send_ref[half:, :384] = three_parts(total)
-    if send_ref.shape[1] > 384:
-        send_ref[half:, 384:] = jnp.zeros((EXTRA, send_ref.shape[1] - 384), BF16)
-
-
-def merge_kernel(keep_ref, got_ref, keep2_ref, got2_ref, table_in, send_ref, next_ref, table_ref):
-    half = next_ref.shape[0]
-    n = 2 * half
-    total = table_in[...] + table_of(got_ref[n:])
+    parts = three_parts(total)
+    for i, out in enumerate((m0_ref, m1_ref, m2_ref, next_ref)):
+        rows = slice(128 * i, 128 * (i + 1))
+        out[:128, :384] = summed(keep_ref, (a0, a1, a2), rows).astype(BF16)
+        out[:128, 384:] = summed(keep2_ref, (b0, b1, b2), rows).astype(BF16)
+        if i < 3:
+            out[128:, :384] = parts
+            out[128:, 384:] = jnp.zeros((EXTRA, 384), BF16)
+
+
+def split_kernel(keep_ref, g0, g1, g2, table_in, one_ref, two_ref, three_ref, own_ref, table_ref):
+    n = own_ref.shape[0]
+    total = summed_table(table_in, (g0, g1, g2), 2 * n)
     table_ref[...] = total
-    send_ref[:half, :384] = added(keep_ref[:half], got_ref[:half]).astype(BF16)
-    send_ref[:half, 384:] = added(keep2_ref[:half], got2_ref[:half]).astype(BF16)
-    next_ref[:, :384] = added(keep_ref[half:], got_ref[half:n]).astype(BF16)
-    next_ref[:, 384:] = added(keep2_ref[half:], got2_ref[half:]).astype(BF16)
-    send_ref[half:, :384] = three_parts(total)
-    send_ref[half:, 384:] = jnp.zeros((EXTRA, 384), BF16)
-
-
-def split_kernel(keep_ref, got_ref, table_in, one_ref, two_ref, three_ref, own_ref, table_ref):
-    n = own_ref.shape[0]
-    total = table_in[...] + table_of(got_ref[2 * n :, :384])
-    table_ref[...] = total
-    far = added(keep_ref[:n], got_ref[:n])
+    far = summed(keep_ref, (g0, g1, g2), slice(0, n))
     one_ref[:n] = far[:, :384].astype(BF16)
     one_ref[n:] = three_parts(total)
     two_ref[...] = far[:, 384:].astype(BF16)
-    near = added(keep_ref[n:], got_ref[n : 2 * n])
+    near = summed(keep_ref, (g0, g1, g2), slice(n, 2 * n))
     own_ref[...] = near[:, :384]
     three_ref[...] = near[:, 384:]
 
@@ -415,8 +425,9 @@
     f32, b16 = (lambda *s: sds(s, F32)), (lambda *s: sds(s, BF16))
     v32, v16 = (lambda *s: pltpu.VMEM(s, F32)), (lambda *s: pltpu.VMEM(s, BF16))
     tile_flops = 6 * 2 * TILE * BAND * HDIM
+    in_hbm = tuple(pltpu.with_memory_space_constraint(v, pltpu.HBM) for v in (inputs, w_query, w_key, w_value))
     tail, x, wq, wk, wv = call(
-        load_kernel, (inputs, w_query, w_key, w_value),
+        load_kernel, in_hbm,
         (b16(REACH, 512), b16(1024, 2048), b16(2048, 256), b16(2048, 256), b16(2048, 256)),
         (pltpu.SemaphoreType.DMA((5,)),), flops=2 * 256 * 2048 * 512, any_ins=(0, 1, 2, 3), limit=LOAD_LIMIT,
     )
@@ -441,34 +452,29 @@
     )
     kg, vg, own, swap = call(finish_kernel, (kg, vg, edge, back, near), (b16(1024, 256),) * 2 + (b16(1024, 384),) * 2)
     got = core_swap(swap)
-    sem = pltpu.SemaphoreType.DMA((3,))
     product = 2 * 1024 * 2048 * 384
-    send, keep, table = call(
-        own_kernel, (x, own, pat), (b16(1024 + EXTRA, 384), b16(1024, 384), f32(2, 384)),
-        (v16(2048, 384), v16(EXTRA, 384), v32(8, 640), sem), flops=product, any_outs=(0, 1),
-    )
-    send2, keep2 = call(
-        other_kernel, (x, got), (b16(1024, 384),) * 2, (v16(2048, 384), sem),
-        flops=product, any_outs=(0, 1),
-    )
-    got = exchange(send, OWN, 0)
-    got2 = exchange(send2, OTHER, 0)
-    send, keep, table = call(level_kernel, (keep, got, table), (b16(512 + EXTRA, 384), b16(512, 384), f32(2, 384)))
-    got = exchange(send, OWN, 1)
-    send2, keep2 = added(keep2[:512], got2[:512]).astype(BF16), added(keep2[512:], got2[512:]).astype(BF16)
-    got2 = exchange(send2, OTHER, 1)
-    send, keep, table = call(
-        merge_kernel, (keep, got, keep2, got2, table), (b16(256 + EXTRA, 768), b16(256, 768), f32(2, 384))
-    )
-    got = exchange(send, OWN, 2)
-    send, keep, table = call(level_kernel, (keep, got, table), (b16(128 + EXTRA, 768), b16(128, 768), f32(2, 384)))
-    got = exchange(send, OWN, 3)
+    *send, keep = call(
+        own_kernel, (x, own), (b16(512, 384),) * 4,
+        (v16(2048, 384), pltpu.SemaphoreType.DMA((4,))), flops=product, any_outs=(0, 1, 2, 3),
+    )
+    *send2, keep2, table = call(
+        other_kernel, (x, got, pat), (b16(512 + EXTRA, 384),) * 3 + (b16(512, 384), f32(2, 384)),
+        (v16(2048, 384), v16(EXTRA, 384), v32(8, 640), pltpu.SemaphoreType.DMA((7,))),
+        flops=product, any_outs=(0, 1, 2, 3),
+    )
+    a = exchange_quarters(send, OWN, 0)
+    b = exchange_quarters(send2, OTHER, 0)
+    *send, keep, table = call(
+        merge_kernel, (keep, *a, keep2, *b, table),
+        (b16(128 + EXTRA, 768),) * 3 + (b16(128, 768), f32(2, 384)),
+    )
+    c = exchange_quarters(send, OWN, 2)
     one, two, three, own, table = call(
-        split_kernel, (keep, got, table),
+        split_kernel, (keep, *c, table),
         (b16(64 + EXTRA, 384), b16(64, 384), f32(64, 384), f32(64, 384), f32(2, 384)),
     )
-    one = exchange(one, OWN, 4)
-    two = exchange(two, OWN, 4, across=1)
+    one = exchange(one, OWN, (4,))
+    two = exchange(two, OWN, (4,), across=1)
     three = core_swap(three)
     dwq, dwk, dwv, table = call(
         output_kernel, (own, one, two, three, table), (f32(64, 256),) * 3 + (f32(*rel_table.shape),)

time: 94.3 us -> 84.1 us (0.89); the launches traced: 92.9 us -> 84 us
  local copies, waits for them, and re-layouts: 5.87 us -> 0.01 us
  starting transfers between devices: 33.9 us -> 28.6 us
  Pallas kernels: 22.2 us -> 25.8 us
  waiting for transfers between devices: 29.9 us -> 28.8 us
    unnamed x12 -> x4, local copies, waits for them, and re-layouts: 5.87 us -> 0.01 us
    ppermute x8 -> x11, starting transfers between devices: 29.1 us -> 23.8 us  [exchange(): lax.ppermute(block, SP + ('core',), level_route(sequences, steps, across))]
    pallas_call x12 -> x10, Pallas kernels: 22.2 us -> 25.8 us  [call(): pl.pallas_call(kernel, grid=grid, in_specs=specs, out_specs=out_specs, ou...]
    ppermute x8 -> x11, waiting for transfers between devices: 26.6 us -> 25.5 us  [exchange(): lax.ppermute(block, SP + ('core',), level_route(sequences, steps, across))]
  transfers between devices with their start and end apart: 12 -> 15, of which waited for: 9 -> 8; matrix products, arithmetic and copies ran while one was open for 0% -> 0% of each run, Pallas kernels for 18% -> 21%
where the time goes in v2:
time: 84.1 us; the launch traced here: 84 us
  waiting for transfers between devices  28.8 us (34%)
  starting transfers between devices  28.6 us (34%)
  Pallas kernels  25.8 us (31%)
    pallas_call x10, Pallas kernels, call(): pl.pallas_call(kernel, grid=grid, in_specs=specs, out_specs=out_specs, ou...  25.8 us
    ppermute x11, waiting for transfers between devices, exchange(): lax.ppermute(block, SP + ('core',), level_route(sequences, steps, across))  25.5 us
    ppermute x11, starting transfers between devices, exchange(): lax.ppermute(block, SP + ('core',), level_route(sequences, steps, across))  23.8 us
    ppermute x2, starting transfers between devices, neighbour(): return lax.ppermute(block, SP, route)  4.7 us
    ppermute x2, waiting for transfers between devices, neighbour(): return lax.ppermute(block, SP, route)  3.28 us
  transfers between devices with their start and end apart: 15, of which 8 were waited for; matrix products, arithmetic and copies ran while one was open for 0% of the time, Pallas kernels for 21%

profile of v2, /device:TPU:8, one launch (start us, length us, event | category | flops | bytes accessed | tf_op | source)
XLA Modules:
  0.0 84.0 jit_solution(17463123056002476773)
XLA Ops:
  0.6 3.2 %shard_map.117 = (bf16[256,512]{1,0:T(8,128)(2,1)S(1)}, bf16[1024,2048]{1,0:T(8,128)(2,1)S(1)}, bf16[2048,256]{1,0:T(8,128)(2,1)S(1)}, bf16[2048,256]{1,0:T(8,128)(2,1)S(1)}, bf16[2048,256]{1,0:T(8,128)(2,1)S(1)}) custom-call(bf16[1024,2048]{1,0:T(8,128)(2,1)} %x_hbm.1, bf16[2048,256]{1,0:T(8,128)(2,1)} %wq_hbm.1, bf16[2048,256]{1,0:T(8,128)(2,1)} %wk_hbm.1, ...), custom_call_target="tpu_custom_call" | custom-call | flops 536870912 | bytes 14942208 | tf_op jit(solution)/shard_map/pallas_call | solution.py:406
  3.9 3.4 %collective-permute-start = (bf16[256,512]{1,0:T(8,128)(2,1)S(1)}, bf16[256,512]{1,0:T(8,128)(2,1)S(1)}, u32[]{:S(2)}, u32[]{:S(2)}) collective-permute-start(bf16[256,512]{1,0:T(8,128)(2,1)S(1)} %get-tuple-element.60), channel_id=1, source_target_pairs={{0,8},{8,16},{16,24},{24,32},{32,40},{40,48},{48,56},{56,64},{64,7... | collective-permute-start | bytes 786440 | tf_op jit(solution)/shard_map/ppermute | solution.py:421
  7.3 0.0 copy-start
  7.3 0.0 copy-start.1
  7.3 3.4 %shard_map.118 = (bf16[1024,256]{1,0:T(8,128)(2,1)S(1)}, bf16[1024,256]{1,0:T(8,128)(2,1)S(1)}, bf16[1024,256]{1,0:T(8,128)(2,1)S(1)}) custom-call(bf16[1024,2048]{1,0:T(8,128)(2,1)S(1)} %get-tuple-element.53.x_ref, bf16[2048,256]{1,0:T(8,128)(2,1)S(1)} %get-tuple-element.54.wq_ref, bf16[2048,256]{1,0:T(8,128)(2,1)S(1)} %get-tuple-element.55.wk_ref, ...), custom_call_target="tpu_custom_call" | custom-call | flops 3221225472 | bytes 8912896 | tf_op jit(solution)/shard_map/pallas_call | solution.py:406
  10.7 2.1 %collective-permute-done.halo_ref = bf16[256,512]{1,0:T(8,128)(2,1)S(1)} collective-permute-done((bf16[256,512]{1,0:T(8,128)(2,1)S(1)}, bf16[256,512]{1,0:T(8,128)(2,1)S(1)}, u32[]{:S(2)}, u32[]{:S(2)}) %collective-permute-start) | collective-permute-done | bytes 262176 | tf_op jit(solution)/shard_map/ppermute | solution.py:421
  12.8 0.0 copy-done
  12.8 0.0 copy-done.1
  12.8 2.3 %shard_map.119 = (bf16[256,256]{1,0:T(8,128)(2,1)S(1)}, f32[256,512]{1,0:T(8,128)S(1)}, bf16[256,512]{1,0:T(8,128)(2,1)S(1)}, f32[2,384,128]{2,1,0:T(8,128)S(1)}, f32[2,384,128]{2,1,0:T(8,128)S(1)}) custom-call(bf16[1024,256]{1,0:T(8,128)(2,1)S(1)} %get-tuple-element.57.q_ref, bf16[1024,256]{1,0:T(8,128)(2,1)S(1)} %get-tuple-element.58.k_ref, ...), custom_call_target="tpu_custom_call" | custom-call | flops 301989888 | bytes 4065288 | tf_op jit(solution)/shard_map/pallas_call | solution.py:406
  15.2 1.3 %collective-permute-start.1 = (bf16[256,512]{1,0:T(8,128)(2,1)S(1)}, bf16[256,512]{1,0:T(8,128)(2,1)S(1)}, u32[]{:S(2)}, u32[]{:S(2)}) collective-permute-start(bf16[256,512]{1,0:T(8,128)(2,1)S(1)} %get-tuple-element.69), channel_id=1, source_target_pairs={{8,0},{16,8},{24,16},{32,24},{40,32},{48,40},{56,48},{64,56},{72,6... | collective-permute-start | bytes 786440 | tf_op jit(solution)/shard_map/ppermute | solution.py:421
  16.5 7.3 %shard_map.120 = (bf16[1024,256]{1,0:T(8,128)(2,1)}, bf16[1024,256]{1,0:T(8,128)(2,1)S(1)}, bf16[768,256]{1,0:T(8,128)(2,1)S(1)}, bf16[768,256]{1,0:T(8,128)(2,1...) custom-call(bf16[1024,256]{1,0:T(8,128)(2,1)S(1)} %get-tuple-element.57.q_ref, ...), custom_call_target="tpu_custom_call" | custom-call | flops 905969664 | bytes 6291456 | tf_op jit(solution)/shard_map/pallas_call | solution.py:406
  23.8 1.2 %collective-permute-done.1.back_ref = bf16[256,512]{1,0:T(8,128)(2,1)S(1)} collective-permute-done((bf16[256,512]{1,0:T(8,128)(2,1)S(1)}, bf16[256,512]{1,0:T(8,128)(2,1)S(1)}, u32[]{:S(2)}, u32[]{:S(2)}) %collective-permute-start.1) | collective-permute-done | bytes 262176 | tf_op jit(solution)/shard_map/ppermute | solution.py:421
  25.0 1.2 %shard_map.121 = (bf16[1024,256]{1,0:T(8,128)(2,1)}, bf16[1024,256]{1,0:T(8,128)(2,1)}, bf16[1024,384]{1,0:T(8,128)(2,1)S(1)}, bf16[1024,384]{1,0:T(8,128)(2,1)S(1)}) custom-call(bf16[768,256]{1,0:T(8,128)(2,1)S(1)} %get-tuple-element.66.kg_in, bf16[768,256]{1,0:T(8,128)(2,1)S(1)} %get-tuple-element.67.vg_in, f32[256,512]{1,0:T(8,128)S(1)} %get-tuple-element.68.edge_ref, ...), custom_call_target="tpu_custom_call" | custom-call | flops 1048576 | bytes 4718592 | tf_op jit(solution)/shard_map/pallas_call | solution.py:406
  26.2 0.0 collective-permute-start.5
  26.2 3.4 %shard_map.122 = (bf16[512,384]{1,0:T(8,128)(2,1)S(1)}, bf16[512,384]{1,0:T(8,128)(2,1)S(1)}, bf16[512,384]{1,0:T(8,128)(2,1)S(1)}, bf16[512,384]{1,0:T(8,128)(2,1)S(1)}) custom-call(bf16[1024,2048]{1,0:T(8,128)(2,1)S(1)} %get-tuple-element.53.x_ref, bf16[1024,384]{1,0:T(8,128)(2,1)S(1)} %get-tuple-element.73.grad_ref), custom_call_target="tpu_custom_call" | custom-call | flops 1610612736 | bytes 6553600 | tf_op jit(solution)/shard_map/pallas_call | solution.py:406
  29.6 4.1 %collective-permute-start.2 = (bf16[512,384]{1,0:T(8,128)(2,1)S(1)}, bf16[512,384]{1,0:T(8,128)(2,1)S(1)}, u32[]{:S(2)}, u32[]{:S(2)}) collective-permute-start(bf16[512,384]{1,0:T(8,128)(2,1)S(1)} %get-tuple-element.75), channel_id=1, source_target_pairs={{0,16},{8,24},{16,0},{24,8},{32,48},{40,56},{48,32},{56,40},{64,80... | collective-permute-start | bytes 1179656 | tf_op jit(solution)/shard_map/ppermute | solution.py:98
  33.6 0.0 collective-permute-done.5.grad_ref
  33.6 3.6 %shard_map.123 = (bf16[528,384]{1,0:T(8,128)(2,1)S(1)}, bf16[528,384]{1,0:T(8,128)(2,1)S(1)}, bf16[528,384]{1,0:T(8,128)(2,1)S(1)}, bf16[512,384]{1,0:T(8,128)(2,1)S(1)}, f32[2,384]{1,0:T(2,128)S(1)}) custom-call(bf16[1024,2048]{1,0:T(8,128)(2,1)S(1)} %get-tuple-element.53.x_ref, bf16[1024,384]{1,0:T(8,128)(2,1)S(1)} %collective-permute-done.5.grad_ref, ...), custom_call_target="tpu_custom_call" | custom-call | flops 1610612736 | bytes 6986752 | tf_op jit(solution)/shard_map/pallas_call | solution.py:406
  37.3 0.1 collective-permute-start.6
  37.4 4.8 %collective-permute-start.7 = (bf16[528,384]{1,0:T(8,128)(2,1)S(1)}, bf16[528,384]{1,0:T(8,128)(2,1)S(1)}, u32[]{:S(2)}, u32[]{:S(2)}) collective-permute-start(bf16[528,384]{1,0:T(8,128)(2,1)S(1)} %get-tuple-element.82), channel_id=1, source_target_pairs={{0,24},{8,16},{16,8},{24,0},{32,56},{40,48},{48,40},{56,32},{64,88... | collective-permute-start | bytes 1216520 | tf_op jit(solution)/shard_map/ppermute | solution.py:98
  42.1 0.0 collective-permute-start.8
  42.1 2.0 %collective-permute-start.3 = (bf16[512,384]{1,0:T(8,128)(2,1)S(1)}, bf16[512,384]{1,0:T(8,128)(2,1)S(1)}, u32[]{:S(2)}, u32[]{:S(2)}) collective-permute-start(bf16[512,384]{1,0:T(8,128)(2,1)S(1)} %get-tuple-element.76), channel_id=1, source_target_pairs={{0,8},{8,0},{16,24},{24,16},{32,40},{40,32},{48,56},{56,48},{64,72... | collective-permute-start | bytes 1179656 | tf_op jit(solution)/shard_map/ppermute | solution.py:98
  44.1 0.0 collective-permute-done.2.a0
  44.2 0.0 collective-permute-start.4
  44.2 10.2 %collective-permute-done.3.a1 = bf16[512,384]{1,0:T(8,128)(2,1)S(1)} collective-permute-done((bf16[512,384]{1,0:T(8,128)(2,1)S(1)}, bf16[512,384]{1,0:T(8,128)(2,1)S(1)}, u32[]{:S(2)}, u32[]{:S(2)}) %collective-permute-start.3) | collective-permute-done | bytes 393248 | tf_op jit(solution)/shard_map/ppermute | solution.py:98
  54.4 0.9 %collective-permute-done.4.a2 = bf16[512,384]{1,0:T(8,128)(2,1)S(1)} collective-permute-done((bf16[512,384]{1,0:T(8,128)(2,1)S(1)}, bf16[512,384]{1,0:T(8,128)(2,1)S(1)}, u32[]{:S(2)}, u32[]{:S(2)}) %collective-permute-start.4) | collective-permute-done | bytes 393248 | tf_op jit(solution)/shard_map/ppermute | solution.py:98
  55.3 0.0 collective-permute-done.6.b0
  55.3 0.0 collective-permute-done.7.b1
  55.3 0.0 collective-permute-done.8.b2
  55.3 0.4 shard_map.124
  55.8 4.0 %collective-permute-start.9 = (bf16[144,768]{1,0:T(8,128)(2,1)S(1)}, bf16[144,768]{1,0:T(8,128)(2,1)S(1)}, u32[]{:S(2)}, u32[]{:S(2)}) collective-permute-start(bf16[144,768]{1,0:T(8,128)(2,1)S(1)} %get-tuple-element.86), channel_id=1, source_target_pairs={{0,64},{8,72},{16,80},{24,88},{32,224},{40,232},{48,240},{56,248},... | collective-permute-start | bytes 663560 | tf_op jit(solution)/shard_map/ppermute | solution.py:98
  59.8 4.0 %collective-permute-start.10 = (bf16[144,768]{1,0:T(8,128)(2,1)S(1)}, bf16[144,768]{1,0:T(8,128)(2,1)S(1)}, u32[]{:S(2)}, u32[]{:S(2)}) collective-permute-start(bf16[144,768]{1,0:T(8,128)(2,1)S(1)} %get-tuple-element.87), channel_id=1, source_target_pairs={{0,32},{8,40},{16,48},{24,56},{32,0},{40,8},{48,16},{56,24},{64,96... | collective-permute-start | bytes 663560 | tf_op jit(solution)/shard_map/ppermute | solution.py:98
  63.8 0.0 collective-permute-start.11
  63.8 2.9 %collective-permute-done.9.g0 = bf16[144,768]{1,0:T(8,128)(2,1)S(1)} collective-permute-done((bf16[144,768]{1,0:T(8,128)(2,1)S(1)}, bf16[144,768]{1,0:T(8,128)(2,1)S(1)}, u32[]{:S(2)}, u32[]{:S(2)}) %collective-permute-start.9) | collective-permute-done | bytes 221216 | tf_op jit(solution)/shard_map/ppermute | solution.py:98
  66.7 3.4 %collective-permute-done.10.g1 = bf16[144,768]{1,0:T(8,128)(2,1)S(1)} collective-permute-done((bf16[144,768]{1,0:T(8,128)(2,1)S(1)}, bf16[144,768]{1,0:T(8,128)(2,1)S(1)}, u32[]{:S(2)}, u32[]{:S(2)}) %collective-permute-start.10) | collective-permute-done | bytes 221216 | tf_op jit(solution)/shard_map/ppermute | solution.py:98
  70.1 0.8 collective-permute-done.11.g2
  70.9 0.1 shard_map.125
  71.1 0.1 collective-permute-start.14
  71.2 3.2 %collective-permute-start.12 = (bf16[80,384]{1,0:T(8,128)(2,1)S(1)}, bf16[80,384]{1,0:T(8,128)(2,1)S(1)}, u32[]{:S(2)}, u32[]{:S(2)}) collective-permute-start(bf16[80,384]{1,0:T(8,128)(2,1)S(1)} %get-tuple-element.91), channel_id=1, source_target_pairs={{0,96},{8,104},{16,112},{24,120},{32,192},{40,200},{48,208},{56,21... | collective-permute-start | bytes 184328 | tf_op jit(solution)/shard_map/ppermute | solution.py:98
  74.4 1.7 %collective-permute-start.13 = (bf16[64,384]{1,0:T(8,128)(2,1)S(1)}, bf16[64,384]{1,0:T(8,128)(2,1)S(1)}, u32[]{:S(2)}, u32[]{:S(2)}) collective-permute-start(bf16[64,384]{1,0:T(8,128)(2,1)S(1)} %get-tuple-element.92), channel_id=1, source_target_pairs={{0,97},{8,105},{16,113},{24,121},{32,193},{40,201},{48,209},{56,21... | collective-permute-start | bytes 147464 | tf_op jit(solution)/shard_map/ppermute | solution.py:98
  76.1 7.2 %collective-permute-done.13.two_ref = bf16[64,384]{1,0:T(8,128)(2,1)S(1)} collective-permute-done((bf16[64,384]{1,0:T(8,128)(2,1)S(1)}, bf16[64,384]{1,0:T(8,128)(2,1)S(1)}, u32[]{:S(2)}, u32[]{:S(2)}) %collective-permute-start.13) | collective-permute-done | bytes 49184 | tf_op jit(solution)/shard_map/ppermute | solution.py:98
  83.3 0.0 collective-permute-done.12.one_ref
  83.3 0.0 collective-permute-done.14.three_ref
  83.3 0.7 shard_map.126
Async XLA Ops:
  3.9 8.9 %collective-permute-start = (bf16[256,512]{1,0:T(8,128)(2,1)S(1)}, bf16[256,512]{1,0:T(8,128)(2,1)S(1)}, u32[]{:S(2)}, u32[]{:S(2)}) collective-permute-start(bf16[256,512]{1,0:T(8,128)(2,1)S(1)} %get-tuple-element.60), channel_id=1, source_target_pairs={{0,8},{8,16},{16,24},{24,32},{32,40},{40,48},{48,56},{56,64},{64,7... | collective-permute-start | bytes 786440 | tf_op jit(solution)/shard_map/ppermute | solution.py:421
  7.3 5.5 %copy-start = (bf16[1024,256]{1,0:T(8,128)(2,1)S(1)}, bf16[1024,256]{1,0:T(8,128)(2,1)}, u32[]{:S(2)}) copy-start(bf16[1024,256]{1,0:T(8,128)(2,1)} %og_ref.3) | copy-start | bytes 1572868
  7.3 5.5 %copy-start.1 = (f32[2,257]{1,0:T(2,128)S(1)}, f32[2,257]{1,0:T(2,128)}, u32[]{:S(2)}) copy-start(f32[2,257]{1,0:T(2,128)} %rel_ref.1) | copy-start | bytes 6172
  15.2 9.8 %collective-permute-start.1 = (bf16[256,512]{1,0:T(8,128)(2,1)S(1)}, bf16[256,512]{1,0:T(8,128)(2,1)S(1)}, u32[]{:S(2)}, u32[]{:S(2)}) collective-permute-start(bf16[256,512]{1,0:T(8,128)(2,1)S(1)} %get-tuple-element.69), channel_id=1, source_target_pairs={{8,0},{16,8},{24,16},{32,24},{40,32},{48,40},{56,48},{64,56},{72,6... | collective-permute-start | bytes 786440 | tf_op jit(solution)/shard_map/ppermute | solution.py:421
  26.2 7.4 %collective-permute-start.5 = (bf16[1024,384]{1,0:T(8,128)(2,1)S(1)}, bf16[1024,384]{1,0:T(8,128)(2,1)S(1)}, u32[]{:S(2)}, u32[]{:S(2)}) collective-permute-start(bf16[1024,384]{1,0:T(8,128)(2,1)S(1)} %get-tuple-element.78), channel_id=1, source_target_pairs={{0,1},{1,0},{2,3},{3,2},{4,5},{5,4},{6,7},{7,6},{8,9},{9,8},{10,11... | collective-permute-start | bytes 2359304 | tf_op jit(solution)/shard_map/ppermute | solution.py:107
  29.6 14.6 %collective-permute-start.2 = (bf16[512,384]{1,0:T(8,128)(2,1)S(1)}, bf16[512,384]{1,0:T(8,128)(2,1)S(1)}, u32[]{:S(2)}, u32[]{:S(2)}) collective-permute-start(bf16[512,384]{1,0:T(8,128)(2,1)S(1)} %get-tuple-element.75), channel_id=1, source_target_pairs={{0,16},{8,24},{16,0},{24,8},{32,48},{40,56},{48,32},{56,40},{64,80... | collective-permute-start | bytes 1179656 | tf_op jit(solution)/shard_map/ppermute | solution.py:98
  37.3 18.0 %collective-permute-start.6 = (bf16[528,384]{1,0:T(8,128)(2,1)S(1)}, bf16[528,384]{1,0:T(8,128)(2,1)S(1)}, u32[]{:S(2)}, u32[]{:S(2)}) collective-permute-start(bf16[528,384]{1,0:T(8,128)(2,1)S(1)} %get-tuple-element.81), channel_id=1, source_target_pairs={{0,16},{8,24},{16,0},{24,8},{32,48},{40,56},{48,32},{56,40},{64,80... | collective-permute-start | bytes 1216520 | tf_op jit(solution)/shard_map/ppermute | solution.py:98
  37.4 18.0 %collective-permute-start.7 = (bf16[528,384]{1,0:T(8,128)(2,1)S(1)}, bf16[528,384]{1,0:T(8,128)(2,1)S(1)}, u32[]{:S(2)}, u32[]{:S(2)}) collective-permute-start(bf16[528,384]{1,0:T(8,128)(2,1)S(1)} %get-tuple-element.82), channel_id=1, source_target_pairs={{0,24},{8,16},{16,8},{24,0},{32,56},{40,48},{48,40},{56,32},{64,88... | collective-permute-start | bytes 1216520 | tf_op jit(solution)/shard_map/ppermute | solution.py:98
  42.1 13.2 %collective-permute-start.8 = (bf16[528,384]{1,0:T(8,128)(2,1)S(1)}, bf16[528,384]{1,0:T(8,128)(2,1)S(1)}, u32[]{:S(2)}, u32[]{:S(2)}) collective-permute-start(bf16[528,384]{1,0:T(8,128)(2,1)S(1)} %get-tuple-element.83), channel_id=1, source_target_pairs={{0,8},{8,0},{16,24},{24,16},{32,40},{40,32},{48,56},{56,48},{64,72... | collective-permute-start | bytes 1216520 | tf_op jit(solution)/shard_map/ppermute | solution.py:98
  42.1 12.3 %collective-permute-start.3 = (bf16[512,384]{1,0:T(8,128)(2,1)S(1)}, bf16[512,384]{1,0:T(8,128)(2,1)S(1)}, u32[]{:S(2)}, u32[]{:S(2)}) collective-permute-start(bf16[512,384]{1,0:T(8,128)(2,1)S(1)} %get-tuple-element.76), channel_id=1, source_target_pairs={{0,8},{8,0},{16,24},{24,16},{32,40},{40,32},{48,56},{56,48},{64,72... | collective-permute-start | bytes 1179656 | tf_op jit(solution)/shard_map/ppermute | solution.py:98
  44.2 11.2 %collective-permute-start.4 = (bf16[512,384]{1,0:T(8,128)(2,1)S(1)}, bf16[512,384]{1,0:T(8,128)(2,1)S(1)}, u32[]{:S(2)}, u32[]{:S(2)}) collective-permute-start(bf16[512,384]{1,0:T(8,128)(2,1)S(1)} %get-tuple-element.77), channel_id=1, source_target_pairs={{0,24},{8,16},{16,8},{24,0},{32,56},{40,48},{48,40},{56,32},{64,88... | collective-permute-start | bytes 1179656 | tf_op jit(solution)/shard_map/ppermute | solution.py:98
  55.8 10.9 %collective-permute-start.9 = (bf16[144,768]{1,0:T(8,128)(2,1)S(1)}, bf16[144,768]{1,0:T(8,128)(2,1)S(1)}, u32[]{:S(2)}, u32[]{:S(2)}) collective-permute-start(bf16[144,768]{1,0:T(8,128)(2,1)S(1)} %get-tuple-element.86), channel_id=1, source_target_pairs={{0,64},{8,72},{16,80},{24,88},{32,224},{40,232},{48,240},{56,248},... | collective-permute-start | bytes 663560 | tf_op jit(solution)/shard_map/ppermute | solution.py:98
  59.8 10.3 %collective-permute-start.10 = (bf16[144,768]{1,0:T(8,128)(2,1)S(1)}, bf16[144,768]{1,0:T(8,128)(2,1)S(1)}, u32[]{:S(2)}, u32[]{:S(2)}) collective-permute-start(bf16[144,768]{1,0:T(8,128)(2,1)S(1)} %get-tuple-element.87), channel_id=1, source_target_pairs={{0,32},{8,40},{16,48},{24,56},{32,0},{40,8},{48,16},{56,24},{64,96... | collective-permute-start | bytes 663560 | tf_op jit(solution)/shard_map/ppermute | solution.py:98
  63.8 7.1 %collective-permute-start.11 = (bf16[144,768]{1,0:T(8,128)(2,1)S(1)}, bf16[144,768]{1,0:T(8,128)(2,1)S(1)}, u32[]{:S(2)}, u32[]{:S(2)}) collective-permute-start(bf16[144,768]{1,0:T(8,128)(2,1)S(1)} %get-tuple-element.88), channel_id=1, source_target_pairs={{0,224},{8,232},{16,240},{24,248},{32,64},{40,72},{48,80},{56,88},... | collective-permute-start | bytes 663560 | tf_op jit(solution)/shard_map/ppermute | solution.py:98
  71.1 12.2 %collective-permute-start.14 = (f32[64,384]{1,0:T(8,128)S(1)}, f32[64,384]{1,0:T(8,128)S(1)}, u32[]{:S(2)}, u32[]{:S(2)}) collective-permute-start(f32[64,384]{1,0:T(8,128)S(1)} %get-tuple-element.93), channel_id=1, source_target_pairs={{0,1},{1,0},{2,3},{3,2},{4,5},{5,4},{6,7},{7,6},{8,9},{9,8},{10,11... | collective-permute-start | bytes 294920 | tf_op jit(solution)/shard_map/ppermute | solution.py:107
  71.2 12.1 %collective-permute-start.12 = (bf16[80,384]{1,0:T(8,128)(2,1)S(1)}, bf16[80,384]{1,0:T(8,128)(2,1)S(1)}, u32[]{:S(2)}, u32[]{:S(2)}) collective-permute-start(bf16[80,384]{1,0:T(8,128)(2,1)S(1)} %get-tuple-element.91), channel_id=1, source_target_pairs={{0,96},{8,104},{16,112},{24,120},{32,192},{40,200},{48,208},{56,21... | collective-permute-start | bytes 184328 | tf_op jit(solution)/shard_map/ppermute | solution.py:98
  74.4 8.9 %collective-permute-start.13 = (bf16[64,384]{1,0:T(8,128)(2,1)S(1)}, bf16[64,384]{1,0:T(8,128)(2,1)S(1)}, u32[]{:S(2)}, u32[]{:S(2)}) collective-permute-start(bf16[64,384]{1,0:T(8,128)(2,1)S(1)} %get-tuple-element.92), channel_id=1, source_target_pairs={{0,97},{8,105},{16,113},{24,121},{32,193},{40,201},{48,209},{56,21... | collective-permute-start | bytes 147464 | tf_op jit(solution)/shard_map/ppermute | solution.py:98

commit v3 on v2

--- a/solution.py
+++ b/solution.py
@@ -17,6 +17,7 @@
 NZ, NX = 8, 4
 ROWS = 64
 EXTRA = 16
+LATE = 384
 VMEM_LIMIT = 24 << 20
 LOAD_LIMIT = 24 << 20
 CHUNKS = 4
@@ -36,10 +37,8 @@
 
 XO, XE = ("sp_1", odd_pair), ("sp_1", even_pair(NX))
 ZO, ZE = ("sp_0", odd_pair), ("sp_0", even_pair(NZ))
-ZF = ("sp_0", lambda i: (i + NZ // 2) % NZ)
 Z3 = ("sp_0", lambda i: (3, 6, 5, 0, 7, 2, 1, 4)[i])
-OWN = ((XO, XE, ZO, ZE, Z3), (ZO, ZE, XO, XE, ZF))
-OTHER = ((XE, XO, ZO, ZE, Z3), (ZE, ZO, XO, XE, ZF))
+LEVELS = ((XO, XE, ZO, ZE, Z3), (ZO, ZE, XO, XE, Z3))
 
 
 def held_order(steps, device):
@@ -71,18 +70,18 @@
     return codes
 
 
-def unit_places(sequences):
+def unit_places():
     core = lax.axis_index("core")
     places = []
-    for levels in sequences:
+    for levels in LEVELS:
         along_z, along_x = axis_codes(levels, "sp_0"), axis_codes(levels, "sp_1")
         places.append([along_z[unit // NX] + along_x[unit % NX] for unit in range(NZ * NX)])
     return [jnp.where(core == 0, a, b) for a, b in zip(*places)]
 
 
-def level_route(sequences, steps, across=0):
+def level_route(steps, across=0):
     route = []
-    for core, levels in enumerate(sequences):
+    for core, levels in enumerate(LEVELS):
         for z in range(NZ):
             for x in range(NX):
                 at = {"sp_0": z, "sp_1": x}
@@ -94,13 +93,13 @@
     return route
 
 
-def exchange(block, sequences, steps, across=0):
-    return lax.ppermute(block, SP + ("core",), level_route(sequences, steps, across))
-
-
-def exchange_quarters(blocks, sequences, level):
+def exchange(block, steps, across=0):
+    return lax.ppermute(block, SP + ("core",), level_route(steps, across))
+
+
+def exchange_quarters(blocks, level):
     paths = ((level, level + 1), (level,), (level + 1,))
-    return [exchange(x, sequences, path) for x, path in zip(blocks, paths)]
+    return [exchange(x, path) for x, path in zip(blocks, paths)]
 
 
 def core_swap(block):
@@ -152,9 +151,54 @@
     v_ref[...] = dot(x, wv_ref[...]).astype(BF16)
 
 
+def tiles(which, q_ref, k_ref, v_ref, og_ref, bias_ref, kt_s, vt_s, pat_ref, dq_ref, dq_at, ka_s, va_s, acc_at):
+    for tile in which:
+        rows = slice(REACH + tile * TILE, REACH + (tile + 1) * TILE)
+        band = slice(tile * TILE, tile * TILE + BAND)
+        to = slice(band.start - acc_at, band.stop - acc_at)
+        for h in range(2):
+            cols = slice(h * HDIM, (h + 1) * HDIM)
+            score_grad, query_part, key_part, value_part = tile_grads(
+                q_ref[rows, cols], og_ref[rows, cols], k_ref[band, cols], v_ref[band, cols],
+                kt_s[cols, to], vt_s[cols, to], bias_ref[h],
+            )
+            pat_ref[h] += score_grad
+            dq_ref[rows.start - dq_at : rows.stop - dq_at, cols] = query_part.astype(BF16)
+            ka_s[to, cols] += key_part
+            va_s[to, cols] += value_part
+
+
+def late_kernel(
+    q_ref, k_ref, v_ref, og_ref, rel_ref,
+    dq_ref, acc_ref, bias_ref, pat_ref,
+    kt_s, vt_s, ka_s, va_s,
+):
+    u = lax.broadcasted_iota(jnp.int32, (BAND, TILE), 0)
+    col = lax.broadcasted_iota(jnp.int32, (BAND, TILE), 1)
+    low = jnp.where(col < SEG, 0, SEG)
+    inside = (u >= low) & (u < low + REACH + SEG)
+    for h in range(2):
+        table = rel_ref[h : h + 1, :]
+        far = jnp.concatenate([table[:, :256], jnp.broadcast_to(table[:, 256:257], (1, 256))], axis=1)
+        far = jnp.broadcast_to(far, (BAND, 512))
+        skew = pltpu.roll(far, 0, 1, stride=1, stride_axis=0)[:, BAND:]
+        bias_ref[h] = jnp.where(inside, skew, -jnp.inf)
+    pat_ref[...] = jnp.zeros_like(pat_ref)
+    kt_s[...] = k_ref[LATE:].T
+    vt_s[...] = v_ref[LATE:].T
+    ka_s[...] = jnp.zeros_like(ka_s)
+    va_s[...] = jnp.zeros_like(va_s)
+    tiles(
+        range(3, 6), q_ref, k_ref, v_ref, og_ref, bias_ref, kt_s, vt_s, pat_ref, dq_ref, LATE + REACH,
+        ka_s, va_s, LATE,
+    )
+    acc_ref[:, :256] = ka_s[...]
+    acc_ref[:, 256:] = va_s[...]
+
+
 def first_kernel(
-    q_ref, k_ref, v_ref, halo_ref, og_ref, rel_ref,
-    dq_ref, edge_ref, back_ref, bias_ref, pat_ref,
+    q_ref, k_ref, v_ref, halo_ref, og_ref, bias_ref, pat_in,
+    dq_ref, edge_ref, back_ref, pat_ref,
     k_s, v_s, kt_s, vt_s, ka_s, va_s,
 ):
     k_s[:REACH] = halo_ref[:, :256]
@@ -165,17 +209,9 @@
     vt_s[...] = v_s[...].T
     ka_s[...] = jnp.zeros_like(ka_s)
     va_s[...] = jnp.zeros_like(va_s)
+    pat_ref[...] = pat_in[...]
     outside = (lax.axis_index("sp_0") == 0) & (lax.axis_index("sp_1") == 0)
     u = lax.broadcasted_iota(jnp.int32, (BAND, TILE), 0)
-    col = lax.broadcasted_iota(jnp.int32, (BAND, TILE), 1)
-    low = jnp.where(col < SEG, 0, SEG)
-    inside = (u >= low) & (u < low + REACH + SEG)
-    for h in range(2):
-        table = rel_ref[h : h + 1, :]
-        far = jnp.concatenate([table[:, :256], jnp.broadcast_to(table[:, 256:257], (1, 256))], axis=1)
-        far = jnp.broadcast_to(far, (BAND, 512))
-        skew = pltpu.roll(far, 0, 1, stride=1, stride_axis=0)[:, BAND:]
-        bias_ref[h] = jnp.where(inside, skew, -jnp.inf)
     for t in range(2):
         rows = slice(t * TILE, (t + 1) * TILE)
         band = slice(t * TILE, t * TILE + BAND)
@@ -186,10 +222,7 @@
                 q_ref[rows, cols], og_ref[rows, cols], k_s[band, cols], v_s[band, cols],
                 kt_s[cols, band], vt_s[cols, band], bias,
             )
-            if t == 0:
-                pat_ref[h] = score_grad
-            else:
-                pat_ref[h] += score_grad
+            pat_ref[h] += score_grad
             dq_ref[rows, cols] = query_part.astype(BF16)
             ka_s[band, cols] += key_part
             va_s[band, cols] += value_part
@@ -200,39 +233,32 @@
 
 
 def attn_kernel(
-    q_ref, k_ref, v_ref, og_ref, bias_ref, pat_in, edge_in, dq_in,
+    q_ref, k_ref, v_ref, og_ref, bias_ref, pat_in, edge_in, acc_in, dq_in, dq_late,
     dq_ref, near_ref, kg_ref, vg_ref, edge_ref, pat_ref,
     kt_s, vt_s, ka_s, va_s,
 ):
-    kt_s[...] = k_ref[...].T
-    vt_s[...] = v_ref[...].T
+    kt_s[...] = k_ref[: LATE + REACH].T
+    vt_s[...] = v_ref[: LATE + REACH].T
     ka_s[:REACH] = edge_in[:, :256]
     va_s[:REACH] = edge_in[:, 256:]
-    ka_s[REACH:] = jnp.zeros((768, 256), F32)
-    va_s[REACH:] = jnp.zeros((768, 256), F32)
+    ka_s[REACH:LATE] = jnp.zeros((LATE - REACH, 256), F32)
+    va_s[REACH:LATE] = jnp.zeros((LATE - REACH, 256), F32)
+    ka_s[LATE:] = acc_in[: LATE + REACH - LATE, :256]
+    va_s[LATE:] = acc_in[: LATE + REACH - LATE, 256:]
     pat_ref[...] = pat_in[...]
     near_ref[:REACH] = dq_in[...]
-    for tile in range(6):
-        rows = slice(REACH + tile * TILE, REACH + (tile + 1) * TILE)
-        band = slice(tile * TILE, tile * TILE + BAND)
-        for h in range(2):
-            cols = slice(h * HDIM, (h + 1) * HDIM)
-            score_grad, query_part, key_part, value_part = tile_grads(
-                q_ref[rows, cols], og_ref[rows, cols], k_ref[band, cols], v_ref[band, cols],
-                kt_s[cols, band], vt_s[cols, band], bias_ref[h],
-            )
-            pat_ref[h] += score_grad
-            near_ref[rows, cols] = query_part.astype(BF16)
-            ka_s[band, cols] += key_part
-            va_s[band, cols] += value_part
+    near_ref[LATE + REACH :] = dq_late[...]
+    tiles(range(3), q_ref, k_ref, v_ref, og_ref, bias_ref, kt_s, vt_s, pat_ref, near_ref, 0, ka_s, va_s, 0)
     dq_ref[...] = near_ref[...]
-    kg_ref[...] = ka_s[:768].astype(BF16)
-    vg_ref[...] = va_s[:768].astype(BF16)
-    edge_ref[:, :256] = ka_s[768:]
-    edge_ref[:, 256:] = va_s[768:]
-
-
-def finish_kernel(kg_in, vg_in, edge_ref, back_ref, dq_ref, kg_ref, vg_ref, own_ref, swap_ref):
+    last = LATE + REACH
+    kg_ref[:last] = ka_s[...].astype(BF16)
+    vg_ref[:last] = va_s[...].astype(BF16)
+    kg_ref[last:] = acc_in[last - LATE : 768 - LATE, :256].astype(BF16)
+    vg_ref[last:] = acc_in[last - LATE : 768 - LATE, 256:].astype(BF16)
+    edge_ref[...] = acc_in[768 - LATE :]
+
+
+def finish_kernel(kg_in, vg_in, edge_ref, back_ref, kg_ref, vg_ref, own_ref, swap_ref):
     kg_ref[:768] = kg_in[...]
     vg_ref[:768] = vg_in[...]
     kg_ref[768:] = (edge_ref[:, :256] + back_ref[:, :256].astype(F32)).astype(BF16)
@@ -241,17 +267,13 @@
 
     @pl.when(core == 0)
     def _():
-        own_ref[:, :256] = kg_ref[...]
-        own_ref[:, 256:] = dq_ref[:, :128]
-        swap_ref[:, :256] = vg_ref[...]
-        swap_ref[:, 256:] = dq_ref[:, 128:]
+        own_ref[...] = kg_ref[...]
+        swap_ref[...] = vg_ref[...]
 
     @pl.when(core == 1)
     def _():
-        own_ref[:, :256] = vg_ref[...]
-        own_ref[:, 256:] = dq_ref[:, 128:]
-        swap_ref[:, :256] = kg_ref[...]
-        swap_ref[:, 256:] = dq_ref[:, :128]
+        own_ref[...] = vg_ref[...]
+        swap_ref[...] = kg_ref[...]
 
 
 def store_units(value, chunk, places, out_s):
@@ -261,8 +283,8 @@
         out_s[pl.ds(at, ROWS), :] = value[i * ROWS : (i + 1) * ROWS].astype(BF16)
 
 
-def placed_product(x_ref, grad_ref, sequences, out_s):
-    places = unit_places(sequences)
+def placed_product(x_ref, grad_ref, out_s):
+    places = unit_places()
     for c in range(CHUNKS):
         cols = slice(c * WIDTH, (c + 1) * WIDTH)
         store_units(dot(x_ref[:, cols], grad_ref[...], ((0,), (0,))), c, places, out_s)
@@ -272,13 +294,13 @@
     high = table.astype(BF16).astype(F32)
     mid = (table - high).astype(BF16).astype(F32)
     low = table - high - mid
-    rest = jnp.zeros((EXTRA - 6, table.shape[1]), F32)
+    rest = jnp.zeros((EXTRA - 12, table.shape[1]), F32)
     return jnp.concatenate([high, mid, low, rest], axis=0).astype(BF16)
 
 
 def table_of(parts):
     parts = parts.astype(F32)
-    return parts[0:2] + parts[2:4] + parts[4:6]
+    return parts[0:4] + parts[4:8] + parts[8:12]
 
 
 def copy_out(pairs, sem):
@@ -289,15 +311,10 @@
         copy.wait()
 
 
-def own_kernel(x_ref, grad_ref, m0_hbm, m1_hbm, m2_hbm, keep_hbm, out_s, sem):
-    placed_product(x_ref, grad_ref, OWN, out_s)
-    copy_out([(out_s.at[512 * i : 512 * (i + 1)], m) for i, m in enumerate((m0_hbm, m1_hbm, m2_hbm, keep_hbm))], sem)
-
-
-def other_kernel(
+def query_kernel(
     x_ref, grad_ref, pat_ref, m0_hbm, m1_hbm, m2_hbm, keep_hbm, table_ref, out_s, parts_s, diag_s, sem
 ):
-    placed_product(x_ref, grad_ref, OTHER, out_s)
+    placed_product(x_ref, grad_ref, out_s)
     for h in range(2):
         diag_s[...] = jnp.zeros_like(diag_s)
         for a in range(BAND // 8):
@@ -307,8 +324,8 @@
         for s in range(8):
             total += diag_s[s : s + 1, s : s + 512]
         far = jnp.sum(total[:, 256:], axis=1, keepdims=True)
-        table_ref[h : h + 1, :256] = total[:, :256]
-        table_ref[h : h + 1, 256:] = jnp.broadcast_to(far, (1, 128))
+        table_ref[h : h + 1, :] = total[:, :256]
+        table_ref[2 + h : 3 + h, :] = jnp.broadcast_to(far, (1, 256))
     parts_s[...] = three_parts(table_ref[...])
     pairs = [(out_s.at[1536:], keep_hbm)]
     for i, m in enumerate((m0_hbm, m1_hbm, m2_hbm)):
@@ -316,6 +333,28 @@
     copy_out(pairs, sem)
 
 
+def own_kernel(x_ref, grad_ref, out_ref):
+    placed_product(x_ref, grad_ref, out_ref)
+
+
+def other_kernel(x_ref, grad_ref, own_hbm, m0_hbm, m1_hbm, m2_hbm, keep_hbm, out_s, sem, sem2):
+    pairs = []
+    for i, m in enumerate((m0_hbm, m1_hbm, m2_hbm, keep_hbm)):
+        rows = slice(512 * i, 512 * (i + 1))
+        pairs.append(pltpu.make_async_copy(own_hbm.at[rows], m.at[:, :256], sem2.at[i]))
+        pairs[-1].start()
+    placed_product(x_ref, grad_ref, out_s)
+    copy_out(
+        [
+            (out_s.at[512 * i : 512 * (i + 1)], m.at[:, 256:])
+            for i, m in enumerate((m0_hbm, m1_hbm, m2_hbm, keep_hbm))
+        ],
+        sem,
+    )
+    for copy in pairs:
+        copy.wait()
+
+
 def summed(keep_ref, got_refs, rows):
     total = keep_ref[rows].astype(F32)
     for got in got_refs:
@@ -326,23 +365,23 @@
 def summed_table(table_in, got_refs, n):
     total = table_in[...]
     for got in got_refs:
-        total += table_of(got[n:, :384])
+        total += table_of(got[n:, :256])
     return total
 
 
 def merge_kernel(
     keep_ref, a0, a1, a2, keep2_ref, b0, b1, b2, table_in, m0_ref, m1_ref, m2_ref, next_ref, table_ref
 ):
-    total = summed_table(table_in, (b0, b1, b2), 512)
+    total = summed_table(table_in, (a0, a1, a2), 512)
     table_ref[...] = total
     parts = three_parts(total)
     for i, out in enumerate((m0_ref, m1_ref, m2_ref, next_ref)):
         rows = slice(128 * i, 128 * (i + 1))
-        out[:128, :384] = summed(keep_ref, (a0, a1, a2), rows).astype(BF16)
-        out[:128, 384:] = summed(keep2_ref, (b0, b1, b2), rows).astype(BF16)
+        out[:128, :256] = summed(keep_ref, (a0, a1, a2), rows).astype(BF16)
+        out[:128, 256:] = summed(keep2_ref, (b0, b1, b2), rows).astype(BF16)
         if i < 3:
-            out[128:, :384] = parts
-            out[128:, 384:] = jnp.zeros((EXTRA, 384), BF16)
+            out[128:, :256] = parts
+            out[128:, 256:] = jnp.zeros((EXTRA, 512), BF16)
 
 
 def split_kernel(keep_ref, g0, g1, g2, table_in, one_ref, two_ref, three_ref, own_ref, table_ref):
@@ -350,35 +389,34 @@
     total = summed_table(table_in, (g0, g1, g2), 2 * n)
     table_ref[...] = total
     far = summed(keep_ref, (g0, g1, g2), slice(0, n))
-    one_ref[:n] = far[:, :384].astype(BF16)
-    one_ref[n:] = three_parts(total)
-    two_ref[...] = far[:, 384:].astype(BF16)
+    one_ref[:n] = far[:, :512].astype(BF16)
+    one_ref[n:, :256] = three_parts(total)
+    one_ref[n:, 256:] = jnp.zeros((EXTRA, 256), BF16)
+    two_ref[...] = far[:, 512:].astype(BF16)
     near = summed(keep_ref, (g0, g1, g2), slice(n, 2 * n))
-    own_ref[...] = near[:, :384]
-    three_ref[...] = near[:, 384:]
+    own_ref[...] = near[:, :512]
+    three_ref[...] = near[:, 512:]
 
 
 def output_kernel(own_ref, one_ref, two_ref, three_ref, table_in, q_ref, k_ref, v_ref, table_ref):
     core = lax.axis_index("core")
     n = own_ref.shape[0]
-    table = table_in[...] + table_of(one_ref[n:])
-    table_ref[...] = table[:, : table_ref.shape[1]]
+    table = table_in[...] + table_of(one_ref[n:, :256])
+    table_ref[:, :256] = table[:2]
+    table_ref[:, 256:] = table[2:, :1]
     own = own_ref[...] + one_ref[:n].astype(F32)
     got = three_ref[...] + two_ref[...].astype(F32)
+    q_ref[...] = own[:, :256]
 
     @pl.when(core == 0)
     def _():
-        k_ref[...] = own[:, :256]
-        v_ref[...] = got[:, :256]
-        q_ref[:, :128] = own[:, 256:]
-        q_ref[:, 128:] = got[:, 256:]
+        k_ref[...] = own[:, 256:]
+        v_ref[...] = got
 
     @pl.when(core == 1)
     def _():
-        v_ref[...] = own[:, :256]
-        k_ref[...] = got[:, :256]
-        q_ref[:, 128:] = own[:, 256:]
-        q_ref[:, :128] = got[:, 256:]
+        v_ref[...] = own[:, 256:]
+        k_ref[...] = got
 
 
 def sds(shape, dtype):
@@ -437,44 +475,51 @@
         flops=2 * 1024 * 2048 * 768,
     )
     block = (REACH, 256)
-    dq0, edge, back, bias, pat = call(
-        first_kernel, (query, key, value, halo, out_grad, rel_table),
-        (b16(REACH, 256), f32(REACH, 512), b16(REACH, 512), f32(2, BAND, TILE), f32(2, BAND, TILE)),
+    span = 1024 - LATE
+    pattern = f32(2, BAND, TILE)
+    dq_late, acc, bias, pat = call(
+        late_kernel, (query, key, value, out_grad, rel_table),
+        (b16(384, 256), f32(span, 512), pattern, pattern),
+        (v16(256, span), v16(256, span), v32(span, 256), v32(span, 256)), flops=6 * tile_flops,
+    )
+    dq0, edge, back, pat = call(
+        first_kernel, (query, key, value, halo, out_grad, bias, pat),
+        (b16(REACH, 256), f32(REACH, 512), b16(REACH, 512), pattern),
         (v16(512, 256), v16(512, 256), v16(256, 512), v16(256, 512), v32(512, 256), v32(512, 256)),
         flops=4 * tile_flops, blocks={0: block, 1: block, 2: block, 4: block},
     )
     back = neighbour(back, -1)
     dq, near, kg, vg, edge, pat = call(
-        attn_kernel, (query, key, value, out_grad, bias, pat, edge, dq0),
-        (b16(1024, 256), b16(1024, 256), b16(768, 256), b16(768, 256), f32(REACH, 512), f32(2, BAND, TILE)),
-        (v16(256, 1024), v16(256, 1024), v32(1024, 256), v32(1024, 256)),
-        flops=12 * tile_flops,
-    )
-    kg, vg, own, swap = call(finish_kernel, (kg, vg, edge, back, near), (b16(1024, 256),) * 2 + (b16(1024, 384),) * 2)
+        attn_kernel, (query, key, value, out_grad, bias, pat, edge, acc, dq0, dq_late),
+        (b16(1024, 256), b16(1024, 256), b16(768, 256), b16(768, 256), f32(REACH, 512), pattern),
+        (v16(256, 640), v16(256, 640), v32(640, 256), v32(640, 256)), flops=6 * tile_flops,
+    )
+    product = 2 * 1024 * 2048 * 256
+    dma = pltpu.SemaphoreType.DMA
+    *send, keep, table = call(
+        query_kernel, (x, near, pat), (b16(512 + EXTRA, 256),) * 3 + (b16(512, 256), f32(4, 256)),
+        (v16(2048, 256), v16(EXTRA, 256), v32(8, 640), dma((7,))), flops=product, any_outs=(0, 1, 2, 3),
+    )
+    a = exchange_quarters(send, 0)
+    kg, vg, own, swap = call(finish_kernel, (kg, vg, edge, back), (b16(1024, 256),) * 4)
     got = core_swap(swap)
-    product = 2 * 1024 * 2048 * 384
-    *send, keep = call(
-        own_kernel, (x, own), (b16(512, 384),) * 4,
-        (v16(2048, 384), pltpu.SemaphoreType.DMA((4,))), flops=product, any_outs=(0, 1, 2, 3),
-    )
-    *send2, keep2, table = call(
-        other_kernel, (x, got, pat), (b16(512 + EXTRA, 384),) * 3 + (b16(512, 384), f32(2, 384)),
-        (v16(2048, 384), v16(EXTRA, 384), v32(8, 640), pltpu.SemaphoreType.DMA((7,))),
-        flops=product, any_outs=(0, 1, 2, 3),
-    )
-    a = exchange_quarters(send, OWN, 0)
-    b = exchange_quarters(send2, OTHER, 0)
+    (placed,) = call(own_kernel, (x, own), (b16(2048, 256),), flops=product)
+    *send2, keep2 = call(
+        other_kernel, (x, got, placed), (b16(512, 512),) * 4,
+        (v16(2048, 256), dma((4,)), dma((4,))), flops=product, any_outs=(0, 1, 2, 3), any_ins=(2,),
+    )
+    b = exchange_quarters(send2, 0)
     *send, keep, table = call(
         merge_kernel, (keep, *a, keep2, *b, table),
-        (b16(128 + EXTRA, 768),) * 3 + (b16(128, 768), f32(2, 384)),
-    )
-    c = exchange_quarters(send, OWN, 2)
+        (b16(128 + EXTRA, 768),) * 3 + (b16(128, 768), f32(4, 256)),
+    )
+    c = exchange_quarters(send, 2)
     one, two, three, own, table = call(
         split_kernel, (keep, *c, table),
-        (b16(64 + EXTRA, 384), b16(64, 384), f32(64, 384), f32(64, 384), f32(2, 384)),
-    )
-    one = exchange(one, OWN, (4,))
-    two = exchange(two, OWN, (4,), across=1)
+        (b16(64 + EXTRA, 512), b16(64, 256), f32(64, 256), f32(64, 512), f32(4, 256)),
+    )
+    one = exchange(one, (4,))
+    two = exchange(two, (4,), across=1)
     three = core_swap(three)
     dwq, dwk, dwv, table = call(
         output_kernel, (own, one, two, three, table), (f32(64, 256),) * 3 + (f32(*rel_table.shape),)

time: 84.1 us -> 81.5 us (0.969)
  the two profiles are of different devices: /device:TPU:8 before, /device:TPU:11 now
where the time goes in v3:
time: 81.5 us; the launch traced here: 81.4 us
  starting transfers between devices  31 us (38%)
  waiting for transfers between devices  25.9 us (32%)
  Pallas kernels  23.7 us (29%)
    pallas_call x12, Pallas kernels, call(): pl.pallas_call(kernel, grid=grid, in_specs=specs, out_specs=out_specs, ou...  23.7 us
    ppermute x11, waiting for transfers between devices, exchange(): return lax.ppermute(block, SP + ('core',), level_route(steps, across))  23.5 us
    ppermute x11, starting transfers between devices, exchange(): return lax.ppermute(block, SP + ('core',), level_route(steps, across))  18 us
    ppermute x2, starting transfers between devices, core_swap(): return lax.ppermute(block, 'core', [(0, 1), (1, 0)])  7.67 us
    ppermute x2, starting transfers between devices, neighbour(): return lax.ppermute(block, SP, route)  5.29 us
    ppermute x2, waiting for transfers between devices, neighbour(): return lax.ppermute(block, SP, route)  2.36 us
  transfers between devices with their start and end apart: 15, of which 6 were waited for; matrix products, arithmetic and copies ran while one was open for 0% of the time, Pallas kernels for 19%

profile of v3, /device:TPU:11, one launch (start us, length us, event | category | flops | bytes accessed | tf_op | source)
XLA Modules:
  0.0 81.4 jit_solution(13918603627840506983)
XLA Ops:
  0.6 3.2 %shard_map.117 = (bf16[256,512]{1,0:T(8,128)(2,1)S(1)}, bf16[1024,2048]{1,0:T(8,128)(2,1)S(1)}, bf16[2048,256]{1,0:T(8,128)(2,1)S(1)}, bf16[2048,256]{1,0:T(8,128)(2,1)S(1)}, bf16[2048,256]{1,0:T(8,128)(2,1)S(1)}) custom-call(bf16[1024,2048]{1,0:T(8,128)(2,1)} %x_hbm.1, bf16[2048,256]{1,0:T(8,128)(2,1)} %wq_hbm.1, bf16[2048,256]{1,0:T(8,128)(2,1)} %wk_hbm.1, ...), custom_call_target="tpu_custom_call" | custom-call | flops 536870912 | bytes 14942208 | tf_op jit(solution)/shard_map/pallas_call | solution.py:444
  3.9 3.1 %collective-permute-start = (bf16[256,512]{1,0:T(8,128)(2,1)S(1)}, bf16[256,512]{1,0:T(8,128)(2,1)S(1)}, u32[]{:S(2)}, u32[]{:S(2)}) collective-permute-start(bf16[256,512]{1,0:T(8,128)(2,1)S(1)} %get-tuple-element.64), channel_id=1, source_target_pairs={{0,8},{8,16},{16,24},{24,32},{32,40},{40,48},{48,56},{56,64},{64,7... | collective-permute-start | bytes 786440 | tf_op jit(solution)/shard_map/ppermute | solution.py:459
  7.0 0.0 copy-start
  7.0 0.0 copy-start.1
  7.0 3.4 %shard_map.118 = (bf16[1024,256]{1,0:T(8,128)(2,1)S(1)}, bf16[1024,256]{1,0:T(8,128)(2,1)S(1)}, bf16[1024,256]{1,0:T(8,128)(2,1)S(1)}) custom-call(bf16[1024,2048]{1,0:T(8,128)(2,1)S(1)} %get-tuple-element.56.x_ref, bf16[2048,256]{1,0:T(8,128)(2,1)S(1)} %get-tuple-element.57.wq_ref, bf16[2048,256]{1,0:T(8,128)(2,1)S(1)} %get-tuple-element.58.wk_ref, ...), custom_call_target="tpu_custom_call" | custom-call | flops 3221225472 | bytes 8912896 | tf_op jit(solution)/shard_map/pallas_call | solution.py:444
  10.4 0.0 copy-done
  10.5 0.0 copy-done.1
  10.5 3.4 %shard_map.119 = (bf16[384,256]{1,0:T(8,128)(2,1)S(1)}, f32[640,512]{1,0:T(8,128)S(1)}, f32[2,384,128]{2,1,0:T(8,128)S(1)}, f32[2,384,128]{2,1,0:T(8,128)S(1)}) custom-call(bf16[1024,256]{1,0:T(8,128)(2,1)S(1)} %get-tuple-element.60.q_ref, bf16[1024,256]{1,0:T(8,128)(2,1)S(1)} %get-tuple-element.61.k_ref, bf16[1024,256]{1,0:T(8,128)(2,1)S(1)} %get-tuple-element.62.v_ref, ...), custom_call_target="tpu_custom_call" | custom-call | flops 452984832 | bytes 4392968 | tf_op jit(solution)/shard_map/pallas_call | solution.py:444
  13.8 0.0 collective-permute-done.halo_ref
  13.9 2.3 %shard_map.120 = (bf16[256,256]{1,0:T(8,128)(2,1)S(1)}, f32[256,512]{1,0:T(8,128)S(1)}, bf16[256,512]{1,0:T(8,128)(2,1)S(1)}, f32[2,384,128]{2,1,0:T(8,128)S(1)}) custom-call(bf16[1024,256]{1,0:T(8,128)(2,1)S(1)} %get-tuple-element.60.q_ref, bf16[1024,256]{1,0:T(8,128)(2,1)S(1)} %get-tuple-element.61.k_ref, bf16[1024,256]{1,0:T(8,128)(2,1)S(1)} %get-tuple-element.62.v_ref, ...), custom_call_target="tpu_custom_call" | custom-call | flops 301989888 | bytes 4456448 | tf_op jit(solution)/shard_map/pallas_call | solution.py:444
  16.2 2.2 %collective-permute-start.1 = (bf16[256,512]{1,0:T(8,128)(2,1)S(1)}, bf16[256,512]{1,0:T(8,128)(2,1)S(1)}, u32[]{:S(2)}, u32[]{:S(2)}) collective-permute-start(bf16[256,512]{1,0:T(8,128)(2,1)S(1)} %get-tuple-element.75), channel_id=1, source_target_pairs={{8,0},{16,8},{24,16},{32,24},{40,32},{48,40},{56,48},{64,56},{72,6... | collective-permute-start | bytes 786440 | tf_op jit(solution)/shard_map/ppermute | solution.py:459
  18.4 4.3 %shard_map.121 = (bf16[1024,256]{1,0:T(8,128)(2,1)}, bf16[1024,256]{1,0:T(8,128)(2,1)S(1)}, bf16[768,256]{1,0:T(8,128)(2,1)S(1)}, bf16[768,256]{1,0:T(8,128)(2,1...) custom-call(bf16[1024,256]{1,0:T(8,128)(2,1)S(1)} %get-tuple-element.60.q_ref, ...), custom_call_target="tpu_custom_call" | custom-call | flops 452984832 | bytes 7798784 | tf_op jit(solution)/shard_map/pallas_call | solution.py:444
  22.6 2.4 %collective-permute-done.1.back_ref = bf16[256,512]{1,0:T(8,128)(2,1)S(1)} collective-permute-done((bf16[256,512]{1,0:T(8,128)(2,1)S(1)}, bf16[256,512]{1,0:T(8,128)(2,1)S(1)}, u32[]{:S(2)}, u32[]{:S(2)}) %collective-permute-start.1) | collective-permute-done | bytes 262176 | tf_op jit(solution)/shard_map/ppermute | solution.py:459
  25.0 1.1 %shard_map.122 = (bf16[1024,256]{1,0:T(8,128)(2,1)}, bf16[1024,256]{1,0:T(8,128)(2,1)}, bf16[1024,256]{1,0:T(8,128)(2,1)S(1)}, bf16[1024,256]{1,0:T(8,128)(2,1)S(1)}) custom-call(bf16[768,256]{1,0:T(8,128)(2,1)S(1)} %get-tuple-element.72.kg_in, bf16[768,256]{1,0:T(8,128)(2,1)S(1)} %get-tuple-element.73.vg_in, f32[256,512]{1,0:T(8,128)S(1)} %get-tuple-element.74.edge_ref, ...), custom_call_target="tpu_custom_call" | custom-call | flops 1048576 | bytes 3670016 | tf_op jit(solution)/shard_map/pallas_call | solution.py:444
  26.1 1.8 %collective-permute-start.5 = (bf16[1024,256]{1,0:T(8,128)(2,1)S(1)}, bf16[1024,256]{1,0:T(8,128)(2,1)S(1)}, u32[]{:S(2)}, u32[]{:S(2)}) collective-permute-start(bf16[1024,256]{1,0:T(8,128)(2,1)S(1)} %get-tuple-element.84), channel_id=1, source_target_pairs={{0,1},{1,0},{2,3},{3,2},{4,5},{5,4},{6,7},{7,6},{8,9},{9,8},{10,11... | collective-permute-start | bytes 1572872 | tf_op jit(solution)/shard_map/ppermute | solution.py:106
  27.9 1.9 %shard_map.123 = (bf16[528,256]{1,0:T(8,128)(2,1)S(1)}, bf16[528,256]{1,0:T(8,128)(2,1)S(1)}, bf16[528,256]{1,0:T(8,128)(2,1)S(1)}, bf16[512,256]{1,0:T(8,128)(2,1)S(1)}, f32[4,256]{1,0:T(4,128)S(1)}) custom-call(bf16[1024,2048]{1,0:T(8,128)(2,1)S(1)} %get-tuple-element.56.x_ref, bf16[1024,256]{1,0:T(8,128)(2,1)S(1)} %get-tuple-element.78.grad_ref, ...), custom_call_target="tpu_custom_call" | custom-call | flops 1073741824 | bytes 6189056 | tf_op jit(solution)/shard_map/pallas_call | solution.py:444
  29.8 3.3 %collective-permute-start.2 = (bf16[528,256]{1,0:T(8,128)(2,1)S(1)}, bf16[528,256]{1,0:T(8,128)(2,1)S(1)}, u32[]{:S(2)}, u32[]{:S(2)}) collective-permute-start(bf16[528,256]{1,0:T(8,128)(2,1)S(1)} %get-tuple-element.81), channel_id=1, source_target_pairs={{0,16},{8,24},{16,0},{24,8},{32,48},{40,56},{48,32},{56,40},{64,80... | collective-permute-start | bytes 811016 | tf_op jit(solution)/shard_map/ppermute | solution.py:97
  33.1 1.3 %shard_map.124.own_hbm = bf16[2048,256]{1,0:T(8,128)(2,1)S(1)} custom-call(bf16[1024,2048]{1,0:T(8,128)(2,1)S(1)} %get-tuple-element.56.x_ref, bf16[1024,256]{1,0:T(8,128)(2,1)S(1)} %get-tuple-element.85.grad_ref), custom_call_target="tpu_custom_call" | custom-call | flops 1073741824 | bytes 5767168 | tf_op jit(solution)/shard_map/pallas_call | solution.py:444
  34.4 0.0 collective-permute-done.5.grad_ref
  34.4 1.6 %shard_map.125 = (bf16[512,512]{1,0:T(8,128)(2,1)S(1)}, bf16[512,512]{1,0:T(8,128)(2,1)S(1)}, bf16[512,512]{1,0:T(8,128)(2,1)S(1)}, bf16[512,512]{1,0:T(8,128)(2,1)S(1)}) custom-call(bf16[1024,2048]{1,0:T(8,128)(2,1)S(1)} %get-tuple-element.56.x_ref, bf16[1024,256]{1,0:T(8,128)(2,1)S(1)} %collective-permute-done.5.grad_ref, ...), custom_call_target="tpu_custom_call" | custom-call | flops 1073741824 | bytes 7864320 | tf_op jit(solution)/shard_map/pallas_call | solution.py:444
  36.0 4.7 %collective-permute-start.6 = (bf16[512,512]{1,0:T(8,128)(2,1)S(1)}, bf16[512,512]{1,0:T(8,128)(2,1)S(1)}, u32[]{:S(2)}, u32[]{:S(2)}) collective-permute-start(bf16[512,512]{1,0:T(8,128)(2,1)S(1)} %get-tuple-element.87), channel_id=1, source_target_pairs={{0,16},{8,24},{16,0},{24,8},{32,48},{40,56},{48,32},{56,40},{64,80... | collective-permute-start | bytes 1572872 | tf_op jit(solution)/shard_map/ppermute | solution.py:97
  40.7 0.3 collective-permute-start.7
  41.0 0.0 collective-permute-start.8
  41.0 1.5 %collective-permute-start.3 = (bf16[528,256]{1,0:T(8,128)(2,1)S(1)}, bf16[528,256]{1,0:T(8,128)(2,1)S(1)}, u32[]{:S(2)}, u32[]{:S(2)}) collective-permute-start(bf16[528,256]{1,0:T(8,128)(2,1)S(1)} %get-tuple-element.82), channel_id=1, source_target_pairs={{0,8},{8,0},{16,24},{24,16},{32,40},{40,32},{48,56},{56,48},{64,72... | collective-permute-start | bytes 811016 | tf_op jit(solution)/shard_map/ppermute | solution.py:97
  42.5 0.0 collective-permute-done.2.a0
  42.5 1.2 %collective-permute-start.4 = (bf16[528,256]{1,0:T(8,128)(2,1)S(1)}, bf16[528,256]{1,0:T(8,128)(2,1)S(1)}, u32[]{:S(2)}, u32[]{:S(2)}) collective-permute-start(bf16[528,256]{1,0:T(8,128)(2,1)S(1)} %get-tuple-element.83), channel_id=1, source_target_pairs={{0,24},{8,16},{16,8},{24,0},{32,56},{40,48},{48,40},{56,32},{64,88... | collective-permute-start | bytes 811016 | tf_op jit(solution)/shard_map/ppermute | solution.py:97
  43.7 12.7 %collective-permute-done.3.a1 = bf16[528,256]{1,0:T(8,128)(2,1)S(1)} collective-permute-done((bf16[528,256]{1,0:T(8,128)(2,1)S(1)}, bf16[528,256]{1,0:T(8,128)(2,1)S(1)}, u32[]{:S(2)}, u32[]{:S(2)}) %collective-permute-start.3) | collective-permute-done | bytes 270368 | tf_op jit(solution)/shard_map/ppermute | solution.py:97
  56.4 0.0 collective-permute-done.4.a2
  56.4 0.0 collective-permute-done.6.b0
  56.4 0.0 collective-permute-done.7.b1
  56.4 0.0 collective-permute-done.8.b2
  56.5 0.4 shard_map.126
  56.9 3.2 %collective-permute-start.9 = (bf16[144,768]{1,0:T(8,128)(2,1)S(1)}, bf16[144,768]{1,0:T(8,128)(2,1)S(1)}, u32[]{:S(2)}, u32[]{:S(2)}) collective-permute-start(bf16[144,768]{1,0:T(8,128)(2,1)S(1)} %get-tuple-element.92), channel_id=1, source_target_pairs={{0,64},{8,72},{16,80},{24,88},{32,224},{40,232},{48,240},{56,248},... | collective-permute-start | bytes 663560 | tf_op jit(solution)/shard_map/ppermute | solution.py:97
  60.0 0.0 collective-permute-start.10
  60.0 0.4 collective-permute-start.11
  60.4 3.0 %collective-permute-done.9.g0 = bf16[144,768]{1,0:T(8,128)(2,1)S(1)} collective-permute-done((bf16[144,768]{1,0:T(8,128)(2,1)S(1)}, bf16[144,768]{1,0:T(8,128)(2,1)S(1)}, u32[]{:S(2)}, u32[]{:S(2)}) %collective-permute-start.9) | collective-permute-done | bytes 221216 | tf_op jit(solution)/shard_map/ppermute | solution.py:97
  63.5 1.9 %collective-permute-done.10.g1 = bf16[144,768]{1,0:T(8,128)(2,1)S(1)} collective-permute-done((bf16[144,768]{1,0:T(8,128)(2,1)S(1)}, bf16[144,768]{1,0:T(8,128)(2,1)S(1)}, u32[]{:S(2)}, u32[]{:S(2)}) %collective-permute-start.10) | collective-permute-done | bytes 221216 | tf_op jit(solution)/shard_map/ppermute | solution.py:97
  65.3 0.7 collective-permute-done.11.g2
  66.0 0.1 shard_map.127
  66.1 3.5 %collective-permute-start.12 = (bf16[80,512]{1,0:T(8,128)(2,1)S(1)}, bf16[80,512]{1,0:T(8,128)(2,1)S(1)}, u32[]{:S(2)}, u32[]{:S(2)}) collective-permute-start(bf16[80,512]{1,0:T(8,128)(2,1)S(1)} %get-tuple-element.97), channel_id=1, source_target_pairs={{0,96},{8,104},{16,112},{24,120},{32,192},{40,200},{48,208},{56,21... | collective-permute-start | bytes 245768 | tf_op jit(solution)/shard_map/ppermute | solution.py:97
  69.7 5.9 %collective-permute-start.14 = (f32[64,256]{1,0:T(8,128)S(1)}, f32[64,256]{1,0:T(8,128)S(1)}, u32[]{:S(2)}, u32[]{:S(2)}) collective-permute-start(f32[64,256]{1,0:T(8,128)S(1)} %get-tuple-element.99), channel_id=1, source_target_pairs={{0,1},{1,0},{2,3},{3,2},{4,5},{5,4},{6,7},{7,6},{8,9},{9,8},{10,11... | collective-permute-start | bytes 196616 | tf_op jit(solution)/shard_map/ppermute | solution.py:106
  75.5 0.0 collective-permute-start.13
  75.5 5.2 %collective-permute-done.13.two_ref = bf16[64,256]{1,0:T(8,128)(2,1)S(1)} collective-permute-done((bf16[64,256]{1,0:T(8,128)(2,1)S(1)}, bf16[64,256]{1,0:T(8,128)(2,1)S(1)}, u32[]{:S(2)}, u32[]{:S(2)}) %collective-permute-start.13) | collective-permute-done | bytes 32800 | tf_op jit(solution)/shard_map/ppermute | solution.py:97
  80.7 0.0 collective-permute-done.14.three_ref
  80.7 0.0 collective-permute-done.12.one_ref
  80.7 0.7 shard_map.128
Async XLA Ops:
  3.9 10.0 %collective-permute-start = (bf16[256,512]{1,0:T(8,128)(2,1)S(1)}, bf16[256,512]{1,0:T(8,128)(2,1)S(1)}, u32[]{:S(2)}, u32[]{:S(2)}) collective-permute-start(bf16[256,512]{1,0:T(8,128)(2,1)S(1)} %get-tuple-element.64), channel_id=1, source_target_pairs={{0,8},{8,16},{16,24},{24,32},{32,40},{40,48},{48,56},{56,64},{64,7... | collective-permute-start | bytes 786440 | tf_op jit(solution)/shard_map/ppermute | solution.py:459
  7.0 3.5 %copy-start = (bf16[1024,256]{1,0:T(8,128)(2,1)S(1)}, bf16[1024,256]{1,0:T(8,128)(2,1)}, u32[]{:S(2)}) copy-start(bf16[1024,256]{1,0:T(8,128)(2,1)} %og_ref.5) | copy-start | bytes 1572868
  7.0 3.5 %copy-start.1 = (f32[2,257]{1,0:T(2,128)S(1)}, f32[2,257]{1,0:T(2,128)}, u32[]{:S(2)}) copy-start(f32[2,257]{1,0:T(2,128)} %rel_ref.1) | copy-start | bytes 6172
  16.2 8.8 %collective-permute-start.1 = (bf16[256,512]{1,0:T(8,128)(2,1)S(1)}, bf16[256,512]{1,0:T(8,128)(2,1)S(1)}, u32[]{:S(2)}, u32[]{:S(2)}) collective-permute-start(bf16[256,512]{1,0:T(8,128)(2,1)S(1)} %get-tuple-element.75), channel_id=1, source_target_pairs={{8,0},{16,8},{24,16},{32,24},{40,32},{48,40},{56,48},{64,56},{72,6... | collective-permute-start | bytes 786440 | tf_op jit(solution)/shard_map/ppermute | solution.py:459
  26.1 8.3 %collective-permute-start.5 = (bf16[1024,256]{1,0:T(8,128)(2,1)S(1)}, bf16[1024,256]{1,0:T(8,128)(2,1)S(1)}, u32[]{:S(2)}, u32[]{:S(2)}) collective-permute-start(bf16[1024,256]{1,0:T(8,128)(2,1)S(1)} %get-tuple-element.84), channel_id=1, source_target_pairs={{0,1},{1,0},{2,3},{3,2},{4,5},{5,4},{6,7},{7,6},{8,9},{9,8},{10,11... | collective-permute-start | bytes 1572872 | tf_op jit(solution)/shard_map/ppermute | solution.py:106
  29.8 12.7 %collective-permute-start.2 = (bf16[528,256]{1,0:T(8,128)(2,1)S(1)}, bf16[528,256]{1,0:T(8,128)(2,1)S(1)}, u32[]{:S(2)}, u32[]{:S(2)}) collective-permute-start(bf16[528,256]{1,0:T(8,128)(2,1)S(1)} %get-tuple-element.81), channel_id=1, source_target_pairs={{0,16},{8,24},{16,0},{24,8},{32,48},{40,56},{48,32},{56,40},{64,80... | collective-permute-start | bytes 811016 | tf_op jit(solution)/shard_map/ppermute | solution.py:97
  36.0 20.4 %collective-permute-start.6 = (bf16[512,512]{1,0:T(8,128)(2,1)S(1)}, bf16[512,512]{1,0:T(8,128)(2,1)S(1)}, u32[]{:S(2)}, u32[]{:S(2)}) collective-permute-start(bf16[512,512]{1,0:T(8,128)(2,1)S(1)} %get-tuple-element.87), channel_id=1, source_target_pairs={{0,16},{8,24},{16,0},{24,8},{32,48},{40,56},{48,32},{56,40},{64,80... | collective-permute-start | bytes 1572872 | tf_op jit(solution)/shard_map/ppermute | solution.py:97
  40.7 15.7 %collective-permute-start.7 = (bf16[512,512]{1,0:T(8,128)(2,1)S(1)}, bf16[512,512]{1,0:T(8,128)(2,1)S(1)}, u32[]{:S(2)}, u32[]{:S(2)}) collective-permute-start(bf16[512,512]{1,0:T(8,128)(2,1)S(1)} %get-tuple-element.88), channel_id=1, source_target_pairs={{0,8},{8,0},{16,24},{24,16},{32,40},{40,32},{48,56},{56,48},{64,72... | collective-permute-start | bytes 1572872 | tf_op jit(solution)/shard_map/ppermute | solution.py:97
  41.0 15.4 %collective-permute-start.8 = (bf16[512,512]{1,0:T(8,128)(2,1)S(1)}, bf16[512,512]{1,0:T(8,128)(2,1)S(1)}, u32[]{:S(2)}, u32[]{:S(2)}) collective-permute-start(bf16[512,512]{1,0:T(8,128)(2,1)S(1)} %get-tuple-element.89), channel_id=1, source_target_pairs={{0,24},{8,16},{16,8},{24,0},{32,56},{40,48},{48,40},{56,32},{64,88... | collective-permute-start | bytes 1572872 | tf_op jit(solution)/shard_map/ppermute | solution.py:97
  41.0 15.4 %collective-permute-start.3 = (bf16[528,256]{1,0:T(8,128)(2,1)S(1)}, bf16[528,256]{1,0:T(8,128)(2,1)S(1)}, u32[]{:S(2)}, u32[]{:S(2)}) collective-permute-start(bf16[528,256]{1,0:T(8,128)(2,1)S(1)} %get-tuple-element.82), channel_id=1, source_target_pairs={{0,8},{8,0},{16,24},{24,16},{32,40},{40,32},{48,56},{56,48},{64,72... | collective-permute-start | bytes 811016 | tf_op jit(solution)/shard_map/ppermute | solution.py:97
  42.5 13.9 %collective-permute-start.4 = (bf16[528,256]{1,0:T(8,128)(2,1)S(1)}, bf16[528,256]{1,0:T(8,128)(2,1)S(1)}, u32[]{:S(2)}, u32[]{:S(2)}) collective-permute-start(bf16[528,256]{1,0:T(8,128)(2,1)S(1)} %get-tuple-element.83), channel_id=1, source_target_pairs={{0,24},{8,16},{16,8},{24,0},{32,56},{40,48},{48,40},{56,32},{64,88... | collective-permute-start | bytes 811016 | tf_op jit(solution)/shard_map/ppermute | solution.py:97
  56.9 6.6 %collective-permute-start.9 = (bf16[144,768]{1,0:T(8,128)(2,1)S(1)}, bf16[144,768]{1,0:T(8,128)(2,1)S(1)}, u32[]{:S(2)}, u32[]{:S(2)}) collective-permute-start(bf16[144,768]{1,0:T(8,128)(2,1)S(1)} %get-tuple-element.92), channel_id=1, source_target_pairs={{0,64},{8,72},{16,80},{24,88},{32,224},{40,232},{48,240},{56,248},... | collective-permute-start | bytes 663560 | tf_op jit(solution)/shard_map/ppermute | solution.py:97
  60.0 5.3 %collective-permute-start.10 = (bf16[144,768]{1,0:T(8,128)(2,1)S(1)}, bf16[144,768]{1,0:T(8,128)(2,1)S(1)}, u32[]{:S(2)}, u32[]{:S(2)}) collective-permute-start(bf16[144,768]{1,0:T(8,128)(2,1)S(1)} %get-tuple-element.93), channel_id=1, source_target_pairs={{0,32},{8,40},{16,48},{24,56},{32,0},{40,8},{48,16},{56,24},{64,96... | collective-permute-start | bytes 663560 | tf_op jit(solution)/shard_map/ppermute | solution.py:97
  60.0 6.0 %collective-permute-start.11 = (bf16[144,768]{1,0:T(8,128)(2,1)S(1)}, bf16[144,768]{1,0:T(8,128)(2,1)S(1)}, u32[]{:S(2)}, u32[]{:S(2)}) collective-permute-start(bf16[144,768]{1,0:T(8,128)(2,1)S(1)} %get-tuple-element.94), channel_id=1, source_target_pairs={{0,224},{8,232},{16,240},{24,248},{32,64},{40,72},{48,80},{56,88},... | collective-permute-start | bytes 663560 | tf_op jit(solution)/shard_map/ppermute | solution.py:97
  66.1 14.5 %collective-permute-start.12 = (bf16[80,512]{1,0:T(8,128)(2,1)S(1)}, bf16[80,512]{1,0:T(8,128)(2,1)S(1)}, u32[]{:S(2)}, u32[]{:S(2)}) collective-permute-start(bf16[80,512]{1,0:T(8,128)(2,1)S(1)} %get-tuple-element.97), channel_id=1, source_target_pairs={{0,96},{8,104},{16,112},{24,120},{32,192},{40,200},{48,208},{56,21... | collective-permute-start | bytes 245768 | tf_op jit(solution)/shard_map/ppermute | solution.py:97
  69.7 11.0 %collective-permute-start.14 = (f32[64,256]{1,0:T(8,128)S(1)}, f32[64,256]{1,0:T(8,128)S(1)}, u32[]{:S(2)}, u32[]{:S(2)}) collective-permute-start(f32[64,256]{1,0:T(8,128)S(1)} %get-tuple-element.99), channel_id=1, source_target_pairs={{0,1},{1,0},{2,3},{3,2},{4,5},{5,4},{6,7},{7,6},{8,9},{9,8},{10,11... | collective-permute-start | bytes 196616 | tf_op jit(solution)/shard_map/ppermute | solution.py:106
  75.5 5.2 %collective-permute-start.13 = (bf16[64,256]{1,0:T(8,128)(2,1)S(1)}, bf16[64,256]{1,0:T(8,128)(2,1)S(1)}, u32[]{:S(2)}, u32[]{:S(2)}) collective-permute-start(bf16[64,256]{1,0:T(8,128)(2,1)S(1)} %get-tuple-element.98), channel_id=1, source_target_pairs={{0,97},{8,105},{16,113},{24,121},{32,193},{40,201},{48,209},{56,21... | collective-permute-start | bytes 98312 | tf_op jit(solution)/shard_map/ppermute | solution.py:97

commit v4 on v3

--- a/solution.py
+++ b/solution.py
@@ -38,7 +38,7 @@
 XO, XE = ("sp_1", odd_pair), ("sp_1", even_pair(NX))
 ZO, ZE = ("sp_0", odd_pair), ("sp_0", even_pair(NZ))
 Z3 = ("sp_0", lambda i: (3, 6, 5, 0, 7, 2, 1, 4)[i])
-LEVELS = ((XO, XE, ZO, ZE, Z3), (ZO, ZE, XO, XE, Z3))
+LEVELS = ((ZO, ZE, XO, XE, Z3), (XO, XE, ZO, ZE, Z3))
 
 
 def held_order(steps, device):
@@ -234,7 +234,7 @@
 
 def attn_kernel(
     q_ref, k_ref, v_ref, og_ref, bias_ref, pat_in, edge_in, acc_in, dq_in, dq_late,
-    dq_ref, near_ref, kg_ref, vg_ref, edge_ref, pat_ref,
+    near_ref, kg_ref, vg_ref, edge_ref, pat_ref,
     kt_s, vt_s, ka_s, va_s,
 ):
     kt_s[...] = k_ref[: LATE + REACH].T
@@ -249,7 +249,6 @@
     near_ref[:REACH] = dq_in[...]
     near_ref[LATE + REACH :] = dq_late[...]
     tiles(range(3), q_ref, k_ref, v_ref, og_ref, bias_ref, kt_s, vt_s, pat_ref, near_ref, 0, ka_s, va_s, 0)
-    dq_ref[...] = near_ref[...]
     last = LATE + REACH
     kg_ref[:last] = ka_s[...].astype(BF16)
     vg_ref[:last] = va_s[...].astype(BF16)
@@ -258,22 +257,40 @@
     edge_ref[...] = acc_in[768 - LATE :]
 
 
-def finish_kernel(kg_in, vg_in, edge_ref, back_ref, kg_ref, vg_ref, own_ref, swap_ref):
-    kg_ref[:768] = kg_in[...]
-    vg_ref[:768] = vg_in[...]
-    kg_ref[768:] = (edge_ref[:, :256] + back_ref[:, :256].astype(F32)).astype(BF16)
-    vg_ref[768:] = (edge_ref[:, 256:] + back_ref[:, 256:].astype(F32)).astype(BF16)
+def finish_kernel(kg_in, vg_in, edge_ref, back_ref, own_ref, swap_ref):
     core = lax.axis_index("core")
+    key = (edge_ref[:, :256] + back_ref[:, :256].astype(F32)).astype(BF16)
+    value = (edge_ref[:, 256:] + back_ref[:, 256:].astype(F32)).astype(BF16)
+
+    def put(to_key, to_value):
+        to_key[:768] = kg_in[...]
+        to_value[:768] = vg_in[...]
+        to_key[768:] = key
+        to_value[768:] = value
 
     @pl.when(core == 0)
     def _():
-        own_ref[...] = kg_ref[...]
-        swap_ref[...] = vg_ref[...]
+        put(own_ref, swap_ref)
 
     @pl.when(core == 1)
     def _():
-        own_ref[...] = vg_ref[...]
-        swap_ref[...] = kg_ref[...]
+        put(swap_ref, own_ref)
+
+
+def emit_kernel(dq_in, own_in, swap_in, dq_ref, kg_ref, vg_ref, sem):
+    core = lax.axis_index("core")
+    query = pltpu.make_async_copy(dq_in, dq_ref, sem.at[0])
+    query.start()
+
+    @pl.when(core == 0)
+    def _():
+        copy_out([(own_in, kg_ref), (swap_in, vg_ref)], sem.at[1:])
+
+    @pl.when(core == 1)
+    def _():
+        copy_out([(swap_in, kg_ref), (own_in, vg_ref)], sem.at[1:])
+
+    query.wait()
 
 
 def store_units(value, chunk, places, out_s):
@@ -489,19 +506,19 @@
         flops=4 * tile_flops, blocks={0: block, 1: block, 2: block, 4: block},
     )
     back = neighbour(back, -1)
-    dq, near, kg, vg, edge, pat = call(
+    dq, kg, vg, edge, pat = call(
         attn_kernel, (query, key, value, out_grad, bias, pat, edge, acc, dq0, dq_late),
-        (b16(1024, 256), b16(1024, 256), b16(768, 256), b16(768, 256), f32(REACH, 512), pattern),
+        (b16(1024, 256), b16(768, 256), b16(768, 256), f32(REACH, 512), pattern),
         (v16(256, 640), v16(256, 640), v32(640, 256), v32(640, 256)), flops=6 * tile_flops,
     )
     product = 2 * 1024 * 2048 * 256
     dma = pltpu.SemaphoreType.DMA
     *send, keep, table = call(
-        query_kernel, (x, near, pat), (b16(512 + EXTRA, 256),) * 3 + (b16(512, 256), f32(4, 256)),
+        query_kernel, (x, dq, pat), (b16(512 + EXTRA, 256),) * 3 + (b16(512, 256), f32(4, 256)),
         (v16(2048, 256), v16(EXTRA, 256), v32(8, 640), dma((7,))), flops=product, any_outs=(0, 1, 2, 3),
     )
     a = exchange_quarters(send, 0)
-    kg, vg, own, swap = call(finish_kernel, (kg, vg, edge, back), (b16(1024, 256),) * 4)
+    own, swap = call(finish_kernel, (kg, vg, edge, back), (b16(1024, 256),) * 2)
     got = core_swap(swap)
     (placed,) = call(own_kernel, (x, own), (b16(2048, 256),), flops=product)
     *send2, keep2 = call(
@@ -509,6 +526,10 @@
         (v16(2048, 256), dma((4,)), dma((4,))), flops=product, any_outs=(0, 1, 2, 3), any_ins=(2,),
     )
     b = exchange_quarters(send2, 0)
+    dq, kg, vg = call(
+        emit_kernel, (dq, own, swap), (b16(1024, 256),) * 3, (dma((3,)),),
+        any_ins=(0, 1, 2), any_outs=(0, 1, 2),
+    )
     *send, keep, table = call(
         merge_kernel, (keep, *a, keep2, *b, table),
         (b16(128 + EXTRA, 768),) * 3 + (b16(128, 768), f32(4, 256)),

time: 81.5 us -> 80.3 us (0.985)
  the two profiles are of different devices: /device:TPU:11 before, /device:TPU:8 now
where the time goes in v4:
time: 80.3 us; the launch traced here: 79.1 us
  waiting for transfers between devices  28.6 us (36%)
  starting transfers between devices  26.7 us (33%)
  Pallas kernels  23 us (29%)
    ppermute x11, waiting for transfers between devices, exchange(): return lax.ppermute(block, SP + ('core',), level_route(steps, across))  23.6 us
    pallas_call x13, Pallas kernels, call(): pl.pallas_call(kernel, grid=grid, in_specs=specs, out_specs=out_specs, ou...  23 us
    ppermute x11, starting transfers between devices, exchange(): return lax.ppermute(block, SP + ('core',), level_route(steps, across))  21.9 us
    ppermute x2, waiting for transfers between devices, neighbour(): return lax.ppermute(block, SP, route)  4.97 us
    ppermute x2, starting transfers between devices, neighbour(): return lax.ppermute(block, SP, route)  4.7 us
  transfers between devices with their start and end apart: 15, of which 6 were waited for; matrix products, arithmetic and copies ran while one was open for 0% of the time, Pallas kernels for 20%

profile of v4, /device:TPU:8, one launch (start us, length us, event | category | flops | bytes accessed | tf_op | source)
XLA Modules:
  0.0 79.1 jit_solution(6878101070147433381)
XLA Ops:
  0.6 3.2 %shard_map.117 = (bf16[256,512]{1,0:T(8,128)(2,1)S(1)}, bf16[1024,2048]{1,0:T(8,128)(2,1)S(1)}, bf16[2048,256]{1,0:T(8,128)(2,1)S(1)}, bf16[2048,256]{1,0:T(8,128)(2,1)S(1)}, bf16[2048,256]{1,0:T(8,128)(2,1)S(1)}) custom-call(bf16[1024,2048]{1,0:T(8,128)(2,1)} %x_hbm.1, bf16[2048,256]{1,0:T(8,128)(2,1)} %wq_hbm.1, bf16[2048,256]{1,0:T(8,128)(2,1)} %wk_hbm.1, ...), custom_call_target="tpu_custom_call" | custom-call | flops 536870912 | bytes 14942208 | tf_op jit(solution)/shard_map/pallas_call | solution.py:461
  3.9 3.4 %collective-permute-start = (bf16[256,512]{1,0:T(8,128)(2,1)S(1)}, bf16[256,512]{1,0:T(8,128)(2,1)S(1)}, u32[]{:S(2)}, u32[]{:S(2)}) collective-permute-start(bf16[256,512]{1,0:T(8,128)(2,1)S(1)} %get-tuple-element.64), channel_id=1, source_target_pairs={{0,8},{8,16},{16,24},{24,32},{32,40},{40,48},{48,56},{56,64},{64,7... | collective-permute-start | bytes 786440 | tf_op jit(solution)/shard_map/ppermute | solution.py:476
  7.3 0.0 copy-start
  7.3 0.0 copy-start.1
  7.3 3.4 %shard_map.118 = (bf16[1024,256]{1,0:T(8,128)(2,1)S(1)}, bf16[1024,256]{1,0:T(8,128)(2,1)S(1)}, bf16[1024,256]{1,0:T(8,128)(2,1)S(1)}) custom-call(bf16[1024,2048]{1,0:T(8,128)(2,1)S(1)} %get-tuple-element.56.x_ref, bf16[2048,256]{1,0:T(8,128)(2,1)S(1)} %get-tuple-element.57.wq_ref, bf16[2048,256]{1,0:T(8,128)(2,1)S(1)} %get-tuple-element.58.wk_ref, ...), custom_call_target="tpu_custom_call" | custom-call | flops 3221225472 | bytes 8912896 | tf_op jit(solution)/shard_map/pallas_call | solution.py:461
  10.7 0.0 copy-done
  10.7 0.0 copy-done.1
  10.8 3.4 %shard_map.119 = (bf16[384,256]{1,0:T(8,128)(2,1)S(1)}, f32[640,512]{1,0:T(8,128)S(1)}, f32[2,384,128]{2,1,0:T(8,128)S(1)}, f32[2,384,128]{2,1,0:T(8,128)S(1)}) custom-call(bf16[1024,256]{1,0:T(8,128)(2,1)S(1)} %get-tuple-element.60.q_ref, bf16[1024,256]{1,0:T(8,128)(2,1)S(1)} %get-tuple-element.61.k_ref, bf16[1024,256]{1,0:T(8,128)(2,1)S(1)} %get-tuple-element.62.v_ref, ...), custom_call_target="tpu_custom_call" | custom-call | flops 452984832 | bytes 4392968 | tf_op jit(solution)/shard_map/pallas_call | solution.py:461
  14.1 0.0 collective-permute-done.halo_ref
  14.2 2.3 %shard_map.120 = (bf16[256,256]{1,0:T(8,128)(2,1)S(1)}, f32[256,512]{1,0:T(8,128)S(1)}, bf16[256,512]{1,0:T(8,128)(2,1)S(1)}, f32[2,384,128]{2,1,0:T(8,128)S(1)}) custom-call(bf16[1024,256]{1,0:T(8,128)(2,1)S(1)} %get-tuple-element.60.q_ref, bf16[1024,256]{1,0:T(8,128)(2,1)S(1)} %get-tuple-element.61.k_ref, bf16[1024,256]{1,0:T(8,128)(2,1)S(1)} %get-tuple-element.62.v_ref, ...), custom_call_target="tpu_custom_call" | custom-call | flops 301989888 | bytes 4456448 | tf_op jit(solution)/shard_map/pallas_call | solution.py:461
  16.5 1.3 %collective-permute-start.1 = (bf16[256,512]{1,0:T(8,128)(2,1)S(1)}, bf16[256,512]{1,0:T(8,128)(2,1)S(1)}, u32[]{:S(2)}, u32[]{:S(2)}) collective-permute-start(bf16[256,512]{1,0:T(8,128)(2,1)S(1)} %get-tuple-element.75), channel_id=1, source_target_pairs={{8,0},{16,8},{24,16},{32,24},{40,32},{48,40},{56,48},{64,56},{72,6... | collective-permute-start | bytes 786440 | tf_op jit(solution)/shard_map/ppermute | solution.py:476
  17.8 3.4 %shard_map.121 = (bf16[1024,256]{1,0:T(8,128)(2,1)S(1)}, bf16[768,256]{1,0:T(8,128)(2,1)S(1)}, bf16[768,256]{1,0:T(8,128)(2,1)S(1)}, f32[256,512]{1,0:T(8,128)S(1)}, f32[2,384,128]{2,1,0:T(8,128)S(1)}) custom-call(bf16[1024,256]{1,0:T(8,128)(2,1)S(1)} %get-tuple-element.60.q_ref, bf16[1024,256]{1,0:T(8,128)(2,1)S(1)} %get-tuple-element.61.k_ref, ...), custom_call_target="tpu_custom_call" | custom-call | flops 452984832 | bytes 7274496 | tf_op jit(solution)/shard_map/pallas_call | solution.py:461
  21.2 5.0 %collective-permute-done.1.back_ref = bf16[256,512]{1,0:T(8,128)(2,1)S(1)} collective-permute-done((bf16[256,512]{1,0:T(8,128)(2,1)S(1)}, bf16[256,512]{1,0:T(8,128)(2,1)S(1)}, u32[]{:S(2)}, u32[]{:S(2)}) %collective-permute-start.1) | collective-permute-done | bytes 262176 | tf_op jit(solution)/shard_map/ppermute | solution.py:476
  26.2 0.1 shard_map.122
  26.3 0.1 collective-permute-start.5
  26.4 1.9 %shard_map.124 = (bf16[528,256]{1,0:T(8,128)(2,1)S(1)}, bf16[528,256]{1,0:T(8,128)(2,1)S(1)}, bf16[528,256]{1,0:T(8,128)(2,1)S(1)}, bf16[512,256]{1,0:T(8,128)(2,1)S(1)}, f32[4,256]{1,0:T(4,128)S(1)}) custom-call(bf16[1024,2048]{1,0:T(8,128)(2,1)S(1)} %get-tuple-element.56.x_ref, bf16[1024,256]{1,0:T(8,128)(2,1)S(1)} %get-tuple-element.71.dq_in.grad_ref, ...), custom_call_target="tpu_custom_call" | custom-call | flops 1073741824 | bytes 6189056 | tf_op jit(solution)/shard_map/pallas_call | solution.py:461
  28.3 4.7 %collective-permute-start.2 = (bf16[528,256]{1,0:T(8,128)(2,1)S(1)}, bf16[528,256]{1,0:T(8,128)(2,1)S(1)}, u32[]{:S(2)}, u32[]{:S(2)}) collective-permute-start(bf16[528,256]{1,0:T(8,128)(2,1)S(1)} %get-tuple-element.83), channel_id=1, source_target_pairs={{0,64},{8,72},{16,80},{24,88},{32,224},{40,232},{48,240},{56,248},... | collective-permute-start | bytes 811016 | tf_op jit(solution)/shard_map/ppermute | solution.py:97
  33.0 1.3 %shard_map.125.own_hbm = bf16[2048,256]{1,0:T(8,128)(2,1)S(1)} custom-call(bf16[1024,2048]{1,0:T(8,128)(2,1)S(1)} %get-tuple-element.56.x_ref, bf16[1024,256]{1,0:T(8,128)(2,1)S(1)} %get-tuple-element.76.own_in.grad_ref), custom_call_target="tpu_custom_call" | custom-call | flops 1073741824 | bytes 5767168 | tf_op jit(solution)/shard_map/pallas_call | solution.py:461
  34.3 0.0 collective-permute-done.5.grad_ref
  34.3 1.6 %shard_map.126 = (bf16[512,512]{1,0:T(8,128)(2,1)S(1)}, bf16[512,512]{1,0:T(8,128)(2,1)S(1)}, bf16[512,512]{1,0:T(8,128)(2,1)S(1)}, bf16[512,512]{1,0:T(8,128)(2,1)S(1)}) custom-call(bf16[1024,2048]{1,0:T(8,128)(2,1)S(1)} %get-tuple-element.56.x_ref, bf16[1024,256]{1,0:T(8,128)(2,1)S(1)} %collective-permute-done.5.grad_ref, ...), custom_call_target="tpu_custom_call" | custom-call | flops 1073741824 | bytes 7864320 | tf_op jit(solution)/shard_map/pallas_call | solution.py:461
  35.9 5.8 %collective-permute-start.6 = (bf16[512,512]{1,0:T(8,128)(2,1)S(1)}, bf16[512,512]{1,0:T(8,128)(2,1)S(1)}, u32[]{:S(2)}, u32[]{:S(2)}) collective-permute-start(bf16[512,512]{1,0:T(8,128)(2,1)S(1)} %get-tuple-element.87), channel_id=1, source_target_pairs={{0,64},{8,72},{16,80},{24,88},{32,224},{40,232},{48,240},{56,248},... | collective-permute-start | bytes 1572872 | tf_op jit(solution)/shard_map/ppermute | solution.py:97
  41.7 0.0 collective-permute-start.7
  41.7 0.0 collective-permute-start.8
  41.7 2.0 %collective-permute-start.3 = (bf16[528,256]{1,0:T(8,128)(2,1)S(1)}, bf16[528,256]{1,0:T(8,128)(2,1)S(1)}, u32[]{:S(2)}, u32[]{:S(2)}) collective-permute-start(bf16[528,256]{1,0:T(8,128)(2,1)S(1)} %get-tuple-element.84), channel_id=1, source_target_pairs={{0,32},{8,40},{16,48},{24,56},{32,0},{40,8},{48,16},{56,24},{64,96... | collective-permute-start | bytes 811016 | tf_op jit(solution)/shard_map/ppermute | solution.py:97
  43.7 0.0 collective-permute-done.2.a0
  43.7 1.2 %collective-permute-start.4 = (bf16[528,256]{1,0:T(8,128)(2,1)S(1)}, bf16[528,256]{1,0:T(8,128)(2,1)S(1)}, u32[]{:S(2)}, u32[]{:S(2)}) collective-permute-start(bf16[528,256]{1,0:T(8,128)(2,1)S(1)} %get-tuple-element.85), channel_id=1, source_target_pairs={{0,224},{8,232},{16,240},{24,248},{32,64},{40,72},{48,80},{56,88},... | collective-permute-start | bytes 811016 | tf_op jit(solution)/shard_map/ppermute | solution.py:97
  44.9 12.3 %collective-permute-done.3.a1 = bf16[528,256]{1,0:T(8,128)(2,1)S(1)} collective-permute-done((bf16[528,256]{1,0:T(8,128)(2,1)S(1)}, bf16[528,256]{1,0:T(8,128)(2,1)S(1)}, u32[]{:S(2)}, u32[]{:S(2)}) %collective-permute-start.3) | collective-permute-done | bytes 270368 | tf_op jit(solution)/shard_map/ppermute | solution.py:97
  57.2 0.0 collective-permute-done.4.a2
  57.2 0.0 collective-permute-done.6.b0
  57.2 0.0 collective-permute-done.7.b1
  57.2 0.0 collective-permute-done.8.b2
  57.2 0.4 shard_map.127
  57.6 1.6 %collective-permute-start.9 = (bf16[144,768]{1,0:T(8,128)(2,1)S(1)}, bf16[144,768]{1,0:T(8,128)(2,1)S(1)}, u32[]{:S(2)}, u32[]{:S(2)}) collective-permute-start(bf16[144,768]{1,0:T(8,128)(2,1)S(1)} %get-tuple-element.92), channel_id=1, source_target_pairs={{0,16},{8,24},{16,0},{24,8},{32,48},{40,56},{48,32},{56,40},{64,80... | collective-permute-start | bytes 663560 | tf_op jit(solution)/shard_map/ppermute | solution.py:97
  59.2 2.4 %collective-permute-start.10 = (bf16[144,768]{1,0:T(8,128)(2,1)S(1)}, bf16[144,768]{1,0:T(8,128)(2,1)S(1)}, u32[]{:S(2)}, u32[]{:S(2)}) collective-permute-start(bf16[144,768]{1,0:T(8,128)(2,1)S(1)} %get-tuple-element.93), channel_id=1, source_target_pairs={{0,8},{8,0},{16,24},{24,16},{32,40},{40,32},{48,56},{56,48},{64,72... | collective-permute-start | bytes 663560 | tf_op jit(solution)/shard_map/ppermute | solution.py:97
  61.7 0.1 collective-permute-start.11
  61.8 3.3 %collective-permute-done.9.g0 = bf16[144,768]{1,0:T(8,128)(2,1)S(1)} collective-permute-done((bf16[144,768]{1,0:T(8,128)(2,1)S(1)}, bf16[144,768]{1,0:T(8,128)(2,1)S(1)}, u32[]{:S(2)}, u32[]{:S(2)}) %collective-permute-start.9) | collective-permute-done | bytes 221216 | tf_op jit(solution)/shard_map/ppermute | solution.py:97
  65.1 2.8 %collective-permute-done.10.g1 = bf16[144,768]{1,0:T(8,128)(2,1)S(1)} collective-permute-done((bf16[144,768]{1,0:T(8,128)(2,1)S(1)}, bf16[144,768]{1,0:T(8,128)(2,1)S(1)}, u32[]{:S(2)}, u32[]{:S(2)}) %collective-permute-start.10) | collective-permute-done | bytes 221216 | tf_op jit(solution)/shard_map/ppermute | solution.py:97
  68.0 0.8 %collective-permute-done.11.g2 = bf16[144,768]{1,0:T(8,128)(2,1)S(1)} collective-permute-done((bf16[144,768]{1,0:T(8,128)(2,1)S(1)}, bf16[144,768]{1,0:T(8,128)(2,1)S(1)}, u32[]{:S(2)}, u32[]{:S(2)}) %collective-permute-start.11) | collective-permute-done | bytes 221216 | tf_op jit(solution)/shard_map/ppermute | solution.py:97
  68.8 0.1 shard_map.128
  68.9 3.4 %collective-permute-start.12 = (bf16[80,512]{1,0:T(8,128)(2,1)S(1)}, bf16[80,512]{1,0:T(8,128)(2,1)S(1)}, u32[]{:S(2)}, u32[]{:S(2)}) collective-permute-start(bf16[80,512]{1,0:T(8,128)(2,1)S(1)} %get-tuple-element.97), channel_id=1, source_target_pairs={{0,96},{8,104},{16,112},{24,120},{32,192},{40,200},{48,208},{56,21... | collective-permute-start | bytes 245768 | tf_op jit(solution)/shard_map/ppermute | solution.py:97
  72.3 0.0 collective-permute-start.14
  72.3 0.7 collective-permute-start.13
  73.0 1.2 %shard_map.123 = (bf16[1024,256]{1,0:T(8,128)(2,1)}, bf16[1024,256]{1,0:T(8,128)(2,1)}, bf16[1024,256]{1,0:T(8,128)(2,1)}) custom-call(bf16[1024,256]{1,0:T(8,128)(2,1)S(1)} %get-tuple-element.71.dq_in.grad_ref, bf16[1024,256]{1,0:T(8,128)(2,1)S(1)} %get-tuple-element.76.own_in.grad_ref, bf16[1024,256]{1,0:T(8,128)(2,1)S(1)} %get-tuple-element.77.swap_in), custom_call_target="tpu_custom_call" | custom-call | flops 1048576 | bytes 3145728 | tf_op jit(solution)/shard_map/pallas_call | solution.py:461
  74.1 4.3 %collective-permute-done.13.two_ref = bf16[64,256]{1,0:T(8,128)(2,1)S(1)} collective-permute-done((bf16[64,256]{1,0:T(8,128)(2,1)S(1)}, bf16[64,256]{1,0:T(8,128)(2,1)S(1)}, u32[]{:S(2)}, u32[]{:S(2)}) %collective-permute-start.13) | collective-permute-done | bytes 32800 | tf_op jit(solution)/shard_map/ppermute | solution.py:97
  78.4 0.0 collective-permute-done.14.three_ref
  78.4 0.0 collective-permute-done.12.one_ref
  78.4 0.7 shard_map.129
Async XLA Ops:
  3.9 10.3 %collective-permute-start = (bf16[256,512]{1,0:T(8,128)(2,1)S(1)}, bf16[256,512]{1,0:T(8,128)(2,1)S(1)}, u32[]{:S(2)}, u32[]{:S(2)}) collective-permute-start(bf16[256,512]{1,0:T(8,128)(2,1)S(1)} %get-tuple-element.64), channel_id=1, source_target_pairs={{0,8},{8,16},{16,24},{24,32},{32,40},{40,48},{48,56},{56,64},{64,7... | collective-permute-start | bytes 786440 | tf_op jit(solution)/shard_map/ppermute | solution.py:476
  7.3 3.5 %copy-start = (bf16[1024,256]{1,0:T(8,128)(2,1)S(1)}, bf16[1024,256]{1,0:T(8,128)(2,1)}, u32[]{:S(2)}) copy-start(bf16[1024,256]{1,0:T(8,128)(2,1)} %og_ref.5) | copy-start | bytes 1572868
  7.3 3.5 %copy-start.1 = (f32[2,257]{1,0:T(2,128)S(1)}, f32[2,257]{1,0:T(2,128)}, u32[]{:S(2)}) copy-start(f32[2,257]{1,0:T(2,128)} %rel_ref.1) | copy-start | bytes 6172
  16.5 9.7 %collective-permute-start.1 = (bf16[256,512]{1,0:T(8,128)(2,1)S(1)}, bf16[256,512]{1,0:T(8,128)(2,1)S(1)}, u32[]{:S(2)}, u32[]{:S(2)}) collective-permute-start(bf16[256,512]{1,0:T(8,128)(2,1)S(1)} %get-tuple-element.75), channel_id=1, source_target_pairs={{8,0},{16,8},{24,16},{32,24},{40,32},{48,40},{56,48},{64,56},{72,6... | collective-permute-start | bytes 786440 | tf_op jit(solution)/shard_map/ppermute | solution.py:476
  26.3 8.0 %collective-permute-start.5 = (bf16[1024,256]{1,0:T(8,128)(2,1)S(1)}, bf16[1024,256]{1,0:T(8,128)(2,1)S(1)}, u32[]{:S(2)}, u32[]{:S(2)}) collective-permute-start(bf16[1024,256]{1,0:T(8,128)(2,1)S(1)} %get-tuple-element.77.swap_in), channel_id=1, source_target_pairs={{0,1},{1,0},{2,3},{3,2},{4,5},{5,4},{6,7},{7,6},{8,9},{9,8},{10,11... | collective-permute-start | bytes 1572872 | tf_op jit(solution)/shard_map/ppermute | solution.py:106
  28.3 15.4 %collective-permute-start.2 = (bf16[528,256]{1,0:T(8,128)(2,1)S(1)}, bf16[528,256]{1,0:T(8,128)(2,1)S(1)}, u32[]{:S(2)}, u32[]{:S(2)}) collective-permute-start(bf16[528,256]{1,0:T(8,128)(2,1)S(1)} %get-tuple-element.83), channel_id=1, source_target_pairs={{0,64},{8,72},{16,80},{24,88},{32,224},{40,232},{48,240},{56,248},... | collective-permute-start | bytes 811016 | tf_op jit(solution)/shard_map/ppermute | solution.py:97
  35.9 21.3 %collective-permute-start.6 = (bf16[512,512]{1,0:T(8,128)(2,1)S(1)}, bf16[512,512]{1,0:T(8,128)(2,1)S(1)}, u32[]{:S(2)}, u32[]{:S(2)}) collective-permute-start(bf16[512,512]{1,0:T(8,128)(2,1)S(1)} %get-tuple-element.87), channel_id=1, source_target_pairs={{0,64},{8,72},{16,80},{24,88},{32,224},{40,232},{48,240},{56,248},... | collective-permute-start | bytes 1572872 | tf_op jit(solution)/shard_map/ppermute | solution.py:97
  41.7 15.5 %collective-permute-start.7 = (bf16[512,512]{1,0:T(8,128)(2,1)S(1)}, bf16[512,512]{1,0:T(8,128)(2,1)S(1)}, u32[]{:S(2)}, u32[]{:S(2)}) collective-permute-start(bf16[512,512]{1,0:T(8,128)(2,1)S(1)} %get-tuple-element.88), channel_id=1, source_target_pairs={{0,32},{8,40},{16,48},{24,56},{32,0},{40,8},{48,16},{56,24},{64,96... | collective-permute-start | bytes 1572872 | tf_op jit(solution)/shard_map/ppermute | solution.py:97
  41.7 15.5 %collective-permute-start.8 = (bf16[512,512]{1,0:T(8,128)(2,1)S(1)}, bf16[512,512]{1,0:T(8,128)(2,1)S(1)}, u32[]{:S(2)}, u32[]{:S(2)}) collective-permute-start(bf16[512,512]{1,0:T(8,128)(2,1)S(1)} %get-tuple-element.89), channel_id=1, source_target_pairs={{0,224},{8,232},{16,240},{24,248},{32,64},{40,72},{48,80},{56,88},... | collective-permute-start | bytes 1572872 | tf_op jit(solution)/shard_map/ppermute | solution.py:97
  41.7 15.5 %collective-permute-start.3 = (bf16[528,256]{1,0:T(8,128)(2,1)S(1)}, bf16[528,256]{1,0:T(8,128)(2,1)S(1)}, u32[]{:S(2)}, u32[]{:S(2)}) collective-permute-start(bf16[528,256]{1,0:T(8,128)(2,1)S(1)} %get-tuple-element.84), channel_id=1, source_target_pairs={{0,32},{8,40},{16,48},{24,56},{32,0},{40,8},{48,16},{56,24},{64,96... | collective-permute-start | bytes 811016 | tf_op jit(solution)/shard_map/ppermute | solution.py:97
  43.7 13.5 %collective-permute-start.4 = (bf16[528,256]{1,0:T(8,128)(2,1)S(1)}, bf16[528,256]{1,0:T(8,128)(2,1)S(1)}, u32[]{:S(2)}, u32[]{:S(2)}) collective-permute-start(bf16[528,256]{1,0:T(8,128)(2,1)S(1)} %get-tuple-element.85), channel_id=1, source_target_pairs={{0,224},{8,232},{16,240},{24,248},{32,64},{40,72},{48,80},{56,88},... | collective-permute-start | bytes 811016 | tf_op jit(solution)/shard_map/ppermute | solution.py:97
  57.6 7.5 %collective-permute-start.9 = (bf16[144,768]{1,0:T(8,128)(2,1)S(1)}, bf16[144,768]{1,0:T(8,128)(2,1)S(1)}, u32[]{:S(2)}, u32[]{:S(2)}) collective-permute-start(bf16[144,768]{1,0:T(8,128)(2,1)S(1)} %get-tuple-element.92), channel_id=1, source_target_pairs={{0,16},{8,24},{16,0},{24,8},{32,48},{40,56},{48,32},{56,40},{64,80... | collective-permute-start | bytes 663560 | tf_op jit(solution)/shard_map/ppermute | solution.py:97
  59.2 8.7 %collective-permute-start.10 = (bf16[144,768]{1,0:T(8,128)(2,1)S(1)}, bf16[144,768]{1,0:T(8,128)(2,1)S(1)}, u32[]{:S(2)}, u32[]{:S(2)}) collective-permute-start(bf16[144,768]{1,0:T(8,128)(2,1)S(1)} %get-tuple-element.93), channel_id=1, source_target_pairs={{0,8},{8,0},{16,24},{24,16},{32,40},{40,32},{48,56},{56,48},{64,72... | collective-permute-start | bytes 663560 | tf_op jit(solution)/shard_map/ppermute | solution.py:97
  61.7 7.1 %collective-permute-start.11 = (bf16[144,768]{1,0:T(8,128)(2,1)S(1)}, bf16[144,768]{1,0:T(8,128)(2,1)S(1)}, u32[]{:S(2)}, u32[]{:S(2)}) collective-permute-start(bf16[144,768]{1,0:T(8,128)(2,1)S(1)} %get-tuple-element.94), channel_id=1, source_target_pairs={{0,24},{8,16},{16,8},{24,0},{32,56},{40,48},{48,40},{56,32},{64,88... | collective-permute-start | bytes 663560 | tf_op jit(solution)/shard_map/ppermute | solution.py:97
  68.9 9.5 %collective-permute-start.12 = (bf16[80,512]{1,0:T(8,128)(2,1)S(1)}, bf16[80,512]{1,0:T(8,128)(2,1)S(1)}, u32[]{:S(2)}, u32[]{:S(2)}) collective-permute-start(bf16[80,512]{1,0:T(8,128)(2,1)S(1)} %get-tuple-element.97), channel_id=1, source_target_pairs={{0,96},{8,104},{16,112},{24,120},{32,192},{40,200},{48,208},{56,21... | collective-permute-start | bytes 245768 | tf_op jit(solution)/shard_map/ppermute | solution.py:97
  72.3 6.1 %collective-permute-start.14 = (f32[64,256]{1,0:T(8,128)S(1)}, f32[64,256]{1,0:T(8,128)S(1)}, u32[]{:S(2)}, u32[]{:S(2)}) collective-permute-start(f32[64,256]{1,0:T(8,128)S(1)} %get-tuple-element.99), channel_id=1, source_target_pairs={{0,1},{1,0},{2,3},{3,2},{4,5},{5,4},{6,7},{7,6},{8,9},{9,8},{10,11... | collective-permute-start | bytes 196616 | tf_op jit(solution)/shard_map/ppermute | solution.py:106
  72.3 6.1 %collective-permute-start.13 = (bf16[64,256]{1,0:T(8,128)(2,1)S(1)}, bf16[64,256]{1,0:T(8,128)(2,1)S(1)}, u32[]{:S(2)}, u32[]{:S(2)}) collective-permute-start(bf16[64,256]{1,0:T(8,128)(2,1)S(1)} %get-tuple-element.98), channel_id=1, source_target_pairs={{0,97},{8,105},{16,113},{24,121},{32,193},{40,201},{48,209},{56,21... | collective-permute-start | bytes 98312 | tf_op jit(solution)/shard_map/ppermute | solution.py:97

commit v5 on v4

--- a/solution.py
+++ b/solution.py
@@ -17,7 +17,7 @@
 NZ, NX = 8, 4
 ROWS = 64
 EXTRA = 16
-LATE = 384
+LATE = 256
 VMEM_LIMIT = 24 << 20
 LOAD_LIMIT = 24 << 20
 CHUNKS = 4
@@ -38,7 +38,7 @@
 XO, XE = ("sp_1", odd_pair), ("sp_1", even_pair(NX))
 ZO, ZE = ("sp_0", odd_pair), ("sp_0", even_pair(NZ))
 Z3 = ("sp_0", lambda i: (3, 6, 5, 0, 7, 2, 1, 4)[i])
-LEVELS = ((ZO, ZE, XO, XE, Z3), (XO, XE, ZO, ZE, Z3))
+LEVELS = ((XO, XE, ZO, ZE, Z3), (ZO, ZE, XO, XE, Z3))
 
 
 def held_order(steps, device):
@@ -189,7 +189,7 @@
     ka_s[...] = jnp.zeros_like(ka_s)
     va_s[...] = jnp.zeros_like(va_s)
     tiles(
-        range(3, 6), q_ref, k_ref, v_ref, og_ref, bias_ref, kt_s, vt_s, pat_ref, dq_ref, LATE + REACH,
+        range(LATE // TILE, 6), q_ref, k_ref, v_ref, og_ref, bias_ref, kt_s, vt_s, pat_ref, dq_ref, LATE + REACH,
         ka_s, va_s, LATE,
     )
     acc_ref[:, :256] = ka_s[...]
@@ -241,14 +241,12 @@
     vt_s[...] = v_ref[: LATE + REACH].T
     ka_s[:REACH] = edge_in[:, :256]
     va_s[:REACH] = edge_in[:, 256:]
-    ka_s[REACH:LATE] = jnp.zeros((LATE - REACH, 256), F32)
-    va_s[REACH:LATE] = jnp.zeros((LATE - REACH, 256), F32)
     ka_s[LATE:] = acc_in[: LATE + REACH - LATE, :256]
     va_s[LATE:] = acc_in[: LATE + REACH - LATE, 256:]
     pat_ref[...] = pat_in[...]
     near_ref[:REACH] = dq_in[...]
     near_ref[LATE + REACH :] = dq_late[...]
-    tiles(range(3), q_ref, k_ref, v_ref, og_ref, bias_ref, kt_s, vt_s, pat_ref, near_ref, 0, ka_s, va_s, 0)
+    tiles(range(LATE // TILE), q_ref, k_ref, v_ref, og_ref, bias_ref, kt_s, vt_s, pat_ref, near_ref, 0, ka_s, va_s, 0)
     last = LATE + REACH
     kg_ref[:last] = ka_s[...].astype(BF16)
     vg_ref[:last] = va_s[...].astype(BF16)
@@ -496,7 +494,7 @@
     pattern = f32(2, BAND, TILE)
     dq_late, acc, bias, pat = call(
         late_kernel, (query, key, value, out_grad, rel_table),
-        (b16(384, 256), f32(span, 512), pattern, pattern),
+        (b16(span - REACH, 256), f32(span, 512), pattern, pattern),
         (v16(256, span), v16(256, span), v32(span, 256), v32(span, 256)), flops=6 * tile_flops,
     )
     dq0, edge, back, pat = call(
@@ -509,7 +507,7 @@
     dq, kg, vg, edge, pat = call(
         attn_kernel, (query, key, value, out_grad, bias, pat, edge, acc, dq0, dq_late),
         (b16(1024, 256), b16(768, 256), b16(768, 256), f32(REACH, 512), pattern),
-        (v16(256, 640), v16(256, 640), v32(640, 256), v32(640, 256)), flops=6 * tile_flops,
+        (v16(256, LATE + REACH), v16(256, LATE + REACH), v32(LATE + REACH, 256), v32(LATE + REACH, 256)), flops=6 * tile_flops,
     )
     product = 2 * 1024 * 2048 * 256
     dma = pltpu.SemaphoreType.DMA

time: 80.3 us -> 81.8 us (1.019)
  the two profiles are of different devices: /device:TPU:8 before, /device:TPU:27 now
where the time goes in v5:
time: 81.8 us; the launch traced here: 81.7 us
  starting transfers between devices  31.2 us (38%)
  waiting for transfers between devices  26.6 us (33%)
  Pallas kernels  23 us (28%)
    pallas_call x13, Pallas kernels, call(): pl.pallas_call(kernel, grid=grid, in_specs=specs, out_specs=out_specs, ou...  23 us
    ppermute x11, waiting for transfers between devices, exchange(): return lax.ppermute(block, SP + ('core',), level_route(steps, across))  22.3 us
    ppermute x11, starting transfers between devices, exchange(): return lax.ppermute(block, SP + ('core',), level_route(steps, across))  18 us
    ppermute x2, starting transfers between devices, core_swap(): return lax.ppermute(block, 'core', [(0, 1), (1, 0)])  7.92 us
    ppermute x2, starting transfers between devices, neighbour(): return lax.ppermute(block, SP, route)  5.29 us
    ppermute x2, waiting for transfers between devices, neighbour(): return lax.ppermute(block, SP, route)  4.26 us
  transfers between devices with their start and end apart: 15, of which 6 were waited for; matrix products, arithmetic and copies ran while one was open for 0% of the time, Pallas kernels for 20%

profile of v5, /device:TPU:27, one launch (start us, length us, event | category | flops | bytes accessed | tf_op | source)
XLA Modules:
  0.0 81.7 jit_solution(14933209611738496161)
XLA Ops:
  0.6 3.2 %shard_map.117 = (bf16[256,512]{1,0:T(8,128)(2,1)S(1)}, bf16[1024,2048]{1,0:T(8,128)(2,1)S(1)}, bf16[2048,256]{1,0:T(8,128)(2,1)S(1)}, bf16[2048,256]{1,0:T(8,128)(2,1)S(1)}, bf16[2048,256]{1,0:T(8,128)(2,1)S(1)}) custom-call(bf16[1024,2048]{1,0:T(8,128)(2,1)} %x_hbm.1, bf16[2048,256]{1,0:T(8,128)(2,1)} %wq_hbm.1, bf16[2048,256]{1,0:T(8,128)(2,1)} %wk_hbm.1, ...), custom_call_target="tpu_custom_call" | custom-call | flops 536870912 | bytes 14942208 | tf_op jit(solution)/shard_map/pallas_call | solution.py:459
  3.9 3.1 %collective-permute-start = (bf16[256,512]{1,0:T(8,128)(2,1)S(1)}, bf16[256,512]{1,0:T(8,128)(2,1)S(1)}, u32[]{:S(2)}, u32[]{:S(2)}) collective-permute-start(bf16[256,512]{1,0:T(8,128)(2,1)S(1)} %get-tuple-element.64), channel_id=1, source_target_pairs={{0,8},{8,16},{16,24},{24,32},{32,40},{40,48},{48,56},{56,64},{64,7... | collective-permute-start | bytes 786440 | tf_op jit(solution)/shard_map/ppermute | solution.py:474
  7.0 0.0 copy-start
  7.0 0.0 copy-start.1
  7.0 3.4 %shard_map.118 = (bf16[1024,256]{1,0:T(8,128)(2,1)S(1)}, bf16[1024,256]{1,0:T(8,128)(2,1)S(1)}, bf16[1024,256]{1,0:T(8,128)(2,1)S(1)}) custom-call(bf16[1024,2048]{1,0:T(8,128)(2,1)S(1)} %get-tuple-element.56.x_ref, bf16[2048,256]{1,0:T(8,128)(2,1)S(1)} %get-tuple-element.57.wq_ref, bf16[2048,256]{1,0:T(8,128)(2,1)S(1)} %get-tuple-element.58.wk_ref, ...), custom_call_target="tpu_custom_call" | custom-call | flops 3221225472 | bytes 8912896 | tf_op jit(solution)/shard_map/pallas_call | solution.py:459
  10.4 0.0 copy-done
  10.4 0.0 copy-done.1
  10.4 4.4 %shard_map.119 = (bf16[512,256]{1,0:T(8,128)(2,1)S(1)}, f32[768,512]{1,0:T(8,128)S(1)}, f32[2,384,128]{2,1,0:T(8,128)S(1)}, f32[2,384,128]{2,1,0:T(8,128)S(1)}) custom-call(bf16[1024,256]{1,0:T(8,128)(2,1)S(1)} %get-tuple-element.60.q_ref, bf16[1024,256]{1,0:T(8,128)(2,1)S(1)} %get-tuple-element.61.k_ref, bf16[1024,256]{1,0:T(8,128)(2,1)S(1)} %get-tuple-element.62.v_ref, ...), custom_call_target="tpu_custom_call" | custom-call | flops 452984832 | bytes 4720648 | tf_op jit(solution)/shard_map/pallas_call | solution.py:459
  14.9 0.0 collective-permute-done.halo_ref
  14.9 2.3 %shard_map.120 = (bf16[256,256]{1,0:T(8,128)(2,1)S(1)}, f32[256,512]{1,0:T(8,128)S(1)}, bf16[256,512]{1,0:T(8,128)(2,1)S(1)}, f32[2,384,128]{2,1,0:T(8,128)S(1)}) custom-call(bf16[1024,256]{1,0:T(8,128)(2,1)S(1)} %get-tuple-element.60.q_ref, bf16[1024,256]{1,0:T(8,128)(2,1)S(1)} %get-tuple-element.61.k_ref, bf16[1024,256]{1,0:T(8,128)(2,1)S(1)} %get-tuple-element.62.v_ref, ...), custom_call_target="tpu_custom_call" | custom-call | flops 301989888 | bytes 4456448 | tf_op jit(solution)/shard_map/pallas_call | solution.py:459
  17.2 2.2 %collective-permute-start.1 = (bf16[256,512]{1,0:T(8,128)(2,1)S(1)}, bf16[256,512]{1,0:T(8,128)(2,1)S(1)}, u32[]{:S(2)}, u32[]{:S(2)}) collective-permute-start(bf16[256,512]{1,0:T(8,128)(2,1)S(1)} %get-tuple-element.75), channel_id=1, source_target_pairs={{8,0},{16,8},{24,16},{32,24},{40,32},{48,40},{56,48},{64,56},{72,6... | collective-permute-start | bytes 786440 | tf_op jit(solution)/shard_map/ppermute | solution.py:474
  19.4 2.4 %shard_map.121 = (bf16[1024,256]{1,0:T(8,128)(2,1)S(1)}, bf16[768,256]{1,0:T(8,128)(2,1)S(1)}, bf16[768,256]{1,0:T(8,128)(2,1)S(1)}, f32[256,512]{1,0:T(8,128)S(1)}, f32[2,384,128]{2,1,0:T(8,128)S(1)}) custom-call(bf16[1024,256]{1,0:T(8,128)(2,1)S(1)} %get-tuple-element.60.q_ref, bf16[1024,256]{1,0:T(8,128)(2,1)S(1)} %get-tuple-element.61.k_ref, ...), custom_call_target="tpu_custom_call" | custom-call | flops 452984832 | bytes 7602176 | tf_op jit(solution)/shard_map/pallas_call | solution.py:459
  21.8 4.3 %collective-permute-done.1.back_ref = bf16[256,512]{1,0:T(8,128)(2,1)S(1)} collective-permute-done((bf16[256,512]{1,0:T(8,128)(2,1)S(1)}, bf16[256,512]{1,0:T(8,128)(2,1)S(1)}, u32[]{:S(2)}, u32[]{:S(2)}) %collective-permute-start.1) | collective-permute-done | bytes 262176 | tf_op jit(solution)/shard_map/ppermute | solution.py:474
  26.0 0.1 shard_map.122
  26.2 1.9 %collective-permute-start.5 = (bf16[1024,256]{1,0:T(8,128)(2,1)S(1)}, bf16[1024,256]{1,0:T(8,128)(2,1)S(1)}, u32[]{:S(2)}, u32[]{:S(2)}) collective-permute-start(bf16[1024,256]{1,0:T(8,128)(2,1)S(1)} %get-tuple-element.77.swap_in), channel_id=1, source_target_pairs={{0,1},{1,0},{2,3},{3,2},{4,5},{5,4},{6,7},{7,6},{8,9},{9,8},{10,11... | collective-permute-start | bytes 1572872 | tf_op jit(solution)/shard_map/ppermute | solution.py:106
  28.1 1.9 %shard_map.124 = (bf16[528,256]{1,0:T(8,128)(2,1)S(1)}, bf16[528,256]{1,0:T(8,128)(2,1)S(1)}, bf16[528,256]{1,0:T(8,128)(2,1)S(1)}, bf16[512,256]{1,0:T(8,128)(2,1)S(1)}, f32[4,256]{1,0:T(4,128)S(1)}) custom-call(bf16[1024,2048]{1,0:T(8,128)(2,1)S(1)} %get-tuple-element.56.x_ref, bf16[1024,256]{1,0:T(8,128)(2,1)S(1)} %get-tuple-element.71.dq_in.grad_ref, ...), custom_call_target="tpu_custom_call" | custom-call | flops 1073741824 | bytes 6189056 | tf_op jit(solution)/shard_map/pallas_call | solution.py:459
  29.9 3.2 %collective-permute-start.2 = (bf16[528,256]{1,0:T(8,128)(2,1)S(1)}, bf16[528,256]{1,0:T(8,128)(2,1)S(1)}, u32[]{:S(2)}, u32[]{:S(2)}) collective-permute-start(bf16[528,256]{1,0:T(8,128)(2,1)S(1)} %get-tuple-element.83), channel_id=1, source_target_pairs={{0,16},{8,24},{16,0},{24,8},{32,48},{40,56},{48,32},{56,40},{64,80... | collective-permute-start | bytes 811016 | tf_op jit(solution)/shard_map/ppermute | solution.py:97
  33.2 1.3 %shard_map.125.own_hbm = bf16[2048,256]{1,0:T(8,128)(2,1)S(1)} custom-call(bf16[1024,2048]{1,0:T(8,128)(2,1)S(1)} %get-tuple-element.56.x_ref, bf16[1024,256]{1,0:T(8,128)(2,1)S(1)} %get-tuple-element.76.own_in.grad_ref), custom_call_target="tpu_custom_call" | custom-call | flops 1073741824 | bytes 5767168 | tf_op jit(solution)/shard_map/pallas_call | solution.py:459
  34.5 0.0 collective-permute-done.5.grad_ref
  34.5 1.6 %shard_map.126 = (bf16[512,512]{1,0:T(8,128)(2,1)S(1)}, bf16[512,512]{1,0:T(8,128)(2,1)S(1)}, bf16[512,512]{1,0:T(8,128)(2,1)S(1)}, bf16[512,512]{1,0:T(8,128)(2,1)S(1)}) custom-call(bf16[1024,2048]{1,0:T(8,128)(2,1)S(1)} %get-tuple-element.56.x_ref, bf16[1024,256]{1,0:T(8,128)(2,1)S(1)} %collective-permute-done.5.grad_ref, ...), custom_call_target="tpu_custom_call" | custom-call | flops 1073741824 | bytes 7864320 | tf_op jit(solution)/shard_map/pallas_call | solution.py:459
  36.1 4.3 %collective-permute-start.6 = (bf16[512,512]{1,0:T(8,128)(2,1)S(1)}, bf16[512,512]{1,0:T(8,128)(2,1)S(1)}, u32[]{:S(2)}, u32[]{:S(2)}) collective-permute-start(bf16[512,512]{1,0:T(8,128)(2,1)S(1)} %get-tuple-element.87), channel_id=1, source_target_pairs={{0,16},{8,24},{16,0},{24,8},{32,48},{40,56},{48,32},{56,40},{64,80... | collective-permute-start | bytes 1572872 | tf_op jit(solution)/shard_map/ppermute | solution.py:97
  40.4 0.8 collective-permute-start.7
  41.1 0.0 collective-permute-start.8
  41.1 1.5 %collective-permute-start.3 = (bf16[528,256]{1,0:T(8,128)(2,1)S(1)}, bf16[528,256]{1,0:T(8,128)(2,1)S(1)}, u32[]{:S(2)}, u32[]{:S(2)}) collective-permute-start(bf16[528,256]{1,0:T(8,128)(2,1)S(1)} %get-tuple-element.84), channel_id=1, source_target_pairs={{0,8},{8,0},{16,24},{24,16},{32,40},{40,32},{48,56},{56,48},{64,72... | collective-permute-start | bytes 811016 | tf_op jit(solution)/shard_map/ppermute | solution.py:97
  42.6 0.0 collective-permute-done.2.a0
  42.6 1.2 %collective-permute-start.4 = (bf16[528,256]{1,0:T(8,128)(2,1)S(1)}, bf16[528,256]{1,0:T(8,128)(2,1)S(1)}, u32[]{:S(2)}, u32[]{:S(2)}) collective-permute-start(bf16[528,256]{1,0:T(8,128)(2,1)S(1)} %get-tuple-element.85), channel_id=1, source_target_pairs={{0,24},{8,16},{16,8},{24,0},{32,56},{40,48},{48,40},{56,32},{64,88... | collective-permute-start | bytes 811016 | tf_op jit(solution)/shard_map/ppermute | solution.py:97
  43.8 12.7 %collective-permute-done.3.a1 = bf16[528,256]{1,0:T(8,128)(2,1)S(1)} collective-permute-done((bf16[528,256]{1,0:T(8,128)(2,1)S(1)}, bf16[528,256]{1,0:T(8,128)(2,1)S(1)}, u32[]{:S(2)}, u32[]{:S(2)}) %collective-permute-start.3) | collective-permute-done | bytes 270368 | tf_op jit(solution)/shard_map/ppermute | solution.py:97
  56.5 0.0 collective-permute-done.4.a2
  56.6 0.0 collective-permute-done.6.b0
  56.6 0.0 collective-permute-done.7.b1
  56.6 0.0 collective-permute-done.8.b2
  56.6 0.4 shard_map.127
  57.0 3.2 %collective-permute-start.9 = (bf16[144,768]{1,0:T(8,128)(2,1)S(1)}, bf16[144,768]{1,0:T(8,128)(2,1)S(1)}, u32[]{:S(2)}, u32[]{:S(2)}) collective-permute-start(bf16[144,768]{1,0:T(8,128)(2,1)S(1)} %get-tuple-element.92), channel_id=1, source_target_pairs={{0,64},{8,72},{16,80},{24,88},{32,224},{40,232},{48,240},{56,248},... | collective-permute-start | bytes 663560 | tf_op jit(solution)/shard_map/ppermute | solution.py:97
  60.1 0.0 collective-permute-start.10
  60.1 0.4 collective-permute-start.11
  60.5 3.0 %collective-permute-done.9.g0 = bf16[144,768]{1,0:T(8,128)(2,1)S(1)} collective-permute-done((bf16[144,768]{1,0:T(8,128)(2,1)S(1)}, bf16[144,768]{1,0:T(8,128)(2,1)S(1)}, u32[]{:S(2)}, u32[]{:S(2)}) %collective-permute-start.9) | collective-permute-done | bytes 221216 | tf_op jit(solution)/shard_map/ppermute | solution.py:97
  63.6 1.9 %collective-permute-done.10.g1 = bf16[144,768]{1,0:T(8,128)(2,1)S(1)} collective-permute-done((bf16[144,768]{1,0:T(8,128)(2,1)S(1)}, bf16[144,768]{1,0:T(8,128)(2,1)S(1)}, u32[]{:S(2)}, u32[]{:S(2)}) %collective-permute-start.10) | collective-permute-done | bytes 221216 | tf_op jit(solution)/shard_map/ppermute | solution.py:97
  65.4 0.7 collective-permute-done.11.g2
  66.1 0.1 shard_map.128
  66.2 3.5 %collective-permute-start.12 = (bf16[80,512]{1,0:T(8,128)(2,1)S(1)}, bf16[80,512]{1,0:T(8,128)(2,1)S(1)}, u32[]{:S(2)}, u32[]{:S(2)}) collective-permute-start(bf16[80,512]{1,0:T(8,128)(2,1)S(1)} %get-tuple-element.97), channel_id=1, source_target_pairs={{0,96},{8,104},{16,112},{24,120},{32,192},{40,200},{48,208},{56,21... | collective-permute-start | bytes 245768 | tf_op jit(solution)/shard_map/ppermute | solution.py:97
  69.8 6.0 %collective-permute-start.14 = (f32[64,256]{1,0:T(8,128)S(1)}, f32[64,256]{1,0:T(8,128)S(1)}, u32[]{:S(2)}, u32[]{:S(2)}) collective-permute-start(f32[64,256]{1,0:T(8,128)S(1)} %get-tuple-element.99), channel_id=1, source_target_pairs={{0,1},{1,0},{2,3},{3,2},{4,5},{5,4},{6,7},{7,6},{8,9},{9,8},{10,11... | collective-permute-start | bytes 196616 | tf_op jit(solution)/shard_map/ppermute | solution.py:106
  75.8 0.0 collective-permute-start.13
  75.8 1.2 %shard_map.123 = (bf16[1024,256]{1,0:T(8,128)(2,1)}, bf16[1024,256]{1,0:T(8,128)(2,1)}, bf16[1024,256]{1,0:T(8,128)(2,1)}) custom-call(bf16[1024,256]{1,0:T(8,128)(2,1)S(1)} %get-tuple-element.71.dq_in.grad_ref, bf16[1024,256]{1,0:T(8,128)(2,1)S(1)} %get-tuple-element.76.own_in.grad_ref, bf16[1024,256]{1,0:T(8,128)(2,1)S(1)} %get-tuple-element.77.swap_in), custom_call_target="tpu_custom_call" | custom-call | flops 1048576 | bytes 3145728 | tf_op jit(solution)/shard_map/pallas_call | solution.py:459
  77.0 4.0 %collective-permute-done.13.two_ref = bf16[64,256]{1,0:T(8,128)(2,1)S(1)} collective-permute-done((bf16[64,256]{1,0:T(8,128)(2,1)S(1)}, bf16[64,256]{1,0:T(8,128)(2,1)S(1)}, u32[]{:S(2)}, u32[]{:S(2)}) %collective-permute-start.13) | collective-permute-done | bytes 32800 | tf_op jit(solution)/shard_map/ppermute | solution.py:97
  80.9 0.0 collective-permute-done.14.three_ref
  80.9 0.0 collective-permute-done.12.one_ref
  80.9 0.7 shard_map.129
Async XLA Ops:
  3.9 11.0 %collective-permute-start = (bf16[256,512]{1,0:T(8,128)(2,1)S(1)}, bf16[256,512]{1,0:T(8,128)(2,1)S(1)}, u32[]{:S(2)}, u32[]{:S(2)}) collective-permute-start(bf16[256,512]{1,0:T(8,128)(2,1)S(1)} %get-tuple-element.64), channel_id=1, source_target_pairs={{0,8},{8,16},{16,24},{24,32},{32,40},{40,48},{48,56},{56,64},{64,7... | collective-permute-start | bytes 786440 | tf_op jit(solution)/shard_map/ppermute | solution.py:474
  7.0 3.4 %copy-start = (bf16[1024,256]{1,0:T(8,128)(2,1)S(1)}, bf16[1024,256]{1,0:T(8,128)(2,1)}, u32[]{:S(2)}) copy-start(bf16[1024,256]{1,0:T(8,128)(2,1)} %og_ref.5) | copy-start | bytes 1572868
  7.0 3.4 %copy-start.1 = (f32[2,257]{1,0:T(2,128)S(1)}, f32[2,257]{1,0:T(2,128)}, u32[]{:S(2)}) copy-start(f32[2,257]{1,0:T(2,128)} %rel_ref.1) | copy-start | bytes 6172
  17.2 8.8 %collective-permute-start.1 = (bf16[256,512]{1,0:T(8,128)(2,1)S(1)}, bf16[256,512]{1,0:T(8,128)(2,1)S(1)}, u32[]{:S(2)}, u32[]{:S(2)}) collective-permute-start(bf16[256,512]{1,0:T(8,128)(2,1)S(1)} %get-tuple-element.75), channel_id=1, source_target_pairs={{8,0},{16,8},{24,16},{32,24},{40,32},{48,40},{56,48},{64,56},{72,6... | collective-permute-start | bytes 786440 | tf_op jit(solution)/shard_map/ppermute | solution.py:474
  26.2 8.4 %collective-permute-start.5 = (bf16[1024,256]{1,0:T(8,128)(2,1)S(1)}, bf16[1024,256]{1,0:T(8,128)(2,1)S(1)}, u32[]{:S(2)}, u32[]{:S(2)}) collective-permute-start(bf16[1024,256]{1,0:T(8,128)(2,1)S(1)} %get-tuple-element.77.swap_in), channel_id=1, source_target_pairs={{0,1},{1,0},{2,3},{3,2},{4,5},{5,4},{6,7},{7,6},{8,9},{9,8},{10,11... | collective-permute-start | bytes 1572872 | tf_op jit(solution)/shard_map/ppermute | solution.py:106
  29.9 12.7 %collective-permute-start.2 = (bf16[528,256]{1,0:T(8,128)(2,1)S(1)}, bf16[528,256]{1,0:T(8,128)(2,1)S(1)}, u32[]{:S(2)}, u32[]{:S(2)}) collective-permute-start(bf16[528,256]{1,0:T(8,128)(2,1)S(1)} %get-tuple-element.83), channel_id=1, source_target_pairs={{0,16},{8,24},{16,0},{24,8},{32,48},{40,56},{48,32},{56,40},{64,80... | collective-permute-start | bytes 811016 | tf_op jit(solution)/shard_map/ppermute | solution.py:97
  36.1 20.4 %collective-permute-start.6 = (bf16[512,512]{1,0:T(8,128)(2,1)S(1)}, bf16[512,512]{1,0:T(8,128)(2,1)S(1)}, u32[]{:S(2)}, u32[]{:S(2)}) collective-permute-start(bf16[512,512]{1,0:T(8,128)(2,1)S(1)} %get-tuple-element.87), channel_id=1, source_target_pairs={{0,16},{8,24},{16,0},{24,8},{32,48},{40,56},{48,32},{56,40},{64,80... | collective-permute-start | bytes 1572872 | tf_op jit(solution)/shard_map/ppermute | solution.py:97
  40.4 16.2 %collective-permute-start.7 = (bf16[512,512]{1,0:T(8,128)(2,1)S(1)}, bf16[512,512]{1,0:T(8,128)(2,1)S(1)}, u32[]{:S(2)}, u32[]{:S(2)}) collective-permute-start(bf16[512,512]{1,0:T(8,128)(2,1)S(1)} %get-tuple-element.88), channel_id=1, source_target_pairs={{0,8},{8,0},{16,24},{24,16},{32,40},{40,32},{48,56},{56,48},{64,72... | collective-permute-start | bytes 1572872 | tf_op jit(solution)/shard_map/ppermute | solution.py:97
  41.1 15.4 %collective-permute-start.8 = (bf16[512,512]{1,0:T(8,128)(2,1)S(1)}, bf16[512,512]{1,0:T(8,128)(2,1)S(1)}, u32[]{:S(2)}, u32[]{:S(2)}) collective-permute-start(bf16[512,512]{1,0:T(8,128)(2,1)S(1)} %get-tuple-element.89), channel_id=1, source_target_pairs={{0,24},{8,16},{16,8},{24,0},{32,56},{40,48},{48,40},{56,32},{64,88... | collective-permute-start | bytes 1572872 | tf_op jit(solution)/shard_map/ppermute | solution.py:97
  41.1 15.4 %collective-permute-start.3 = (bf16[528,256]{1,0:T(8,128)(2,1)S(1)}, bf16[528,256]{1,0:T(8,128)(2,1)S(1)}, u32[]{:S(2)}, u32[]{:S(2)}) collective-permute-start(bf16[528,256]{1,0:T(8,128)(2,1)S(1)} %get-tuple-element.84), channel_id=1, source_target_pairs={{0,8},{8,0},{16,24},{24,16},{32,40},{40,32},{48,56},{56,48},{64,72... | collective-permute-start | bytes 811016 | tf_op jit(solution)/shard_map/ppermute | solution.py:97
  42.6 14.0 %collective-permute-start.4 = (bf16[528,256]{1,0:T(8,128)(2,1)S(1)}, bf16[528,256]{1,0:T(8,128)(2,1)S(1)}, u32[]{:S(2)}, u32[]{:S(2)}) collective-permute-start(bf16[528,256]{1,0:T(8,128)(2,1)S(1)} %get-tuple-element.85), channel_id=1, source_target_pairs={{0,24},{8,16},{16,8},{24,0},{32,56},{40,48},{48,40},{56,32},{64,88... | collective-permute-start | bytes 811016 | tf_op jit(solution)/shard_map/ppermute | solution.py:97
  57.0 6.6 %collective-permute-start.9 = (bf16[144,768]{1,0:T(8,128)(2,1)S(1)}, bf16[144,768]{1,0:T(8,128)(2,1)S(1)}, u32[]{:S(2)}, u32[]{:S(2)}) collective-permute-start(bf16[144,768]{1,0:T(8,128)(2,1)S(1)} %get-tuple-element.92), channel_id=1, source_target_pairs={{0,64},{8,72},{16,80},{24,88},{32,224},{40,232},{48,240},{56,248},... | collective-permute-start | bytes 663560 | tf_op jit(solution)/shard_map/ppermute | solution.py:97
  60.1 5.3 %collective-permute-start.10 = (bf16[144,768]{1,0:T(8,128)(2,1)S(1)}, bf16[144,768]{1,0:T(8,128)(2,1)S(1)}, u32[]{:S(2)}, u32[]{:S(2)}) collective-permute-start(bf16[144,768]{1,0:T(8,128)(2,1)S(1)} %get-tuple-element.93), channel_id=1, source_target_pairs={{0,32},{8,40},{16,48},{24,56},{32,0},{40,8},{48,16},{56,24},{64,96... | collective-permute-start | bytes 663560 | tf_op jit(solution)/shard_map/ppermute | solution.py:97
  60.1 6.0 %collective-permute-start.11 = (bf16[144,768]{1,0:T(8,128)(2,1)S(1)}, bf16[144,768]{1,0:T(8,128)(2,1)S(1)}, u32[]{:S(2)}, u32[]{:S(2)}) collective-permute-start(bf16[144,768]{1,0:T(8,128)(2,1)S(1)} %get-tuple-element.94), channel_id=1, source_target_pairs={{0,224},{8,232},{16,240},{24,248},{32,64},{40,72},{48,80},{56,88},... | collective-permute-start | bytes 663560 | tf_op jit(solution)/shard_map/ppermute | solution.py:97
  66.2 14.7 %collective-permute-start.12 = (bf16[80,512]{1,0:T(8,128)(2,1)S(1)}, bf16[80,512]{1,0:T(8,128)(2,1)S(1)}, u32[]{:S(2)}, u32[]{:S(2)}) collective-permute-start(bf16[80,512]{1,0:T(8,128)(2,1)S(1)} %get-tuple-element.97), channel_id=1, source_target_pairs={{0,96},{8,104},{16,112},{24,120},{32,192},{40,200},{48,208},{56,21... | collective-permute-start | bytes 245768 | tf_op jit(solution)/shard_map/ppermute | solution.py:97
  69.8 11.2 %collective-permute-start.14 = (f32[64,256]{1,0:T(8,128)S(1)}, f32[64,256]{1,0:T(8,128)S(1)}, u32[]{:S(2)}, u32[]{:S(2)}) collective-permute-start(f32[64,256]{1,0:T(8,128)S(1)} %get-tuple-element.99), channel_id=1, source_target_pairs={{0,1},{1,0},{2,3},{3,2},{4,5},{5,4},{6,7},{7,6},{8,9},{9,8},{10,11... | collective-permute-start | bytes 196616 | tf_op jit(solution)/shard_map/ppermute | solution.py:106
  75.8 5.1 %collective-permute-start.13 = (bf16[64,256]{1,0:T(8,128)(2,1)S(1)}, bf16[64,256]{1,0:T(8,128)(2,1)S(1)}, u32[]{:S(2)}, u32[]{:S(2)}) collective-permute-start(bf16[64,256]{1,0:T(8,128)(2,1)S(1)} %get-tuple-element.98), channel_id=1, source_target_pairs={{0,97},{8,105},{16,113},{24,121},{32,193},{40,201},{48,209},{56,21... | collective-permute-start | bytes 98312 | tf_op jit(solution)/shard_map/ppermute | solution.py:97

commit v6 on v5

--- a/solution.py
+++ b/solution.py
@@ -126,22 +126,16 @@
     return score_grad, query_part, key_part, value_part
 
 
-def load_kernel(x_hbm, wq_hbm, wk_hbm, wv_hbm, tail_ref, x_ref, wq_ref, wk_ref, wv_ref, sem):
-    top = 1024 - REACH
-    pairs = (
-        (wk_hbm, wk_ref), (wv_hbm, wv_ref), (x_hbm.at[top:], x_ref.at[top:]),
-        (wq_hbm, wq_ref), (x_hbm.at[:top], x_ref.at[:top]),
-    )
+def load_kernel(x_hbm, wk_hbm, wv_hbm, tail_ref, wk_ref, wv_ref, x_s, sem):
+    pairs = ((wk_hbm, wk_ref), (x_hbm.at[1024 - REACH :], x_s), (wv_hbm, wv_ref))
     copies = [pltpu.make_async_copy(src, dst, sem.at[i]) for i, (src, dst) in enumerate(pairs)]
     for copy in copies:
         copy.start()
-    for copy in copies[:3]:
+    for copy in copies[:2]:
         copy.wait()
-    x = x_ref[top:]
-    tail_ref[:, :256] = dot(x, wk_ref[...]).astype(BF16)
-    tail_ref[:, 256:] = dot(x, wv_ref[...]).astype(BF16)
-    for copy in copies[3:]:
-        copy.wait()
+    tail_ref[:, :256] = dot(x_s[...], wk_ref[...]).astype(BF16)
+    copies[2].wait()
+    tail_ref[:, 256:] = dot(x_s[...], wv_ref[...]).astype(BF16)
 
 
 def proj_kernel(x_ref, wq_ref, wk_ref, wv_ref, q_ref, k_ref, v_ref):
@@ -478,12 +472,13 @@
     f32, b16 = (lambda *s: sds(s, F32)), (lambda *s: sds(s, BF16))
     v32, v16 = (lambda *s: pltpu.VMEM(s, F32)), (lambda *s: pltpu.VMEM(s, BF16))
     tile_flops = 6 * 2 * TILE * BAND * HDIM
-    in_hbm = tuple(pltpu.with_memory_space_constraint(v, pltpu.HBM) for v in (inputs, w_query, w_key, w_value))
-    tail, x, wq, wk, wv = call(
-        load_kernel, in_hbm,
-        (b16(REACH, 512), b16(1024, 2048), b16(2048, 256), b16(2048, 256), b16(2048, 256)),
-        (pltpu.SemaphoreType.DMA((5,)),), flops=2 * 256 * 2048 * 512, any_ins=(0, 1, 2, 3), limit=LOAD_LIMIT,
-    )
+    in_hbm = tuple(pltpu.with_memory_space_constraint(v, pltpu.HBM) for v in (inputs, w_key, w_value))
+    tail, wk, wv = call(
+        load_kernel, in_hbm, (b16(REACH, 512), b16(2048, 256), b16(2048, 256)),
+        (v16(REACH, 2048), pltpu.SemaphoreType.DMA((3,))), flops=2 * 256 * 2048 * 512, any_ins=(0, 1, 2),
+        limit=LOAD_LIMIT,
+    )
+    x, wq = inputs, w_query
     halo = neighbour(tail, 1)
     query, key, value = call(
         proj_kernel, (x, wq, wk, wv), (b16(1024, 256),) * 3,

time: 81.8 us -> 81.7 us (level)
  the two profiles are of different devices: /device:TPU:27 before, /device:TPU:3 now
where the time goes in v6:
time: 81.7 us; the launch traced here: 81.6 us
  starting transfers between devices  31.3 us (38%)
  waiting for transfers between devices  26.6 us (33%)
  Pallas kernels  22.9 us (28%)
  between operations  0.83 us (1%)
    pallas_call x13, Pallas kernels, call(): pl.pallas_call(kernel, grid=grid, in_specs=specs, out_specs=out_specs, ou...  22.9 us
    ppermute x11, waiting for transfers between devices, exchange(): return lax.ppermute(block, SP + ('core',), level_route(steps, across))  22.3 us
    ppermute x11, starting transfers between devices, exchange(): return lax.ppermute(block, SP + ('core',), level_route(steps, across))  18 us
    ppermute x2, starting transfers between devices, core_swap(): return lax.ppermute(block, 'core', [(0, 1), (1, 0)])  7.93 us
    ppermute x2, starting transfers between devices, neighbour(): return lax.ppermute(block, SP, route)  5.31 us
    ppermute x2, waiting for transfers between devices, neighbour(): return lax.ppermute(block, SP, route)  4.24 us
  transfers between devices with their start and end apart: 15, of which 6 were waited for; matrix products, arithmetic and copies ran while one was open for 0% of the time, Pallas kernels for 20%

profile of v6, /device:TPU:3, one launch (start us, length us, event | category | flops | bytes accessed | tf_op | source)
XLA Modules:
  0.0 81.6 jit_solution(2439305250379579616)
XLA Ops:
  0.6 0.0 copy-start
  0.6 0.0 copy-start.3
  0.7 3.1 %shard_map.117 = (bf16[256,512]{1,0:T(8,128)(2,1)S(1)}, bf16[2048,256]{1,0:T(8,128)(2,1)S(1)}, bf16[2048,256]{1,0:T(8,128)(2,1)S(1)}) custom-call(bf16[1024,2048]{1,0:T(8,128)(2,1)} %x_ref.7, bf16[2048,256]{1,0:T(8,128)(2,1)} %wk_hbm.1, bf16[2048,256]{1,0:T(8,128)(2,1)} %wv_hbm.1), custom_call_target="tpu_custom_call" | custom-call | flops 536870912 | bytes 8650752 | tf_op jit(solution)/shard_map/pallas_call | solution.py:453
  3.8 3.1 %collective-permute-start = (bf16[256,512]{1,0:T(8,128)(2,1)S(1)}, bf16[256,512]{1,0:T(8,128)(2,1)S(1)}, u32[]{:S(2)}, u32[]{:S(2)}) collective-permute-start(bf16[256,512]{1,0:T(8,128)(2,1)S(1)} %get-tuple-element.60), channel_id=1, source_target_pairs={{0,8},{8,16},{16,24},{24,32},{32,40},{40,48},{48,56},{56,64},{64,7... | collective-permute-start | bytes 786440 | tf_op jit(solution)/shard_map/ppermute | solution.py:468
  6.9 0.0 copy-done
  6.9 0.0 copy-done.3
  6.9 0.0 copy-start.1
  6.9 0.0 copy-start.2
  6.9 3.4 %shard_map.118 = (bf16[1024,256]{1,0:T(8,128)(2,1)S(1)}, bf16[1024,256]{1,0:T(8,128)(2,1)S(1)}, bf16[1024,256]{1,0:T(8,128)(2,1)S(1)}) custom-call(bf16[1024,2048]{1,0:T(8,128)(2,1)S(1)} %copy-done, bf16[2048,256]{1,0:T(8,128)(2,1)S(1)} %copy-done.3, bf16[2048,256]{1,0:T(8,128)(2,1)S(1)} %get-tuple-element.54.wk_ref, ...), custom_call_target="tpu_custom_call" | custom-call | flops 3221225472 | bytes 8912896 | tf_op jit(solution)/shard_map/pallas_call | solution.py:453
  10.3 0.0 copy-done.1
  10.4 0.0 copy-done.2
  10.4 4.4 %shard_map.119 = (bf16[512,256]{1,0:T(8,128)(2,1)S(1)}, f32[768,512]{1,0:T(8,128)S(1)}, f32[2,384,128]{2,1,0:T(8,128)S(1)}, f32[2,384,128]{2,1,0:T(8,128)S(1)}) custom-call(bf16[1024,256]{1,0:T(8,128)(2,1)S(1)} %get-tuple-element.56.q_ref, bf16[1024,256]{1,0:T(8,128)(2,1)S(1)} %get-tuple-element.57.k_ref, bf16[1024,256]{1,0:T(8,128)(2,1)S(1)} %get-tuple-element.58.v_ref, ...), custom_call_target="tpu_custom_call" | custom-call | flops 452984832 | bytes 4720648 | tf_op jit(solution)/shard_map/pallas_call | solution.py:453
  14.8 0.0 collective-permute-done.halo_ref
  14.8 2.3 %shard_map.120 = (bf16[256,256]{1,0:T(8,128)(2,1)S(1)}, f32[256,512]{1,0:T(8,128)S(1)}, bf16[256,512]{1,0:T(8,128)(2,1)S(1)}, f32[2,384,128]{2,1,0:T(8,128)S(1)}) custom-call(bf16[1024,256]{1,0:T(8,128)(2,1)S(1)} %get-tuple-element.56.q_ref, bf16[1024,256]{1,0:T(8,128)(2,1)S(1)} %get-tuple-element.57.k_ref, bf16[1024,256]{1,0:T(8,128)(2,1)S(1)} %get-tuple-element.58.v_ref, ...), custom_call_target="tpu_custom_call" | custom-call | flops 301989888 | bytes 4456448 | tf_op jit(solution)/shard_map/pallas_call | solution.py:453
  17.1 2.2 %collective-permute-start.1 = (bf16[256,512]{1,0:T(8,128)(2,1)S(1)}, bf16[256,512]{1,0:T(8,128)(2,1)S(1)}, u32[]{:S(2)}, u32[]{:S(2)}) collective-permute-start(bf16[256,512]{1,0:T(8,128)(2,1)S(1)} %get-tuple-element.71), channel_id=1, source_target_pairs={{8,0},{16,8},{24,16},{32,24},{40,32},{48,40},{56,48},{64,56},{72,6... | collective-permute-start | bytes 786440 | tf_op jit(solution)/shard_map/ppermute | solution.py:468
  19.3 2.4 %shard_map.121 = (bf16[1024,256]{1,0:T(8,128)(2,1)S(1)}, bf16[768,256]{1,0:T(8,128)(2,1)S(1)}, bf16[768,256]{1,0:T(8,128)(2,1)S(1)}, f32[256,512]{1,0:T(8,128)S(1)}, f32[2,384,128]{2,1,0:T(8,128)S(1)}) custom-call(bf16[1024,256]{1,0:T(8,128)(2,1)S(1)} %get-tuple-element.56.q_ref, bf16[1024,256]{1,0:T(8,128)(2,1)S(1)} %get-tuple-element.57.k_ref, ...), custom_call_target="tpu_custom_call" | custom-call | flops 452984832 | bytes 7602176 | tf_op jit(solution)/shard_map/pallas_call | solution.py:453
  21.7 4.2 %collective-permute-done.1.back_ref = bf16[256,512]{1,0:T(8,128)(2,1)S(1)} collective-permute-done((bf16[256,512]{1,0:T(8,128)(2,1)S(1)}, bf16[256,512]{1,0:T(8,128)(2,1)S(1)}, u32[]{:S(2)}, u32[]{:S(2)}) %collective-permute-start.1) | collective-permute-done | bytes 262176 | tf_op jit(solution)/shard_map/ppermute | solution.py:468
  25.9 0.1 shard_map.122
  26.0 1.9 %collective-permute-start.5 = (bf16[1024,256]{1,0:T(8,128)(2,1)S(1)}, bf16[1024,256]{1,0:T(8,128)(2,1)S(1)}, u32[]{:S(2)}, u32[]{:S(2)}) collective-permute-start(bf16[1024,256]{1,0:T(8,128)(2,1)S(1)} %get-tuple-element.73.swap_in), channel_id=1, source_target_pairs={{0,1},{1,0},{2,3},{3,2},{4,5},{5,4},{6,7},{7,6},{8,9},{9,8},{10,11... | collective-permute-start | bytes 1572872 | tf_op jit(solution)/shard_map/ppermute | solution.py:106
  28.0 1.9 %shard_map.124 = (bf16[528,256]{1,0:T(8,128)(2,1)S(1)}, bf16[528,256]{1,0:T(8,128)(2,1)S(1)}, bf16[528,256]{1,0:T(8,128)(2,1)S(1)}, bf16[512,256]{1,0:T(8,128)(2,1)S(1)}, f32[4,256]{1,0:T(4,128)S(1)}) custom-call(bf16[1024,2048]{1,0:T(8,128)(2,1)S(1)} %copy-done, bf16[1024,256]{1,0:T(8,128)(2,1)S(1)} %get-tuple-element.67.dq_in.grad_ref, ...), custom_call_target="tpu_custom_call" | custom-call | flops 1073741824 | bytes 6189056 | tf_op jit(solution)/shard_map/pallas_call | solution.py:453
  29.8 3.2 %collective-permute-start.2 = (bf16[528,256]{1,0:T(8,128)(2,1)S(1)}, bf16[528,256]{1,0:T(8,128)(2,1)S(1)}, u32[]{:S(2)}, u32[]{:S(2)}) collective-permute-start(bf16[528,256]{1,0:T(8,128)(2,1)S(1)} %get-tuple-element.79), channel_id=1, source_target_pairs={{0,16},{8,24},{16,0},{24,8},{32,48},{40,56},{48,32},{56,40},{64,80... | collective-permute-start | bytes 811016 | tf_op jit(solution)/shard_map/ppermute | solution.py:97
  33.1 1.3 %shard_map.125.own_hbm = bf16[2048,256]{1,0:T(8,128)(2,1)S(1)} custom-call(bf16[1024,2048]{1,0:T(8,128)(2,1)S(1)} %copy-done, bf16[1024,256]{1,0:T(8,128)(2,1)S(1)} %get-tuple-element.72.own_in.grad_ref), custom_call_target="tpu_custom_call" | custom-call | flops 1073741824 | bytes 5767168 | tf_op jit(solution)/shard_map/pallas_call | solution.py:453
  34.4 0.0 collective-permute-done.5.grad_ref
  34.4 1.6 %shard_map.126 = (bf16[512,512]{1,0:T(8,128)(2,1)S(1)}, bf16[512,512]{1,0:T(8,128)(2,1)S(1)}, bf16[512,512]{1,0:T(8,128)(2,1)S(1)}, bf16[512,512]{1,0:T(8,128)(2,1)S(1)}) custom-call(bf16[1024,2048]{1,0:T(8,128)(2,1)S(1)} %copy-done, bf16[1024,256]{1,0:T(8,128)(2,1)S(1)} %collective-permute-done.5.grad_ref, bf16[2048,256]{1,0:T(8,128)(2,1)S(1)} %shard_map.125.own_hbm), custom_call_target="tpu_custom_call" | custom-call | flops 1073741824 | bytes 7864320 | tf_op jit(solution)/shard_map/pallas_call | solution.py:453
  36.0 4.3 %collective-permute-start.6 = (bf16[512,512]{1,0:T(8,128)(2,1)S(1)}, bf16[512,512]{1,0:T(8,128)(2,1)S(1)}, u32[]{:S(2)}, u32[]{:S(2)}) collective-permute-start(bf16[512,512]{1,0:T(8,128)(2,1)S(1)} %get-tuple-element.83), channel_id=1, source_target_pairs={{0,16},{8,24},{16,0},{24,8},{32,48},{40,56},{48,32},{56,40},{64,80... | collective-permute-start | bytes 1572872 | tf_op jit(solution)/shard_map/ppermute | solution.py:97
  40.3 0.7 collective-permute-start.7
  41.0 0.0 collective-permute-start.8
  41.0 1.5 %collective-permute-start.3 = (bf16[528,256]{1,0:T(8,128)(2,1)S(1)}, bf16[528,256]{1,0:T(8,128)(2,1)S(1)}, u32[]{:S(2)}, u32[]{:S(2)}) collective-permute-start(bf16[528,256]{1,0:T(8,128)(2,1)S(1)} %get-tuple-element.80), channel_id=1, source_target_pairs={{0,8},{8,0},{16,24},{24,16},{32,40},{40,32},{48,56},{56,48},{64,72... | collective-permute-start | bytes 811016 | tf_op jit(solution)/shard_map/ppermute | solution.py:97
  42.5 0.0 collective-permute-done.2.a0
  42.5 1.2 %collective-permute-start.4 = (bf16[528,256]{1,0:T(8,128)(2,1)S(1)}, bf16[528,256]{1,0:T(8,128)(2,1)S(1)}, u32[]{:S(2)}, u32[]{:S(2)}) collective-permute-start(bf16[528,256]{1,0:T(8,128)(2,1)S(1)} %get-tuple-element.81), channel_id=1, source_target_pairs={{0,24},{8,16},{16,8},{24,0},{32,56},{40,48},{48,40},{56,32},{64,88... | collective-permute-start | bytes 811016 | tf_op jit(solution)/shard_map/ppermute | solution.py:97
  43.7 12.7 %collective-permute-done.3.a1 = bf16[528,256]{1,0:T(8,128)(2,1)S(1)} collective-permute-done((bf16[528,256]{1,0:T(8,128)(2,1)S(1)}, bf16[528,256]{1,0:T(8,128)(2,1)S(1)}, u32[]{:S(2)}, u32[]{:S(2)}) %collective-permute-start.3) | collective-permute-done | bytes 270368 | tf_op jit(solution)/shard_map/ppermute | solution.py:97
  56.5 0.0 collective-permute-done.4.a2
  56.5 0.0 collective-permute-done.6.b0
  56.5 0.0 collective-permute-done.7.b1
  56.5 0.0 collective-permute-done.8.b2
  56.5 0.4 shard_map.127
  56.9 3.2 %collective-permute-start.9 = (bf16[144,768]{1,0:T(8,128)(2,1)S(1)}, bf16[144,768]{1,0:T(8,128)(2,1)S(1)}, u32[]{:S(2)}, u32[]{:S(2)}) collective-permute-start(bf16[144,768]{1,0:T(8,128)(2,1)S(1)} %get-tuple-element.88), channel_id=1, source_target_pairs={{0,64},{8,72},{16,80},{24,88},{32,224},{40,232},{48,240},{56,248},... | collective-permute-start | bytes 663560 | tf_op jit(solution)/shard_map/ppermute | solution.py:97
  60.1 0.0 collective-permute-start.10
  60.1 0.4 collective-permute-start.11
  60.5 3.0 %collective-permute-done.9.g0 = bf16[144,768]{1,0:T(8,128)(2,1)S(1)} collective-permute-done((bf16[144,768]{1,0:T(8,128)(2,1)S(1)}, bf16[144,768]{1,0:T(8,128)(2,1)S(1)}, u32[]{:S(2)}, u32[]{:S(2)}) %collective-permute-start.9) | collective-permute-done | bytes 221216 | tf_op jit(solution)/shard_map/ppermute | solution.py:97
  63.5 1.9 %collective-permute-done.10.g1 = bf16[144,768]{1,0:T(8,128)(2,1)S(1)} collective-permute-done((bf16[144,768]{1,0:T(8,128)(2,1)S(1)}, bf16[144,768]{1,0:T(8,128)(2,1)S(1)}, u32[]{:S(2)}, u32[]{:S(2)}) %collective-permute-start.10) | collective-permute-done | bytes 221216 | tf_op jit(solution)/shard_map/ppermute | solution.py:97
  65.4 0.7 collective-permute-done.11.g2
  66.1 0.1 shard_map.128
  66.2 3.5 %collective-permute-start.12 = (bf16[80,512]{1,0:T(8,128)(2,1)S(1)}, bf16[80,512]{1,0:T(8,128)(2,1)S(1)}, u32[]{:S(2)}, u32[]{:S(2)}) collective-permute-start(bf16[80,512]{1,0:T(8,128)(2,1)S(1)} %get-tuple-element.93), channel_id=1, source_target_pairs={{0,96},{8,104},{16,112},{24,120},{32,192},{40,200},{48,208},{56,21... | collective-permute-start | bytes 245768 | tf_op jit(solution)/shard_map/ppermute | solution.py:97
  69.7 6.0 %collective-permute-start.14 = (f32[64,256]{1,0:T(8,128)S(1)}, f32[64,256]{1,0:T(8,128)S(1)}, u32[]{:S(2)}, u32[]{:S(2)}) collective-permute-start(f32[64,256]{1,0:T(8,128)S(1)} %get-tuple-element.95), channel_id=1, source_target_pairs={{0,1},{1,0},{2,3},{3,2},{4,5},{5,4},{6,7},{7,6},{8,9},{9,8},{10,11... | collective-permute-start | bytes 196616 | tf_op jit(solution)/shard_map/ppermute | solution.py:106
  75.7 0.0 collective-permute-start.13
  75.7 1.2 %shard_map.123 = (bf16[1024,256]{1,0:T(8,128)(2,1)}, bf16[1024,256]{1,0:T(8,128)(2,1)}, bf16[1024,256]{1,0:T(8,128)(2,1)}) custom-call(bf16[1024,256]{1,0:T(8,128)(2,1)S(1)} %get-tuple-element.67.dq_in.grad_ref, bf16[1024,256]{1,0:T(8,128)(2,1)S(1)} %get-tuple-element.72.own_in.grad_ref, bf16[1024,256]{1,0:T(8,128)(2,1)S(1)} %get-tuple-element.73.swap_in), custom_call_target="tpu_custom_call" | custom-call | flops 1048576 | bytes 3145728 | tf_op jit(solution)/shard_map/pallas_call | solution.py:453
  76.9 4.0 %collective-permute-done.13.two_ref = bf16[64,256]{1,0:T(8,128)(2,1)S(1)} collective-permute-done((bf16[64,256]{1,0:T(8,128)(2,1)S(1)}, bf16[64,256]{1,0:T(8,128)(2,1)S(1)}, u32[]{:S(2)}, u32[]{:S(2)}) %collective-permute-start.13) | collective-permute-done | bytes 32800 | tf_op jit(solution)/shard_map/ppermute | solution.py:97
  80.8 0.0 collective-permute-done.14.three_ref
  80.8 0.0 collective-permute-done.12.one_ref
  80.8 0.7 shard_map.129
Async XLA Ops:
  0.6 6.3 %copy-start = (bf16[1024,2048]{1,0:T(8,128)(2,1)S(1)}, bf16[1024,2048]{1,0:T(8,128)(2,1)}, u32[]{:S(2)}) copy-start(bf16[1024,2048]{1,0:T(8,128)(2,1)} %x_ref.7) | copy-start | bytes 12582916
  0.6 6.3 %copy-start.3 = (bf16[2048,256]{1,0:T(8,128)(2,1)S(1)}, bf16[2048,256]{1,0:T(8,128)(2,1)}, u32[]{:S(2)}) copy-start(bf16[2048,256]{1,0:T(8,128)(2,1)} %wq_ref.1) | copy-start | bytes 3145732
  3.8 11.0 %collective-permute-start = (bf16[256,512]{1,0:T(8,128)(2,1)S(1)}, bf16[256,512]{1,0:T(8,128)(2,1)S(1)}, u32[]{:S(2)}, u32[]{:S(2)}) collective-permute-start(bf16[256,512]{1,0:T(8,128)(2,1)S(1)} %get-tuple-element.60), channel_id=1, source_target_pairs={{0,8},{8,16},{16,24},{24,32},{32,40},{40,48},{48,56},{56,64},{64,7... | collective-permute-start | bytes 786440 | tf_op jit(solution)/shard_map/ppermute | solution.py:468
  6.9 3.4 %copy-start.1 = (bf16[1024,256]{1,0:T(8,128)(2,1)S(1)}, bf16[1024,256]{1,0:T(8,128)(2,1)}, u32[]{:S(2)}) copy-start(bf16[1024,256]{1,0:T(8,128)(2,1)} %og_ref.5) | copy-start | bytes 1572868
  6.9 3.4 %copy-start.2 = (f32[2,257]{1,0:T(2,128)S(1)}, f32[2,257]{1,0:T(2,128)}, u32[]{:S(2)}) copy-start(f32[2,257]{1,0:T(2,128)} %rel_ref.1) | copy-start | bytes 6172
  17.1 8.8 %collective-permute-start.1 = (bf16[256,512]{1,0:T(8,128)(2,1)S(1)}, bf16[256,512]{1,0:T(8,128)(2,1)S(1)}, u32[]{:S(2)}, u32[]{:S(2)}) collective-permute-start(bf16[256,512]{1,0:T(8,128)(2,1)S(1)} %get-tuple-element.71), channel_id=1, source_target_pairs={{8,0},{16,8},{24,16},{32,24},{40,32},{48,40},{56,48},{64,56},{72,6... | collective-permute-start | bytes 786440 | tf_op jit(solution)/shard_map/ppermute | solution.py:468
  26.0 8.4 %collective-permute-start.5 = (bf16[1024,256]{1,0:T(8,128)(2,1)S(1)}, bf16[1024,256]{1,0:T(8,128)(2,1)S(1)}, u32[]{:S(2)}, u32[]{:S(2)}) collective-permute-start(bf16[1024,256]{1,0:T(8,128)(2,1)S(1)} %get-tuple-element.73.swap_in), channel_id=1, source_target_pairs={{0,1},{1,0},{2,3},{3,2},{4,5},{5,4},{6,7},{7,6},{8,9},{9,8},{10,11... | collective-permute-start | bytes 1572872 | tf_op jit(solution)/shard_map/ppermute | solution.py:106
  29.8 12.7 %collective-permute-start.2 = (bf16[528,256]{1,0:T(8,128)(2,1)S(1)}, bf16[528,256]{1,0:T(8,128)(2,1)S(1)}, u32[]{:S(2)}, u32[]{:S(2)}) collective-permute-start(bf16[528,256]{1,0:T(8,128)(2,1)S(1)} %get-tuple-element.79), channel_id=1, source_target_pairs={{0,16},{8,24},{16,0},{24,8},{32,48},{40,56},{48,32},{56,40},{64,80... | collective-permute-start | bytes 811016 | tf_op jit(solution)/shard_map/ppermute | solution.py:97
  36.0 20.4 %collective-permute-start.6 = (bf16[512,512]{1,0:T(8,128)(2,1)S(1)}, bf16[512,512]{1,0:T(8,128)(2,1)S(1)}, u32[]{:S(2)}, u32[]{:S(2)}) collective-permute-start(bf16[512,512]{1,0:T(8,128)(2,1)S(1)} %get-tuple-element.83), channel_id=1, source_target_pairs={{0,16},{8,24},{16,0},{24,8},{32,48},{40,56},{48,32},{56,40},{64,80... | collective-permute-start | bytes 1572872 | tf_op jit(solution)/shard_map/ppermute | solution.py:97
  40.3 16.2 %collective-permute-start.7 = (bf16[512,512]{1,0:T(8,128)(2,1)S(1)}, bf16[512,512]{1,0:T(8,128)(2,1)S(1)}, u32[]{:S(2)}, u32[]{:S(2)}) collective-permute-start(bf16[512,512]{1,0:T(8,128)(2,1)S(1)} %get-tuple-element.84), channel_id=1, source_target_pairs={{0,8},{8,0},{16,24},{24,16},{32,40},{40,32},{48,56},{56,48},{64,72... | collective-permute-start | bytes 1572872 | tf_op jit(solution)/shard_map/ppermute | solution.py:97
  41.0 15.4 %collective-permute-start.8 = (bf16[512,512]{1,0:T(8,128)(2,1)S(1)}, bf16[512,512]{1,0:T(8,128)(2,1)S(1)}, u32[]{:S(2)}, u32[]{:S(2)}) collective-permute-start(bf16[512,512]{1,0:T(8,128)(2,1)S(1)} %get-tuple-element.85), channel_id=1, source_target_pairs={{0,24},{8,16},{16,8},{24,0},{32,56},{40,48},{48,40},{56,32},{64,88... | collective-permute-start | bytes 1572872 | tf_op jit(solution)/shard_map/ppermute | solution.py:97
  41.0 15.4 %collective-permute-start.3 = (bf16[528,256]{1,0:T(8,128)(2,1)S(1)}, bf16[528,256]{1,0:T(8,128)(2,1)S(1)}, u32[]{:S(2)}, u32[]{:S(2)}) collective-permute-start(bf16[528,256]{1,0:T(8,128)(2,1)S(1)} %get-tuple-element.80), channel_id=1, source_target_pairs={{0,8},{8,0},{16,24},{24,16},{32,40},{40,32},{48,56},{56,48},{64,72... | collective-permute-start | bytes 811016 | tf_op jit(solution)/shard_map/ppermute | solution.py:97
  42.5 13.9 %collective-permute-start.4 = (bf16[528,256]{1,0:T(8,128)(2,1)S(1)}, bf16[528,256]{1,0:T(8,128)(2,1)S(1)}, u32[]{:S(2)}, u32[]{:S(2)}) collective-permute-start(bf16[528,256]{1,0:T(8,128)(2,1)S(1)} %get-tuple-element.81), channel_id=1, source_target_pairs={{0,24},{8,16},{16,8},{24,0},{32,56},{40,48},{48,40},{56,32},{64,88... | collective-permute-start | bytes 811016 | tf_op jit(solution)/shard_map/ppermute | solution.py:97
  56.9 6.6 %collective-permute-start.9 = (bf16[144,768]{1,0:T(8,128)(2,1)S(1)}, bf16[144,768]{1,0:T(8,128)(2,1)S(1)}, u32[]{:S(2)}, u32[]{:S(2)}) collective-permute-start(bf16[144,768]{1,0:T(8,128)(2,1)S(1)} %get-tuple-element.88), channel_id=1, source_target_pairs={{0,64},{8,72},{16,80},{24,88},{32,224},{40,232},{48,240},{56,248},... | collective-permute-start | bytes 663560 | tf_op jit(solution)/shard_map/ppermute | solution.py:97
  60.1 5.3 %collective-permute-start.10 = (bf16[144,768]{1,0:T(8,128)(2,1)S(1)}, bf16[144,768]{1,0:T(8,128)(2,1)S(1)}, u32[]{:S(2)}, u32[]{:S(2)}) collective-permute-start(bf16[144,768]{1,0:T(8,128)(2,1)S(1)} %get-tuple-element.89), channel_id=1, source_target_pairs={{0,32},{8,40},{16,48},{24,56},{32,0},{40,8},{48,16},{56,24},{64,96... | collective-permute-start | bytes 663560 | tf_op jit(solution)/shard_map/ppermute | solution.py:97
  60.1 6.0 %collective-permute-start.11 = (bf16[144,768]{1,0:T(8,128)(2,1)S(1)}, bf16[144,768]{1,0:T(8,128)(2,1)S(1)}, u32[]{:S(2)}, u32[]{:S(2)}) collective-permute-start(bf16[144,768]{1,0:T(8,128)(2,1)S(1)} %get-tuple-element.90), channel_id=1, source_target_pairs={{0,224},{8,232},{16,240},{24,248},{32,64},{40,72},{48,80},{56,88},... | collective-permute-start | bytes 663560 | tf_op jit(solution)/shard_map/ppermute | solution.py:97
  66.2 14.7 %collective-permute-start.12 = (bf16[80,512]{1,0:T(8,128)(2,1)S(1)}, bf16[80,512]{1,0:T(8,128)(2,1)S(1)}, u32[]{:S(2)}, u32[]{:S(2)}) collective-permute-start(bf16[80,512]{1,0:T(8,128)(2,1)S(1)} %get-tuple-element.93), channel_id=1, source_target_pairs={{0,96},{8,104},{16,112},{24,120},{32,192},{40,200},{48,208},{56,21... | collective-permute-start | bytes 245768 | tf_op jit(solution)/shard_map/ppermute | solution.py:97
  69.7 11.2 %collective-permute-start.14 = (f32[64,256]{1,0:T(8,128)S(1)}, f32[64,256]{1,0:T(8,128)S(1)}, u32[]{:S(2)}, u32[]{:S(2)}) collective-permute-start(f32[64,256]{1,0:T(8,128)S(1)} %get-tuple-element.95), channel_id=1, source_target_pairs={{0,1},{1,0},{2,3},{3,2},{4,5},{5,4},{6,7},{7,6},{8,9},{9,8},{10,11... | collective-permute-start | bytes 196616 | tf_op jit(solution)/shard_map/ppermute | solution.py:106
  75.7 5.1 %collective-permute-start.13 = (bf16[64,256]{1,0:T(8,128)(2,1)S(1)}, bf16[64,256]{1,0:T(8,128)(2,1)S(1)}, u32[]{:S(2)}, u32[]{:S(2)}) collective-permute-start(bf16[64,256]{1,0:T(8,128)(2,1)S(1)} %get-tuple-element.94), channel_id=1, source_target_pairs={{0,97},{8,105},{16,113},{24,121},{32,193},{40,201},{48,209},{56,21... | collective-permute-start | bytes 98312 | tf_op jit(solution)/shard_map/ppermute | solution.py:97

commit v7 on v6

--- a/solution.py
+++ b/solution.py
@@ -17,9 +17,8 @@
 NZ, NX = 8, 4
 ROWS = 64
 EXTRA = 16
-LATE = 256
+LATE = 384
 VMEM_LIMIT = 24 << 20
-LOAD_LIMIT = 24 << 20
 CHUNKS = 4
 WIDTH = 2048 // CHUNKS
 SCALE = HDIM ** (-0.5)
@@ -126,23 +125,35 @@
     return score_grad, query_part, key_part, value_part
 
 
-def load_kernel(x_hbm, wk_hbm, wv_hbm, tail_ref, wk_ref, wv_ref, x_s, sem):
-    pairs = ((wk_hbm, wk_ref), (x_hbm.at[1024 - REACH :], x_s), (wv_hbm, wv_ref))
+def load_kernel(x_hbm, wk_hbm, wv_hbm, tail_ref, wk_ref, wv_ref, x_ref, sem):
+    pairs = ((wk_hbm, wk_ref), (x_hbm.at[1024 - REACH :], x_ref), (wv_hbm, wv_ref))
     copies = [pltpu.make_async_copy(src, dst, sem.at[i]) for i, (src, dst) in enumerate(pairs)]
     for copy in copies:
         copy.start()
     for copy in copies[:2]:
         copy.wait()
-    tail_ref[:, :256] = dot(x_s[...], wk_ref[...]).astype(BF16)
+    tail_ref[:, :256] = dot(x_ref[...], wk_ref[...]).astype(BF16)
     copies[2].wait()
-    tail_ref[:, 256:] = dot(x_s[...], wv_ref[...]).astype(BF16)
-
-
-def proj_kernel(x_ref, wq_ref, wk_ref, wv_ref, q_ref, k_ref, v_ref):
-    x = x_ref[...]
-    q_ref[...] = dot(x, wq_ref[...]).astype(BF16)
-    k_ref[...] = dot(x, wk_ref[...]).astype(BF16)
-    v_ref[...] = dot(x, wv_ref[...]).astype(BF16)
+    tail_ref[:, 256:] = dot(x_ref[...], wv_ref[...]).astype(BF16)
+
+
+def proj_kernel(x_hbm, wq_hbm, wk_ref, wv_ref, x_tail, tail_ref, q_ref, k_ref, v_ref, x_ref, wq_s, sem):
+    top = 1024 - REACH
+    pairs = [(x_hbm.at[c : c + REACH], x_ref.at[c : c + REACH]) for c in range(0, top, REACH)]
+    pairs += [(wq_hbm, wq_s)]
+    copies = [pltpu.make_async_copy(src, dst, sem.at[i]) for i, (src, dst) in enumerate(pairs)]
+    for copy in copies:
+        copy.start()
+    x_ref[top:] = x_tail[...]
+    k_ref[top:] = tail_ref[:, :256]
+    v_ref[top:] = tail_ref[:, 256:]
+    for i, c in enumerate(range(0, top, REACH)):
+        copies[i].wait()
+        x = x_ref[c : c + REACH]
+        k_ref[c : c + REACH] = dot(x, wk_ref[...]).astype(BF16)
+        v_ref[c : c + REACH] = dot(x, wv_ref[...]).astype(BF16)
+    copies[-1].wait()
+    q_ref[...] = dot(x_ref[...], wq_s[...]).astype(BF16)
 
 
 def tiles(which, q_ref, k_ref, v_ref, og_ref, bias_ref, kt_s, vt_s, pat_ref, dq_ref, dq_at, ka_s, va_s, acc_at):
@@ -235,6 +246,9 @@
     vt_s[...] = v_ref[: LATE + REACH].T
     ka_s[:REACH] = edge_in[:, :256]
     va_s[:REACH] = edge_in[:, 256:]
+    if LATE > REACH:
+        ka_s[REACH:LATE] = jnp.zeros((LATE - REACH, 256), F32)
+        va_s[REACH:LATE] = jnp.zeros((LATE - REACH, 256), F32)
     ka_s[LATE:] = acc_in[: LATE + REACH - LATE, :256]
     va_s[LATE:] = acc_in[: LATE + REACH - LATE, 256:]
     pat_ref[...] = pat_in[...]
@@ -472,17 +486,20 @@
     f32, b16 = (lambda *s: sds(s, F32)), (lambda *s: sds(s, BF16))
     v32, v16 = (lambda *s: pltpu.VMEM(s, F32)), (lambda *s: pltpu.VMEM(s, BF16))
     tile_flops = 6 * 2 * TILE * BAND * HDIM
-    in_hbm = tuple(pltpu.with_memory_space_constraint(v, pltpu.HBM) for v in (inputs, w_key, w_value))
-    tail, wk, wv = call(
-        load_kernel, in_hbm, (b16(REACH, 512), b16(2048, 256), b16(2048, 256)),
-        (v16(REACH, 2048), pltpu.SemaphoreType.DMA((3,))), flops=2 * 256 * 2048 * 512, any_ins=(0, 1, 2),
-        limit=LOAD_LIMIT,
-    )
-    x, wq = inputs, w_query
+    x_hbm, wq_hbm, wk_hbm, wv_hbm = (
+        pltpu.with_memory_space_constraint(v, pltpu.HBM) for v in (inputs, w_query, w_key, w_value)
+    )
+    dma = pltpu.SemaphoreType.DMA
+    tail, wk, wv, x_tail = call(
+        load_kernel, (x_hbm, wk_hbm, wv_hbm),
+        (b16(REACH, 512), b16(2048, 256), b16(2048, 256), b16(REACH, 2048)),
+        (dma((3,)),), flops=2 * 256 * 2048 * 512, any_ins=(0, 1, 2),
+    )
     halo = neighbour(tail, 1)
-    query, key, value = call(
-        proj_kernel, (x, wq, wk, wv), (b16(1024, 256),) * 3,
-        flops=2 * 1024 * 2048 * 768,
+    query, key, value, x = call(
+        proj_kernel, (x_hbm, wq_hbm, wk, wv, x_tail, tail),
+        (b16(1024, 256),) * 3 + (b16(1024, 2048),), (v16(2048, 256), dma((4,))),
+        flops=2 * 1024 * 2048 * 768, any_ins=(0, 1),
     )
     block = (REACH, 256)
     span = 1024 - LATE
@@ -505,7 +522,6 @@
         (v16(256, LATE + REACH), v16(256, LATE + REACH), v32(LATE + REACH, 256), v32(LATE + REACH, 256)), flops=6 * tile_flops,
     )
     product = 2 * 1024 * 2048 * 256
-    dma = pltpu.SemaphoreType.DMA
     *send, keep, table = call(
         query_kernel, (x, dq, pat), (b16(512 + EXTRA, 256),) * 3 + (b16(512, 256), f32(4, 256)),
         (v16(2048, 256), v16(EXTRA, 256), v32(8, 640), dma((7,))), flops=product, any_outs=(0, 1, 2, 3),

time: 81.7 us -> 81.8 us (level)
  the two profiles are of different devices: /device:TPU:3 before, /device:TPU:11 now
where the time goes in v7:
time: 81.8 us; the launch traced here: 81.7 us
  starting transfers between devices  31.2 us (38%)
  waiting for transfers between devices  25.6 us (31%)
  Pallas kernels  24.1 us (29%)
    pallas_call x13, Pallas kernels, call(): pl.pallas_call(kernel, grid=grid, in_specs=specs, out_specs=out_specs, ou...  24.1 us
    ppermute x11, waiting for transfers between devices, exchange(): return lax.ppermute(block, SP + ('core',), level_route(steps, across))  22.3 us
    ppermute x11, starting transfers between devices, exchange(): return lax.ppermute(block, SP + ('core',), level_route(steps, across))  18 us
    ppermute x2, starting transfers between devices, core_swap(): return lax.ppermute(block, 'core', [(0, 1), (1, 0)])  7.92 us
    ppermute x2, starting transfers between devices, neighbour(): return lax.ppermute(block, SP, route)  5.29 us
    ppermute x2, waiting for transfers between devices, neighbour(): return lax.ppermute(block, SP, route)  3.24 us
  transfers between devices with their start and end apart: 15, of which 6 were waited for; matrix products, arithmetic and copies ran while one was open for 0% of the time, Pallas kernels for 21%

profile of v7, /device:TPU:11, one launch (start us, length us, event | category | flops | bytes accessed | tf_op | source)
XLA Modules:
  0.0 81.7 jit_solution(11150809081592389486)
XLA Ops:
  0.6 2.9 %shard_map.117 = (bf16[256,512]{1,0:T(8,128)(2,1)S(1)}, bf16[2048,256]{1,0:T(8,128)(2,1)S(1)}, bf16[2048,256]{1,0:T(8,128)(2,1)S(1)}, bf16[256,2048]{1,0:T(8,128)(2,1)S(1)}) custom-call(bf16[1024,2048]{1,0:T(8,128)(2,1)} %x_hbm.3, bf16[2048,256]{1,0:T(8,128)(2,1)} %wk_hbm.1, bf16[2048,256]{1,0:T(8,128)(2,1)} %wv_hbm.1), custom_call_target="tpu_custom_call" | custom-call | flops 536870912 | bytes 9699328 | tf_op jit(solution)/shard_map/pallas_call | solution.py:467
  3.6 3.1 %collective-permute-start = (bf16[256,512]{1,0:T(8,128)(2,1)S(1)}, bf16[256,512]{1,0:T(8,128)(2,1)S(1)}, u32[]{:S(2)}, u32[]{:S(2)}) collective-permute-start(bf16[256,512]{1,0:T(8,128)(2,1)S(1)} %get-tuple-element.59.tail_ref), channel_id=1, source_target_pairs={{0,8},{8,16},{16,24},{24,32},{32,40},{40,48},{48,56},{56,64},{64,7... | collective-permute-start | bytes 786440 | tf_op jit(solution)/shard_map/ppermute | solution.py:482
  6.7 0.0 copy-start
  6.7 0.0 copy-start.1
  6.7 4.7 %shard_map.118 = (bf16[1024,256]{1,0:T(8,128)(2,1)S(1)}, bf16[1024,256]{1,0:T(8,128)(2,1)S(1)}, bf16[1024,256]{1,0:T(8,128)(2,1)S(1)}, bf16[1024,2048]{1,0:T(8,128)(2,1)S(1)}) custom-call(bf16[1024,2048]{1,0:T(8,128)(2,1)} %x_hbm.3, bf16[2048,256]{1,0:T(8,128)(2,1)} %wq_hbm.1, bf16[2048,256]{1,0:T(8,128)(2,1)S(1)} %get-tuple-element.56.wk_ref, ...), custom_call_target="tpu_custom_call" | custom-call | flops 3221225472 | bytes 14417920 | tf_op jit(solution)/shard_map/pallas_call | solution.py:467
  11.4 0.0 copy-done
  11.5 0.0 copy-done.1
  11.5 3.4 %shard_map.119 = (bf16[384,256]{1,0:T(8,128)(2,1)S(1)}, f32[640,512]{1,0:T(8,128)S(1)}, f32[2,384,128]{2,1,0:T(8,128)S(1)}, f32[2,384,128]{2,1,0:T(8,128)S(1)}) custom-call(bf16[1024,256]{1,0:T(8,128)(2,1)S(1)} %get-tuple-element.60.q_ref, bf16[1024,256]{1,0:T(8,128)(2,1)S(1)} %get-tuple-element.61.k_ref, bf16[1024,256]{1,0:T(8,128)(2,1)S(1)} %get-tuple-element.62.v_ref, ...), custom_call_target="tpu_custom_call" | custom-call | flops 452984832 | bytes 4392968 | tf_op jit(solution)/shard_map/pallas_call | solution.py:467
  14.9 0.0 collective-permute-done.halo_ref
  14.9 2.3 %shard_map.120 = (bf16[256,256]{1,0:T(8,128)(2,1)S(1)}, f32[256,512]{1,0:T(8,128)S(1)}, bf16[256,512]{1,0:T(8,128)(2,1)S(1)}, f32[2,384,128]{2,1,0:T(8,128)S(1)}) custom-call(bf16[1024,256]{1,0:T(8,128)(2,1)S(1)} %get-tuple-element.60.q_ref, bf16[1024,256]{1,0:T(8,128)(2,1)S(1)} %get-tuple-element.61.k_ref, bf16[1024,256]{1,0:T(8,128)(2,1)S(1)} %get-tuple-element.62.v_ref, ...), custom_call_target="tpu_custom_call" | custom-call | flops 301989888 | bytes 4456448 | tf_op jit(solution)/shard_map/pallas_call | solution.py:467
  17.2 2.2 %collective-permute-start.1 = (bf16[256,512]{1,0:T(8,128)(2,1)S(1)}, bf16[256,512]{1,0:T(8,128)(2,1)S(1)}, u32[]{:S(2)}, u32[]{:S(2)}) collective-permute-start(bf16[256,512]{1,0:T(8,128)(2,1)S(1)} %get-tuple-element.74), channel_id=1, source_target_pairs={{8,0},{16,8},{24,16},{32,24},{40,32},{48,40},{56,48},{64,56},{72,6... | collective-permute-start | bytes 786440 | tf_op jit(solution)/shard_map/ppermute | solution.py:482
  19.4 3.4 %shard_map.121 = (bf16[1024,256]{1,0:T(8,128)(2,1)S(1)}, bf16[768,256]{1,0:T(8,128)(2,1)S(1)}, bf16[768,256]{1,0:T(8,128)(2,1)S(1)}, f32[256,512]{1,0:T(8,128)S(1)}, f32[2,384,128]{2,1,0:T(8,128)S(1)}) custom-call(bf16[1024,256]{1,0:T(8,128)(2,1)S(1)} %get-tuple-element.60.q_ref, bf16[1024,256]{1,0:T(8,128)(2,1)S(1)} %get-tuple-element.61.k_ref, ...), custom_call_target="tpu_custom_call" | custom-call | flops 452984832 | bytes 7274496 | tf_op jit(solution)/shard_map/pallas_call | solution.py:467
  22.8 3.2 %collective-permute-done.1.back_ref = bf16[256,512]{1,0:T(8,128)(2,1)S(1)} collective-permute-done((bf16[256,512]{1,0:T(8,128)(2,1)S(1)}, bf16[256,512]{1,0:T(8,128)(2,1)S(1)}, u32[]{:S(2)}, u32[]{:S(2)}) %collective-permute-start.1) | collective-permute-done | bytes 262176 | tf_op jit(solution)/shard_map/ppermute | solution.py:482
  26.0 0.1 shard_map.122
  26.1 1.9 %collective-permute-start.5 = (bf16[1024,256]{1,0:T(8,128)(2,1)S(1)}, bf16[1024,256]{1,0:T(8,128)(2,1)S(1)}, u32[]{:S(2)}, u32[]{:S(2)}) collective-permute-start(bf16[1024,256]{1,0:T(8,128)(2,1)S(1)} %get-tuple-element.76.swap_in), channel_id=1, source_target_pairs={{0,1},{1,0},{2,3},{3,2},{4,5},{5,4},{6,7},{7,6},{8,9},{9,8},{10,11... | collective-permute-start | bytes 1572872 | tf_op jit(solution)/shard_map/ppermute | solution.py:105
  28.0 1.9 %shard_map.124 = (bf16[528,256]{1,0:T(8,128)(2,1)S(1)}, bf16[528,256]{1,0:T(8,128)(2,1)S(1)}, bf16[528,256]{1,0:T(8,128)(2,1)S(1)}, bf16[512,256]{1,0:T(8,128)(2,1)S(1)}, f32[4,256]{1,0:T(4,128)S(1)}) custom-call(bf16[1024,2048]{1,0:T(8,128)(2,1)S(1)} %get-tuple-element.80.x_ref, bf16[1024,256]{1,0:T(8,128)(2,1)S(1)} %get-tuple-element.70.dq_in.grad_ref, ...), custom_call_target="tpu_custom_call" | custom-call | flops 1073741824 | bytes 6189056 | tf_op jit(solution)/shard_map/pallas_call | solution.py:467
  29.9 3.2 %collective-permute-start.2 = (bf16[528,256]{1,0:T(8,128)(2,1)S(1)}, bf16[528,256]{1,0:T(8,128)(2,1)S(1)}, u32[]{:S(2)}, u32[]{:S(2)}) collective-permute-start(bf16[528,256]{1,0:T(8,128)(2,1)S(1)} %get-tuple-element.83), channel_id=1, source_target_pairs={{0,16},{8,24},{16,0},{24,8},{32,48},{40,56},{48,32},{56,40},{64,80... | collective-permute-start | bytes 811016 | tf_op jit(solution)/shard_map/ppermute | solution.py:96
  33.2 1.4 %shard_map.125.own_hbm = bf16[2048,256]{1,0:T(8,128)(2,1)S(1)} custom-call(bf16[1024,2048]{1,0:T(8,128)(2,1)S(1)} %get-tuple-element.80.x_ref, bf16[1024,256]{1,0:T(8,128)(2,1)S(1)} %get-tuple-element.75.own_in.grad_ref), custom_call_target="tpu_custom_call" | custom-call | flops 1073741824 | bytes 5767168 | tf_op jit(solution)/shard_map/pallas_call | solution.py:467
  34.5 0.0 collective-permute-done.5.grad_ref
  34.5 1.6 %shard_map.126 = (bf16[512,512]{1,0:T(8,128)(2,1)S(1)}, bf16[512,512]{1,0:T(8,128)(2,1)S(1)}, bf16[512,512]{1,0:T(8,128)(2,1)S(1)}, bf16[512,512]{1,0:T(8,128)(2,1)S(1)}) custom-call(bf16[1024,2048]{1,0:T(8,128)(2,1)S(1)} %get-tuple-element.80.x_ref, bf16[1024,256]{1,0:T(8,128)(2,1)S(1)} %collective-permute-done.5.grad_ref, ...), custom_call_target="tpu_custom_call" | custom-call | flops 1073741824 | bytes 7864320 | tf_op jit(solution)/shard_map/pallas_call | solution.py:467
  36.1 4.3 %collective-permute-start.6 = (bf16[512,512]{1,0:T(8,128)(2,1)S(1)}, bf16[512,512]{1,0:T(8,128)(2,1)S(1)}, u32[]{:S(2)}, u32[]{:S(2)}) collective-permute-start(bf16[512,512]{1,0:T(8,128)(2,1)S(1)} %get-tuple-element.87), channel_id=1, source_target_pairs={{0,16},{8,24},{16,0},{24,8},{32,48},{40,56},{48,32},{56,40},{64,80... | collective-permute-start | bytes 1572872 | tf_op jit(solution)/shard_map/ppermute | solution.py:96
  40.4 0.7 collective-permute-start.7
  41.2 0.0 collective-permute-start.8
  41.2 1.5 %collective-permute-start.3 = (bf16[528,256]{1,0:T(8,128)(2,1)S(1)}, bf16[528,256]{1,0:T(8,128)(2,1)S(1)}, u32[]{:S(2)}, u32[]{:S(2)}) collective-permute-start(bf16[528,256]{1,0:T(8,128)(2,1)S(1)} %get-tuple-element.84), channel_id=1, source_target_pairs={{0,8},{8,0},{16,24},{24,16},{32,40},{40,32},{48,56},{56,48},{64,72... | collective-permute-start | bytes 811016 | tf_op jit(solution)/shard_map/ppermute | solution.py:96
  42.6 0.0 collective-permute-done.2.a0
  42.6 1.2 %collective-permute-start.4 = (bf16[528,256]{1,0:T(8,128)(2,1)S(1)}, bf16[528,256]{1,0:T(8,128)(2,1)S(1)}, u32[]{:S(2)}, u32[]{:S(2)}) collective-permute-start(bf16[528,256]{1,0:T(8,128)(2,1)S(1)} %get-tuple-element.85), channel_id=1, source_target_pairs={{0,24},{8,16},{16,8},{24,0},{32,56},{40,48},{48,40},{56,32},{64,88... | collective-permute-start | bytes 811016 | tf_op jit(solution)/shard_map/ppermute | solution.py:96
  43.8 12.7 %collective-permute-done.3.a1 = bf16[528,256]{1,0:T(8,128)(2,1)S(1)} collective-permute-done((bf16[528,256]{1,0:T(8,128)(2,1)S(1)}, bf16[528,256]{1,0:T(8,128)(2,1)S(1)}, u32[]{:S(2)}, u32[]{:S(2)}) %collective-permute-start.3) | collective-permute-done | bytes 270368 | tf_op jit(solution)/shard_map/ppermute | solution.py:96
  56.6 0.0 collective-permute-done.4.a2
  56.6 0.0 collective-permute-done.6.b0
  56.6 0.0 collective-permute-done.7.b1
  56.6 0.0 collective-permute-done.8.b2
  56.6 0.4 shard_map.127
  57.0 3.2 %collective-permute-start.9 = (bf16[144,768]{1,0:T(8,128)(2,1)S(1)}, bf16[144,768]{1,0:T(8,128)(2,1)S(1)}, u32[]{:S(2)}, u32[]{:S(2)}) collective-permute-start(bf16[144,768]{1,0:T(8,128)(2,1)S(1)} %get-tuple-element.92), channel_id=1, source_target_pairs={{0,64},{8,72},{16,80},{24,88},{32,224},{40,232},{48,240},{56,248},... | collective-permute-start | bytes 663560 | tf_op jit(solution)/shard_map/ppermute | solution.py:96
  60.2 0.0 collective-permute-start.10
  60.2 0.4 collective-permute-start.11
  60.6 3.0 %collective-permute-done.9.g0 = bf16[144,768]{1,0:T(8,128)(2,1)S(1)} collective-permute-done((bf16[144,768]{1,0:T(8,128)(2,1)S(1)}, bf16[144,768]{1,0:T(8,128)(2,1)S(1)}, u32[]{:S(2)}, u32[]{:S(2)}) %collective-permute-start.9) | collective-permute-done | bytes 221216 | tf_op jit(solution)/shard_map/ppermute | solution.py:96
  63.6 1.9 %collective-permute-done.10.g1 = bf16[144,768]{1,0:T(8,128)(2,1)S(1)} collective-permute-done((bf16[144,768]{1,0:T(8,128)(2,1)S(1)}, bf16[144,768]{1,0:T(8,128)(2,1)S(1)}, u32[]{:S(2)}, u32[]{:S(2)}) %collective-permute-start.10) | collective-permute-done | bytes 221216 | tf_op jit(solution)/shard_map/ppermute | solution.py:96
  65.5 0.7 collective-permute-done.11.g2
  66.2 0.1 shard_map.128
  66.3 3.5 %collective-permute-start.12 = (bf16[80,512]{1,0:T(8,128)(2,1)S(1)}, bf16[80,512]{1,0:T(8,128)(2,1)S(1)}, u32[]{:S(2)}, u32[]{:S(2)}) collective-permute-start(bf16[80,512]{1,0:T(8,128)(2,1)S(1)} %get-tuple-element.97), channel_id=1, source_target_pairs={{0,96},{8,104},{16,112},{24,120},{32,192},{40,200},{48,208},{56,21... | collective-permute-start | bytes 245768 | tf_op jit(solution)/shard_map/ppermute | solution.py:96
  69.8 6.0 %collective-permute-start.14 = (f32[64,256]{1,0:T(8,128)S(1)}, f32[64,256]{1,0:T(8,128)S(1)}, u32[]{:S(2)}, u32[]{:S(2)}) collective-permute-start(f32[64,256]{1,0:T(8,128)S(1)} %get-tuple-element.99), channel_id=1, source_target_pairs={{0,1},{1,0},{2,3},{3,2},{4,5},{5,4},{6,7},{7,6},{8,9},{9,8},{10,11... | collective-permute-start | bytes 196616 | tf_op jit(solution)/shard_map/ppermute | solution.py:105
  75.8 0.0 collective-permute-start.13
  75.8 1.2 %shard_map.123 = (bf16[1024,256]{1,0:T(8,128)(2,1)}, bf16[1024,256]{1,0:T(8,128)(2,1)}, bf16[1024,256]{1,0:T(8,128)(2,1)}) custom-call(bf16[1024,256]{1,0:T(8,128)(2,1)S(1)} %get-tuple-element.70.dq_in.grad_ref, bf16[1024,256]{1,0:T(8,128)(2,1)S(1)} %get-tuple-element.75.own_in.grad_ref, bf16[1024,256]{1,0:T(8,128)(2,1)S(1)} %get-tuple-element.76.swap_in), custom_call_target="tpu_custom_call" | custom-call | flops 1048576 | bytes 3145728 | tf_op jit(solution)/shard_map/pallas_call | solution.py:467
  77.0 4.0 %collective-permute-done.13.two_ref = bf16[64,256]{1,0:T(8,128)(2,1)S(1)} collective-permute-done((bf16[64,256]{1,0:T(8,128)(2,1)S(1)}, bf16[64,256]{1,0:T(8,128)(2,1)S(1)}, u32[]{:S(2)}, u32[]{:S(2)}) %collective-permute-start.13) | collective-permute-done | bytes 32800 | tf_op jit(solution)/shard_map/ppermute | solution.py:96
  81.0 0.0 collective-permute-done.14.three_ref
  81.0 0.0 collective-permute-done.12.one_ref
  81.0 0.7 shard_map.129
Async XLA Ops:
  3.6 11.3 %collective-permute-start = (bf16[256,512]{1,0:T(8,128)(2,1)S(1)}, bf16[256,512]{1,0:T(8,128)(2,1)S(1)}, u32[]{:S(2)}, u32[]{:S(2)}) collective-permute-start(bf16[256,512]{1,0:T(8,128)(2,1)S(1)} %get-tuple-element.59.tail_ref), channel_id=1, source_target_pairs={{0,8},{8,16},{16,24},{24,32},{32,40},{40,48},{48,56},{56,64},{64,7... | collective-permute-start | bytes 786440 | tf_op jit(solution)/shard_map/ppermute | solution.py:482
  6.7 4.7 %copy-start = (bf16[1024,256]{1,0:T(8,128)(2,1)S(1)}, bf16[1024,256]{1,0:T(8,128)(2,1)}, u32[]{:S(2)}) copy-start(bf16[1024,256]{1,0:T(8,128)(2,1)} %og_ref.5) | copy-start | bytes 1572868
  6.7 4.7 %copy-start.1 = (f32[2,257]{1,0:T(2,128)S(1)}, f32[2,257]{1,0:T(2,128)}, u32[]{:S(2)}) copy-start(f32[2,257]{1,0:T(2,128)} %rel_ref.1) | copy-start | bytes 6172
  17.2 8.8 %collective-permute-start.1 = (bf16[256,512]{1,0:T(8,128)(2,1)S(1)}, bf16[256,512]{1,0:T(8,128)(2,1)S(1)}, u32[]{:S(2)}, u32[]{:S(2)}) collective-permute-start(bf16[256,512]{1,0:T(8,128)(2,1)S(1)} %get-tuple-element.74), channel_id=1, source_target_pairs={{8,0},{16,8},{24,16},{32,24},{40,32},{48,40},{56,48},{64,56},{72,6... | collective-permute-start | bytes 786440 | tf_op jit(solution)/shard_map/ppermute | solution.py:482
  26.1 8.4 %collective-permute-start.5 = (bf16[1024,256]{1,0:T(8,128)(2,1)S(1)}, bf16[1024,256]{1,0:T(8,128)(2,1)S(1)}, u32[]{:S(2)}, u32[]{:S(2)}) collective-permute-start(bf16[1024,256]{1,0:T(8,128)(2,1)S(1)} %get-tuple-element.76.swap_in), channel_id=1, source_target_pairs={{0,1},{1,0},{2,3},{3,2},{4,5},{5,4},{6,7},{7,6},{8,9},{9,8},{10,11... | collective-permute-start | bytes 1572872 | tf_op jit(solution)/shard_map/ppermute | solution.py:105
  29.9 12.7 %collective-permute-start.2 = (bf16[528,256]{1,0:T(8,128)(2,1)S(1)}, bf16[528,256]{1,0:T(8,128)(2,1)S(1)}, u32[]{:S(2)}, u32[]{:S(2)}) collective-permute-start(bf16[528,256]{1,0:T(8,128)(2,1)S(1)} %get-tuple-element.83), channel_id=1, source_target_pairs={{0,16},{8,24},{16,0},{24,8},{32,48},{40,56},{48,32},{56,40},{64,80... | collective-permute-start | bytes 811016 | tf_op jit(solution)/shard_map/ppermute | solution.py:96
  36.1 20.4 %collective-permute-start.6 = (bf16[512,512]{1,0:T(8,128)(2,1)S(1)}, bf16[512,512]{1,0:T(8,128)(2,1)S(1)}, u32[]{:S(2)}, u32[]{:S(2)}) collective-permute-start(bf16[512,512]{1,0:T(8,128)(2,1)S(1)} %get-tuple-element.87), channel_id=1, source_target_pairs={{0,16},{8,24},{16,0},{24,8},{32,48},{40,56},{48,32},{56,40},{64,80... | collective-permute-start | bytes 1572872 | tf_op jit(solution)/shard_map/ppermute | solution.py:96
  40.4 16.2 %collective-permute-start.7 = (bf16[512,512]{1,0:T(8,128)(2,1)S(1)}, bf16[512,512]{1,0:T(8,128)(2,1)S(1)}, u32[]{:S(2)}, u32[]{:S(2)}) collective-permute-start(bf16[512,512]{1,0:T(8,128)(2,1)S(1)} %get-tuple-element.88), channel_id=1, source_target_pairs={{0,8},{8,0},{16,24},{24,16},{32,40},{40,32},{48,56},{56,48},{64,72... | collective-permute-start | bytes 1572872 | tf_op jit(solution)/shard_map/ppermute | solution.py:96
  41.2 15.4 %collective-permute-start.8 = (bf16[512,512]{1,0:T(8,128)(2,1)S(1)}, bf16[512,512]{1,0:T(8,128)(2,1)S(1)}, u32[]{:S(2)}, u32[]{:S(2)}) collective-permute-start(bf16[512,512]{1,0:T(8,128)(2,1)S(1)} %get-tuple-element.89), channel_id=1, source_target_pairs={{0,24},{8,16},{16,8},{24,0},{32,56},{40,48},{48,40},{56,32},{64,88... | collective-permute-start | bytes 1572872 | tf_op jit(solution)/shard_map/ppermute | solution.py:96
  41.2 15.4 %collective-permute-start.3 = (bf16[528,256]{1,0:T(8,128)(2,1)S(1)}, bf16[528,256]{1,0:T(8,128)(2,1)S(1)}, u32[]{:S(2)}, u32[]{:S(2)}) collective-permute-start(bf16[528,256]{1,0:T(8,128)(2,1)S(1)} %get-tuple-element.84), channel_id=1, source_target_pairs={{0,8},{8,0},{16,24},{24,16},{32,40},{40,32},{48,56},{56,48},{64,72... | collective-permute-start | bytes 811016 | tf_op jit(solution)/shard_map/ppermute | solution.py:96
  42.6 13.9 %collective-permute-start.4 = (bf16[528,256]{1,0:T(8,128)(2,1)S(1)}, bf16[528,256]{1,0:T(8,128)(2,1)S(1)}, u32[]{:S(2)}, u32[]{:S(2)}) collective-permute-start(bf16[528,256]{1,0:T(8,128)(2,1)S(1)} %get-tuple-element.85), channel_id=1, source_target_pairs={{0,24},{8,16},{16,8},{24,0},{32,56},{40,48},{48,40},{56,32},{64,88... | collective-permute-start | bytes 811016 | tf_op jit(solution)/shard_map/ppermute | solution.py:96
  57.0 6.6 %collective-permute-start.9 = (bf16[144,768]{1,0:T(8,128)(2,1)S(1)}, bf16[144,768]{1,0:T(8,128)(2,1)S(1)}, u32[]{:S(2)}, u32[]{:S(2)}) collective-permute-start(bf16[144,768]{1,0:T(8,128)(2,1)S(1)} %get-tuple-element.92), channel_id=1, source_target_pairs={{0,64},{8,72},{16,80},{24,88},{32,224},{40,232},{48,240},{56,248},... | collective-permute-start | bytes 663560 | tf_op jit(solution)/shard_map/ppermute | solution.py:96
  60.2 5.3 %collective-permute-start.10 = (bf16[144,768]{1,0:T(8,128)(2,1)S(1)}, bf16[144,768]{1,0:T(8,128)(2,1)S(1)}, u32[]{:S(2)}, u32[]{:S(2)}) collective-permute-start(bf16[144,768]{1,0:T(8,128)(2,1)S(1)} %get-tuple-element.93), channel_id=1, source_target_pairs={{0,32},{8,40},{16,48},{24,56},{32,0},{40,8},{48,16},{56,24},{64,96... | collective-permute-start | bytes 663560 | tf_op jit(solution)/shard_map/ppermute | solution.py:96
  60.2 6.0 %collective-permute-start.11 = (bf16[144,768]{1,0:T(8,128)(2,1)S(1)}, bf16[144,768]{1,0:T(8,128)(2,1)S(1)}, u32[]{:S(2)}, u32[]{:S(2)}) collective-permute-start(bf16[144,768]{1,0:T(8,128)(2,1)S(1)} %get-tuple-element.94), channel_id=1, source_target_pairs={{0,224},{8,232},{16,240},{24,248},{32,64},{40,72},{48,80},{56,88},... | collective-permute-start | bytes 663560 | tf_op jit(solution)/shard_map/ppermute | solution.py:96
  66.3 14.7 %collective-permute-start.12 = (bf16[80,512]{1,0:T(8,128)(2,1)S(1)}, bf16[80,512]{1,0:T(8,128)(2,1)S(1)}, u32[]{:S(2)}, u32[]{:S(2)}) collective-permute-start(bf16[80,512]{1,0:T(8,128)(2,1)S(1)} %get-tuple-element.97), channel_id=1, source_target_pairs={{0,96},{8,104},{16,112},{24,120},{32,192},{40,200},{48,208},{56,21... | collective-permute-start | bytes 245768 | tf_op jit(solution)/shard_map/ppermute | solution.py:96
  69.8 11.2 %collective-permute-start.14 = (f32[64,256]{1,0:T(8,128)S(1)}, f32[64,256]{1,0:T(8,128)S(1)}, u32[]{:S(2)}, u32[]{:S(2)}) collective-permute-start(f32[64,256]{1,0:T(8,128)S(1)} %get-tuple-element.99), channel_id=1, source_target_pairs={{0,1},{1,0},{2,3},{3,2},{4,5},{5,4},{6,7},{7,6},{8,9},{9,8},{10,11... | collective-permute-start | bytes 196616 | tf_op jit(solution)/shard_map/ppermute | solution.py:105
  75.8 5.1 %collective-permute-start.13 = (bf16[64,256]{1,0:T(8,128)(2,1)S(1)}, bf16[64,256]{1,0:T(8,128)(2,1)S(1)}, u32[]{:S(2)}, u32[]{:S(2)}) collective-permute-start(bf16[64,256]{1,0:T(8,128)(2,1)S(1)} %get-tuple-element.98), channel_id=1, source_target_pairs={{0,97},{8,105},{16,113},{24,121},{32,193},{40,201},{48,209},{56,21... | collective-permute-start | bytes 98312 | tf_op jit(solution)/shard_map/ppermute | solution.py:96

commit v8 on v7

--- a/solution.py
+++ b/solution.py
@@ -126,15 +126,19 @@
 
 
 def load_kernel(x_hbm, wk_hbm, wv_hbm, tail_ref, wk_ref, wv_ref, x_ref, sem):
-    pairs = ((wk_hbm, wk_ref), (x_hbm.at[1024 - REACH :], x_ref), (wv_hbm, wv_ref))
+    halves = (slice(0, 1024), slice(1024, 2048))
+    pairs = [(x_hbm.at[1024 - REACH :], x_ref)]
+    pairs += [(w_hbm.at[rows], w_ref.at[rows]) for w_hbm, w_ref in ((wk_hbm, wk_ref), (wv_hbm, wv_ref)) for rows in halves]
     copies = [pltpu.make_async_copy(src, dst, sem.at[i]) for i, (src, dst) in enumerate(pairs)]
     for copy in copies:
         copy.start()
-    for copy in copies[:2]:
-        copy.wait()
-    tail_ref[:, :256] = dot(x_ref[...], wk_ref[...]).astype(BF16)
-    copies[2].wait()
-    tail_ref[:, 256:] = dot(x_ref[...], wv_ref[...]).astype(BF16)
+    copies[0].wait()
+    for at, w_ref in enumerate((wk_ref, wv_ref)):
+        total = jnp.zeros((REACH, 256), F32)
+        for i, rows in enumerate(halves):
+            copies[1 + 2 * at + i].wait()
+            total += dot(x_ref[:, rows], w_ref[rows])
+        tail_ref[:, 256 * at : 256 * (at + 1)] = total.astype(BF16)
 
 
 def proj_kernel(x_hbm, wq_hbm, wk_ref, wv_ref, x_tail, tail_ref, q_ref, k_ref, v_ref, x_ref, wq_s, sem):
@@ -493,7 +497,7 @@
     tail, wk, wv, x_tail = call(
         load_kernel, (x_hbm, wk_hbm, wv_hbm),
         (b16(REACH, 512), b16(2048, 256), b16(2048, 256), b16(REACH, 2048)),
-        (dma((3,)),), flops=2 * 256 * 2048 * 512, any_ins=(0, 1, 2),
+        (dma((5,)),), flops=2 * 256 * 2048 * 512, any_ins=(0, 1, 2),
     )
     halo = neighbour(tail, 1)
     query, key, value, x = call(

time: 81.8 us -> 81.9 us (level)
  no operation moved by 1% of the time
where the time goes in v8:
time: 81.9 us; the launch traced here: 81.8 us
  starting transfers between devices  31.2 us (38%)
  waiting for transfers between devices  25.6 us (31%)
  Pallas kernels  24.2 us (30%)
    pallas_call x13, Pallas kernels, call(): pl.pallas_call(kernel, grid=grid, in_specs=specs, out_specs=out_specs, ou...  24.2 us
    ppermute x11, waiting for transfers between devices, exchange(): return lax.ppermute(block, SP + ('core',), level_route(steps, across))  22.3 us
    ppermute x11, starting transfers between devices, exchange(): return lax.ppermute(block, SP + ('core',), level_route(steps, across))  17.8 us
    ppermute x2, starting transfers between devices, core_swap(): return lax.ppermute(block, 'core', [(0, 1), (1, 0)])  8.1 us
    ppermute x2, starting transfers between devices, neighbour(): return lax.ppermute(block, SP, route)  5.29 us
    ppermute x2, waiting for transfers between devices, neighbour(): return lax.ppermute(block, SP, route)  3.24 us
  transfers between devices with their start and end apart: 15, of which 6 were waited for; matrix products, arithmetic and copies ran while one was open for 0% of the time, Pallas kernels for 21%

profile of v8, /device:TPU:11, one launch (start us, length us, event | category | flops | bytes accessed | tf_op | source)
XLA Modules:
  0.0 81.8 jit_solution(12358847003018310612)
XLA Ops:
  0.6 3.0 %shard_map.117 = (bf16[256,512]{1,0:T(8,128)(2,1)S(1)}, bf16[2048,256]{1,0:T(8,128)(2,1)S(1)}, bf16[2048,256]{1,0:T(8,128)(2,1)S(1)}, bf16[256,2048]{1,0:T(8,128)(2,1)S(1)}) custom-call(bf16[1024,2048]{1,0:T(8,128)(2,1)} %x_hbm.3, bf16[2048,256]{1,0:T(8,128)(2,1)} %wk_hbm.1, bf16[2048,256]{1,0:T(8,128)(2,1)} %wv_hbm.1), custom_call_target="tpu_custom_call" | custom-call | flops 536870912 | bytes 9699328 | tf_op jit(solution)/shard_map/pallas_call | solution.py:471
  3.7 3.1 %collective-permute-start = (bf16[256,512]{1,0:T(8,128)(2,1)S(1)}, bf16[256,512]{1,0:T(8,128)(2,1)S(1)}, u32[]{:S(2)}, u32[]{:S(2)}) collective-permute-start(bf16[256,512]{1,0:T(8,128)(2,1)S(1)} %get-tuple-element.59.tail_ref), channel_id=1, source_target_pairs={{0,8},{8,16},{16,24},{24,32},{32,40},{40,48},{48,56},{56,64},{64,7... | collective-permute-start | bytes 786440 | tf_op jit(solution)/shard_map/ppermute | solution.py:486
  6.8 0.0 copy-start
  6.8 0.0 copy-start.1
  6.8 4.7 %shard_map.118 = (bf16[1024,256]{1,0:T(8,128)(2,1)S(1)}, bf16[1024,256]{1,0:T(8,128)(2,1)S(1)}, bf16[1024,256]{1,0:T(8,128)(2,1)S(1)}, bf16[1024,2048]{1,0:T(8,128)(2,1)S(1)}) custom-call(bf16[1024,2048]{1,0:T(8,128)(2,1)} %x_hbm.3, bf16[2048,256]{1,0:T(8,128)(2,1)} %wq_hbm.1, bf16[2048,256]{1,0:T(8,128)(2,1)S(1)} %get-tuple-element.56.wk_ref, ...), custom_call_target="tpu_custom_call" | custom-call | flops 3221225472 | bytes 14417920 | tf_op jit(solution)/shard_map/pallas_call | solution.py:471
  11.5 0.0 copy-done
  11.5 0.0 copy-done.1
  11.5 3.4 %shard_map.119 = (bf16[384,256]{1,0:T(8,128)(2,1)S(1)}, f32[640,512]{1,0:T(8,128)S(1)}, f32[2,384,128]{2,1,0:T(8,128)S(1)}, f32[2,384,128]{2,1,0:T(8,128)S(1)}) custom-call(bf16[1024,256]{1,0:T(8,128)(2,1)S(1)} %get-tuple-element.60.q_ref, bf16[1024,256]{1,0:T(8,128)(2,1)S(1)} %get-tuple-element.61.k_ref, bf16[1024,256]{1,0:T(8,128)(2,1)S(1)} %get-tuple-element.62.v_ref, ...), custom_call_target="tpu_custom_call" | custom-call | flops 452984832 | bytes 4392968 | tf_op jit(solution)/shard_map/pallas_call | solution.py:471
  14.9 0.0 collective-permute-done.halo_ref
  14.9 2.3 %shard_map.120 = (bf16[256,256]{1,0:T(8,128)(2,1)S(1)}, f32[256,512]{1,0:T(8,128)S(1)}, bf16[256,512]{1,0:T(8,128)(2,1)S(1)}, f32[2,384,128]{2,1,0:T(8,128)S(1)}) custom-call(bf16[1024,256]{1,0:T(8,128)(2,1)S(1)} %get-tuple-element.60.q_ref, bf16[1024,256]{1,0:T(8,128)(2,1)S(1)} %get-tuple-element.61.k_ref, bf16[1024,256]{1,0:T(8,128)(2,1)S(1)} %get-tuple-element.62.v_ref, ...), custom_call_target="tpu_custom_call" | custom-call | flops 301989888 | bytes 4456448 | tf_op jit(solution)/shard_map/pallas_call | solution.py:471
  17.3 2.2 %collective-permute-start.1 = (bf16[256,512]{1,0:T(8,128)(2,1)S(1)}, bf16[256,512]{1,0:T(8,128)(2,1)S(1)}, u32[]{:S(2)}, u32[]{:S(2)}) collective-permute-start(bf16[256,512]{1,0:T(8,128)(2,1)S(1)} %get-tuple-element.74), channel_id=1, source_target_pairs={{8,0},{16,8},{24,16},{32,24},{40,32},{48,40},{56,48},{64,56},{72,6... | collective-permute-start | bytes 786440 | tf_op jit(solution)/shard_map/ppermute | solution.py:486
  19.5 3.4 %shard_map.121 = (bf16[1024,256]{1,0:T(8,128)(2,1)S(1)}, bf16[768,256]{1,0:T(8,128)(2,1)S(1)}, bf16[768,256]{1,0:T(8,128)(2,1)S(1)}, f32[256,512]{1,0:T(8,128)S(1)}, f32[2,384,128]{2,1,0:T(8,128)S(1)}) custom-call(bf16[1024,256]{1,0:T(8,128)(2,1)S(1)} %get-tuple-element.60.q_ref, bf16[1024,256]{1,0:T(8,128)(2,1)S(1)} %get-tuple-element.61.k_ref, ...), custom_call_target="tpu_custom_call" | custom-call | flops 452984832 | bytes 7274496 | tf_op jit(solution)/shard_map/pallas_call | solution.py:471
  22.8 3.2 %collective-permute-done.1.back_ref = bf16[256,512]{1,0:T(8,128)(2,1)S(1)} collective-permute-done((bf16[256,512]{1,0:T(8,128)(2,1)S(1)}, bf16[256,512]{1,0:T(8,128)(2,1)S(1)}, u32[]{:S(2)}, u32[]{:S(2)}) %collective-permute-start.1) | collective-permute-done | bytes 262176 | tf_op jit(solution)/shard_map/ppermute | solution.py:486
  26.1 0.1 shard_map.122
  26.2 2.1 %collective-permute-start.5 = (bf16[1024,256]{1,0:T(8,128)(2,1)S(1)}, bf16[1024,256]{1,0:T(8,128)(2,1)S(1)}, u32[]{:S(2)}, u32[]{:S(2)}) collective-permute-start(bf16[1024,256]{1,0:T(8,128)(2,1)S(1)} %get-tuple-element.76.swap_in), channel_id=1, source_target_pairs={{0,1},{1,0},{2,3},{3,2},{4,5},{5,4},{6,7},{7,6},{8,9},{9,8},{10,11... | collective-permute-start | bytes 1572872 | tf_op jit(solution)/shard_map/ppermute | solution.py:105
  28.3 1.9 %shard_map.124 = (bf16[528,256]{1,0:T(8,128)(2,1)S(1)}, bf16[528,256]{1,0:T(8,128)(2,1)S(1)}, bf16[528,256]{1,0:T(8,128)(2,1)S(1)}, bf16[512,256]{1,0:T(8,128)(2,1)S(1)}, f32[4,256]{1,0:T(4,128)S(1)}) custom-call(bf16[1024,2048]{1,0:T(8,128)(2,1)S(1)} %get-tuple-element.80.x_ref, bf16[1024,256]{1,0:T(8,128)(2,1)S(1)} %get-tuple-element.70.dq_in.grad_ref, ...), custom_call_target="tpu_custom_call" | custom-call | flops 1073741824 | bytes 6189056 | tf_op jit(solution)/shard_map/pallas_call | solution.py:471
  30.2 3.1 %collective-permute-start.2 = (bf16[528,256]{1,0:T(8,128)(2,1)S(1)}, bf16[528,256]{1,0:T(8,128)(2,1)S(1)}, u32[]{:S(2)}, u32[]{:S(2)}) collective-permute-start(bf16[528,256]{1,0:T(8,128)(2,1)S(1)} %get-tuple-element.83), channel_id=1, source_target_pairs={{0,16},{8,24},{16,0},{24,8},{32,48},{40,56},{48,32},{56,40},{64,80... | collective-permute-start | bytes 811016 | tf_op jit(solution)/shard_map/ppermute | solution.py:96
  33.2 1.4 %shard_map.125.own_hbm = bf16[2048,256]{1,0:T(8,128)(2,1)S(1)} custom-call(bf16[1024,2048]{1,0:T(8,128)(2,1)S(1)} %get-tuple-element.80.x_ref, bf16[1024,256]{1,0:T(8,128)(2,1)S(1)} %get-tuple-element.75.own_in.grad_ref), custom_call_target="tpu_custom_call" | custom-call | flops 1073741824 | bytes 5767168 | tf_op jit(solution)/shard_map/pallas_call | solution.py:471
  34.6 0.0 collective-permute-done.5.grad_ref
  34.6 1.6 %shard_map.126 = (bf16[512,512]{1,0:T(8,128)(2,1)S(1)}, bf16[512,512]{1,0:T(8,128)(2,1)S(1)}, bf16[512,512]{1,0:T(8,128)(2,1)S(1)}, bf16[512,512]{1,0:T(8,128)(2,1)S(1)}) custom-call(bf16[1024,2048]{1,0:T(8,128)(2,1)S(1)} %get-tuple-element.80.x_ref, bf16[1024,256]{1,0:T(8,128)(2,1)S(1)} %collective-permute-done.5.grad_ref, ...), custom_call_target="tpu_custom_call" | custom-call | flops 1073741824 | bytes 7864320 | tf_op jit(solution)/shard_map/pallas_call | solution.py:471
  36.2 4.3 %collective-permute-start.6 = (bf16[512,512]{1,0:T(8,128)(2,1)S(1)}, bf16[512,512]{1,0:T(8,128)(2,1)S(1)}, u32[]{:S(2)}, u32[]{:S(2)}) collective-permute-start(bf16[512,512]{1,0:T(8,128)(2,1)S(1)} %get-tuple-element.87), channel_id=1, source_target_pairs={{0,16},{8,24},{16,0},{24,8},{32,48},{40,56},{48,32},{56,40},{64,80... | collective-permute-start | bytes 1572872 | tf_op jit(solution)/shard_map/ppermute | solution.py:96
  40.5 0.7 collective-permute-start.7
  41.2 0.0 collective-permute-start.8
  41.2 1.5 %collective-permute-start.3 = (bf16[528,256]{1,0:T(8,128)(2,1)S(1)}, bf16[528,256]{1,0:T(8,128)(2,1)S(1)}, u32[]{:S(2)}, u32[]{:S(2)}) collective-permute-start(bf16[528,256]{1,0:T(8,128)(2,1)S(1)} %get-tuple-element.84), channel_id=1, source_target_pairs={{0,8},{8,0},{16,24},{24,16},{32,40},{40,32},{48,56},{56,48},{64,72... | collective-permute-start | bytes 811016 | tf_op jit(solution)/shard_map/ppermute | solution.py:96
  42.7 0.0 collective-permute-done.2.a0
  42.7 1.2 %collective-permute-start.4 = (bf16[528,256]{1,0:T(8,128)(2,1)S(1)}, bf16[528,256]{1,0:T(8,128)(2,1)S(1)}, u32[]{:S(2)}, u32[]{:S(2)}) collective-permute-start(bf16[528,256]{1,0:T(8,128)(2,1)S(1)} %get-tuple-element.85), channel_id=1, source_target_pairs={{0,24},{8,16},{16,8},{24,0},{32,56},{40,48},{48,40},{56,32},{64,88... | collective-permute-start | bytes 811016 | tf_op jit(solution)/shard_map/ppermute | solution.py:96
  43.9 12.7 %collective-permute-done.3.a1 = bf16[528,256]{1,0:T(8,128)(2,1)S(1)} collective-permute-done((bf16[528,256]{1,0:T(8,128)(2,1)S(1)}, bf16[528,256]{1,0:T(8,128)(2,1)S(1)}, u32[]{:S(2)}, u32[]{:S(2)}) %collective-permute-start.3) | collective-permute-done | bytes 270368 | tf_op jit(solution)/shard_map/ppermute | solution.py:96
  56.7 0.0 collective-permute-done.4.a2
  56.7 0.0 collective-permute-done.6.b0
  56.7 0.0 collective-permute-done.7.b1
  56.7 0.0 collective-permute-done.8.b2
  56.7 0.4 shard_map.127
  57.1 3.2 %collective-permute-start.9 = (bf16[144,768]{1,0:T(8,128)(2,1)S(1)}, bf16[144,768]{1,0:T(8,128)(2,1)S(1)}, u32[]{:S(2)}, u32[]{:S(2)}) collective-permute-start(bf16[144,768]{1,0:T(8,128)(2,1)S(1)} %get-tuple-element.92), channel_id=1, source_target_pairs={{0,64},{8,72},{16,80},{24,88},{32,224},{40,232},{48,240},{56,248},... | collective-permute-start | bytes 663560 | tf_op jit(solution)/shard_map/ppermute | solution.py:96
  60.3 0.0 collective-permute-start.10
  60.3 0.4 collective-permute-start.11
  60.6 3.0 %collective-permute-done.9.g0 = bf16[144,768]{1,0:T(8,128)(2,1)S(1)} collective-permute-done((bf16[144,768]{1,0:T(8,128)(2,1)S(1)}, bf16[144,768]{1,0:T(8,128)(2,1)S(1)}, u32[]{:S(2)}, u32[]{:S(2)}) %collective-permute-start.9) | collective-permute-done | bytes 221216 | tf_op jit(solution)/shard_map/ppermute | solution.py:96
  63.7 1.9 %collective-permute-done.10.g1 = bf16[144,768]{1,0:T(8,128)(2,1)S(1)} collective-permute-done((bf16[144,768]{1,0:T(8,128)(2,1)S(1)}, bf16[144,768]{1,0:T(8,128)(2,1)S(1)}, u32[]{:S(2)}, u32[]{:S(2)}) %collective-permute-start.10) | collective-permute-done | bytes 221216 | tf_op jit(solution)/shard_map/ppermute | solution.py:96
  65.5 0.7 collective-permute-done.11.g2
  66.2 0.1 shard_map.128
  66.4 3.5 %collective-permute-start.12 = (bf16[80,512]{1,0:T(8,128)(2,1)S(1)}, bf16[80,512]{1,0:T(8,128)(2,1)S(1)}, u32[]{:S(2)}, u32[]{:S(2)}) collective-permute-start(bf16[80,512]{1,0:T(8,128)(2,1)S(1)} %get-tuple-element.97), channel_id=1, source_target_pairs={{0,96},{8,104},{16,112},{24,120},{32,192},{40,200},{48,208},{56,21... | collective-permute-start | bytes 245768 | tf_op jit(solution)/shard_map/ppermute | solution.py:96
  69.9 6.0 %collective-permute-start.14 = (f32[64,256]{1,0:T(8,128)S(1)}, f32[64,256]{1,0:T(8,128)S(1)}, u32[]{:S(2)}, u32[]{:S(2)}) collective-permute-start(f32[64,256]{1,0:T(8,128)S(1)} %get-tuple-element.99), channel_id=1, source_target_pairs={{0,1},{1,0},{2,3},{3,2},{4,5},{5,4},{6,7},{7,6},{8,9},{9,8},{10,11... | collective-permute-start | bytes 196616 | tf_op jit(solution)/shard_map/ppermute | solution.py:105
  75.9 0.0 collective-permute-start.13
  75.9 1.2 %shard_map.123 = (bf16[1024,256]{1,0:T(8,128)(2,1)}, bf16[1024,256]{1,0:T(8,128)(2,1)}, bf16[1024,256]{1,0:T(8,128)(2,1)}) custom-call(bf16[1024,256]{1,0:T(8,128)(2,1)S(1)} %get-tuple-element.70.dq_in.grad_ref, bf16[1024,256]{1,0:T(8,128)(2,1)S(1)} %get-tuple-element.75.own_in.grad_ref, bf16[1024,256]{1,0:T(8,128)(2,1)S(1)} %get-tuple-element.76.swap_in), custom_call_target="tpu_custom_call" | custom-call | flops 1048576 | bytes 3145728 | tf_op jit(solution)/shard_map/pallas_call | solution.py:471
  77.1 4.0 %collective-permute-done.13.two_ref = bf16[64,256]{1,0:T(8,128)(2,1)S(1)} collective-permute-done((bf16[64,256]{1,0:T(8,128)(2,1)S(1)}, bf16[64,256]{1,0:T(8,128)(2,1)S(1)}, u32[]{:S(2)}, u32[]{:S(2)}) %collective-permute-start.13) | collective-permute-done | bytes 32800 | tf_op jit(solution)/shard_map/ppermute | solution.py:96
  81.0 0.0 collective-permute-done.14.three_ref
  81.0 0.0 collective-permute-done.12.one_ref
  81.0 0.7 shard_map.129
Async XLA Ops:
  3.7 11.3 %collective-permute-start = (bf16[256,512]{1,0:T(8,128)(2,1)S(1)}, bf16[256,512]{1,0:T(8,128)(2,1)S(1)}, u32[]{:S(2)}, u32[]{:S(2)}) collective-permute-start(bf16[256,512]{1,0:T(8,128)(2,1)S(1)} %get-tuple-element.59.tail_ref), channel_id=1, source_target_pairs={{0,8},{8,16},{16,24},{24,32},{32,40},{40,48},{48,56},{56,64},{64,7... | collective-permute-start | bytes 786440 | tf_op jit(solution)/shard_map/ppermute | solution.py:486
  6.8 4.7 %copy-start = (bf16[1024,256]{1,0:T(8,128)(2,1)S(1)}, bf16[1024,256]{1,0:T(8,128)(2,1)}, u32[]{:S(2)}) copy-start(bf16[1024,256]{1,0:T(8,128)(2,1)} %og_ref.5) | copy-start | bytes 1572868
  6.8 4.7 %copy-start.1 = (f32[2,257]{1,0:T(2,128)S(1)}, f32[2,257]{1,0:T(2,128)}, u32[]{:S(2)}) copy-start(f32[2,257]{1,0:T(2,128)} %rel_ref.1) | copy-start | bytes 6172
  17.3 8.8 %collective-permute-start.1 = (bf16[256,512]{1,0:T(8,128)(2,1)S(1)}, bf16[256,512]{1,0:T(8,128)(2,1)S(1)}, u32[]{:S(2)}, u32[]{:S(2)}) collective-permute-start(bf16[256,512]{1,0:T(8,128)(2,1)S(1)} %get-tuple-element.74), channel_id=1, source_target_pairs={{8,0},{16,8},{24,16},{32,24},{40,32},{48,40},{56,48},{64,56},{72,6... | collective-permute-start | bytes 786440 | tf_op jit(solution)/shard_map/ppermute | solution.py:486
  26.2 8.4 %collective-permute-start.5 = (bf16[1024,256]{1,0:T(8,128)(2,1)S(1)}, bf16[1024,256]{1,0:T(8,128)(2,1)S(1)}, u32[]{:S(2)}, u32[]{:S(2)}) collective-permute-start(bf16[1024,256]{1,0:T(8,128)(2,1)S(1)} %get-tuple-element.76.swap_in), channel_id=1, source_target_pairs={{0,1},{1,0},{2,3},{3,2},{4,5},{5,4},{6,7},{7,6},{8,9},{9,8},{10,11... | collective-permute-start | bytes 1572872 | tf_op jit(solution)/shard_map/ppermute | solution.py:105
  30.2 12.5 %collective-permute-start.2 = (bf16[528,256]{1,0:T(8,128)(2,1)S(1)}, bf16[528,256]{1,0:T(8,128)(2,1)S(1)}, u32[]{:S(2)}, u32[]{:S(2)}) collective-permute-start(bf16[528,256]{1,0:T(8,128)(2,1)S(1)} %get-tuple-element.83), channel_id=1, source_target_pairs={{0,16},{8,24},{16,0},{24,8},{32,48},{40,56},{48,32},{56,40},{64,80... | collective-permute-start | bytes 811016 | tf_op jit(solution)/shard_map/ppermute | solution.py:96
  36.2 20.4 %collective-permute-start.6 = (bf16[512,512]{1,0:T(8,128)(2,1)S(1)}, bf16[512,512]{1,0:T(8,128)(2,1)S(1)}, u32[]{:S(2)}, u32[]{:S(2)}) collective-permute-start(bf16[512,512]{1,0:T(8,128)(2,1)S(1)} %get-tuple-element.87), channel_id=1, source_target_pairs={{0,16},{8,24},{16,0},{24,8},{32,48},{40,56},{48,32},{56,40},{64,80... | collective-permute-start | bytes 1572872 | tf_op jit(solution)/shard_map/ppermute | solution.py:96
  40.5 16.2 %collective-permute-start.7 = (bf16[512,512]{1,0:T(8,128)(2,1)S(1)}, bf16[512,512]{1,0:T(8,128)(2,1)S(1)}, u32[]{:S(2)}, u32[]{:S(2)}) collective-permute-start(bf16[512,512]{1,0:T(8,128)(2,1)S(1)} %get-tuple-element.88), channel_id=1, source_target_pairs={{0,8},{8,0},{16,24},{24,16},{32,40},{40,32},{48,56},{56,48},{64,72... | collective-permute-start | bytes 1572872 | tf_op jit(solution)/shard_map/ppermute | solution.py:96
  41.2 15.4 %collective-permute-start.8 = (bf16[512,512]{1,0:T(8,128)(2,1)S(1)}, bf16[512,512]{1,0:T(8,128)(2,1)S(1)}, u32[]{:S(2)}, u32[]{:S(2)}) collective-permute-start(bf16[512,512]{1,0:T(8,128)(2,1)S(1)} %get-tuple-element.89), channel_id=1, source_target_pairs={{0,24},{8,16},{16,8},{24,0},{32,56},{40,48},{48,40},{56,32},{64,88... | collective-permute-start | bytes 1572872 | tf_op jit(solution)/shard_map/ppermute | solution.py:96
  41.2 15.4 %collective-permute-start.3 = (bf16[528,256]{1,0:T(8,128)(2,1)S(1)}, bf16[528,256]{1,0:T(8,128)(2,1)S(1)}, u32[]{:S(2)}, u32[]{:S(2)}) collective-permute-start(bf16[528,256]{1,0:T(8,128)(2,1)S(1)} %get-tuple-element.84), channel_id=1, source_target_pairs={{0,8},{8,0},{16,24},{24,16},{32,40},{40,32},{48,56},{56,48},{64,72... | collective-permute-start | bytes 811016 | tf_op jit(solution)/shard_map/ppermute | solution.py:96
  42.7 13.9 %collective-permute-start.4 = (bf16[528,256]{1,0:T(8,128)(2,1)S(1)}, bf16[528,256]{1,0:T(8,128)(2,1)S(1)}, u32[]{:S(2)}, u32[]{:S(2)}) collective-permute-start(bf16[528,256]{1,0:T(8,128)(2,1)S(1)} %get-tuple-element.85), channel_id=1, source_target_pairs={{0,24},{8,16},{16,8},{24,0},{32,56},{40,48},{48,40},{56,32},{64,88... | collective-permute-start | bytes 811016 | tf_op jit(solution)/shard_map/ppermute | solution.py:96
  57.1 6.6 %collective-permute-start.9 = (bf16[144,768]{1,0:T(8,128)(2,1)S(1)}, bf16[144,768]{1,0:T(8,128)(2,1)S(1)}, u32[]{:S(2)}, u32[]{:S(2)}) collective-permute-start(bf16[144,768]{1,0:T(8,128)(2,1)S(1)} %get-tuple-element.92), channel_id=1, source_target_pairs={{0,64},{8,72},{16,80},{24,88},{32,224},{40,232},{48,240},{56,248},... | collective-permute-start | bytes 663560 | tf_op jit(solution)/shard_map/ppermute | solution.py:96
  60.3 5.3 %collective-permute-start.10 = (bf16[144,768]{1,0:T(8,128)(2,1)S(1)}, bf16[144,768]{1,0:T(8,128)(2,1)S(1)}, u32[]{:S(2)}, u32[]{:S(2)}) collective-permute-start(bf16[144,768]{1,0:T(8,128)(2,1)S(1)} %get-tuple-element.93), channel_id=1, source_target_pairs={{0,32},{8,40},{16,48},{24,56},{32,0},{40,8},{48,16},{56,24},{64,96... | collective-permute-start | bytes 663560 | tf_op jit(solution)/shard_map/ppermute | solution.py:96
  60.3 6.0 %collective-permute-start.11 = (bf16[144,768]{1,0:T(8,128)(2,1)S(1)}, bf16[144,768]{1,0:T(8,128)(2,1)S(1)}, u32[]{:S(2)}, u32[]{:S(2)}) collective-permute-start(bf16[144,768]{1,0:T(8,128)(2,1)S(1)} %get-tuple-element.94), channel_id=1, source_target_pairs={{0,224},{8,232},{16,240},{24,248},{32,64},{40,72},{48,80},{56,88},... | collective-permute-start | bytes 663560 | tf_op jit(solution)/shard_map/ppermute | solution.py:96
  66.4 14.7 %collective-permute-start.12 = (bf16[80,512]{1,0:T(8,128)(2,1)S(1)}, bf16[80,512]{1,0:T(8,128)(2,1)S(1)}, u32[]{:S(2)}, u32[]{:S(2)}) collective-permute-start(bf16[80,512]{1,0:T(8,128)(2,1)S(1)} %get-tuple-element.97), channel_id=1, source_target_pairs={{0,96},{8,104},{16,112},{24,120},{32,192},{40,200},{48,208},{56,21... | collective-permute-start | bytes 245768 | tf_op jit(solution)/shard_map/ppermute | solution.py:96
  69.9 11.2 %collective-permute-start.14 = (f32[64,256]{1,0:T(8,128)S(1)}, f32[64,256]{1,0:T(8,128)S(1)}, u32[]{:S(2)}, u32[]{:S(2)}) collective-permute-start(f32[64,256]{1,0:T(8,128)S(1)} %get-tuple-element.99), channel_id=1, source_target_pairs={{0,1},{1,0},{2,3},{3,2},{4,5},{5,4},{6,7},{7,6},{8,9},{9,8},{10,11... | collective-permute-start | bytes 196616 | tf_op jit(solution)/shard_map/ppermute | solution.py:105
  75.9 5.1 %collective-permute-start.13 = (bf16[64,256]{1,0:T(8,128)(2,1)S(1)}, bf16[64,256]{1,0:T(8,128)(2,1)S(1)}, u32[]{:S(2)}, u32[]{:S(2)}) collective-permute-start(bf16[64,256]{1,0:T(8,128)(2,1)S(1)} %get-tuple-element.98), channel_id=1, source_target_pairs={{0,97},{8,105},{16,113},{24,121},{32,193},{40,201},{48,209},{56,21... | collective-permute-start | bytes 98312 | tf_op jit(solution)/shard_map/ppermute | solution.py:96
